TPU v7x, 32 devices: a whole 2x2x4 slice. The times are simulated.
32 devices in a mesh: ep: 16 (over z, y, x), tp: 2 (over core).
Axes of the slice: x: 2, y: 2, z: 4, core: 2. Of those that a mesh axis runs over, the one named last changes fastest.
Arguments:
- tokens: bfloat16 [256, 2048], P('ep'), may hold values from -6 to 6
- cache_keys: bfloat16 [256, 2, 64, 1024], P('ep', 'tp'), may hold values from -6 to 6
- cache_values: bfloat16 [256, 2, 64, 1024], P('ep', 'tp'), may hold values from -6 to 6
- cache_lengths: int32 [256], P('ep'), may hold values from 1 to 1024, as said below
- norm_in: float32 [2048], replicated, may hold values from 0.1 to 1.9
- w_query: bfloat16 [2048, 512], P(None, 'tp'), may hold values from -0.125 to 0.125
- w_key: bfloat16 [2048, 128], P(None, 'tp'), may hold values from -0.125 to 0.125
- w_value: bfloat16 [2048, 128], P(None, 'tp'), may hold values from -0.125 to 0.125
- stick_bias: float32 [8], P('tp'), may hold values from -8 to -1.5
- w_output: bfloat16 [512, 2048], P('tp'), may hold values from -0.75 to 0.75
- norm_mid: float32 [2048], replicated, may hold values from 0.1 to 1.9
- routes: int32 [256, 6], P('ep'), may hold values from 0 to 15, all different within a row; in each aligned block of 16 rows (0 to 15, 16 to 31, ...) at most 6 rows name the same one
- route_weights: float32 [256, 6], P('ep'), may hold values from 0.1 to 1
- expert_gate: bfloat16 [16, 2048, 512], P('ep', None, 'tp'), may hold values from -0.125 to 0.125
- expert_up: bfloat16 [16, 2048, 512], P('ep', None, 'tp'), may hold values from -0.125 to 0.125
- expert_down: bfloat16 [16, 512, 2048], P('ep', 'tp'), may hold values from -0.25 to 0.25
- dense_gate: bfloat16 [2048, 256], P('ep'), may hold values from -0.125 to 0.125
- dense_up: bfloat16 [2048, 256], P('ep'), may hold values from -0.125 to 0.125
- dense_down: bfloat16 [256, 2048], P(None, 'ep'), may hold values from -0.375 to 0.375
- mix_gate: float32 [2048], replicated, may hold values from -0.125 to 0.125
- norm_out: float32 [2048], replicated, may hold values from 0.1 to 1.9
Outputs:
- mixed: bfloat16 [256, 2048], P('ep')
- fresh_keys: bfloat16 [256, 128], P('ep', 'tp')
- fresh_values: bfloat16 [256, 128], P('ep', 'tp')
Inputs may be any that keep to these rules, and one draw needn't show every extreme that they name: `cache_lengths`: positions at or past a sequence's length are not read. Among the sequences of one index of ep some sequence has length 1024. `routes`: each row names 6 different experts; among the rows of one index of ep (aligned blocks of 16 rows) no expert is named by more than 6 rows, and that bound is reached.
All inputs are finite; a program needn't handle non-finite values.
Results may differ from a plain program's by a relative error of at most 0.015.
Values may be sent and summed in bfloat16 or wider, within the bound.
No kernel may reach another device: no remote copies, remote signals or barrier semaphores. Data moves between devices by JAX's collectives and lax.ppermute only.
A program may use at most 64 MiB of HBM per device.

v0:
```python
import jax
import jax.numpy as jnp
from jax import lax
from jax.sharding import PartitionSpec as P


def layer_norm(values, gain):
    floats = values.astype(jnp.float32)
    center = jnp.mean(floats, -1, keepdims=True)
    spread = jnp.mean(jnp.square(floats - center), -1, keepdims=True)
    return (floats - center) * lax.rsqrt(spread + 1e-05) * gain


def later_positions(log_keep):
    length = log_keep.shape[-1]
    span = 128
    count = length // span
    lead = log_keep.shape[:-1]
    blocks = log_keep.reshape(lead + (count, span))
    inner = jnp.arange(span)
    within_table = (inner[:, None] > inner[None, :]).astype(jnp.float32)
    within = jnp.einsum("...nb,bc->...nc", blocks, within_table, precision=lax.Precision.HIGHEST)
    totals = jnp.sum(blocks, axis=-1)
    outer = jnp.arange(count)
    outer_table = (outer[:, None] > outer[None, :]).astype(jnp.float32)
    carried = jnp.einsum("...m,mn->...n", totals, outer_table, precision=lax.Precision.HIGHEST)
    return (within + carried[..., None]).reshape(lead + (length,))


def shards(
    tokens,
    cache_keys,
    cache_values,
    cache_lengths,
    norm_in,
    w_query,
    w_key,
    w_value,
    stick_bias,
    w_output,
    norm_mid,
    routes,
    route_weights,
    expert_gate,
    expert_up,
    expert_down,
    dense_gate,
    dense_up,
    dense_down,
    mix_gate,
    norm_out,
):
    normed = layer_norm(tokens, norm_in).astype(jnp.bfloat16)
    queries = jnp.dot(normed, w_query, preferred_element_type=jnp.float32).astype(jnp.bfloat16)
    fresh_keys = jnp.dot(normed, w_key, preferred_element_type=jnp.float32).astype(jnp.bfloat16)
    fresh_values = jnp.dot(normed, w_value, preferred_element_type=jnp.float32).astype(jnp.bfloat16)
    sequences = tokens.shape[0]
    kv_local = cache_keys.shape[1]
    head_dim = cache_keys.shape[2]
    length = cache_keys.shape[3]
    heads_local = stick_bias.shape[0]
    groups = heads_local // kv_local
    query_grid = queries.reshape(sequences, kv_local, groups, head_dim)
    scores = jnp.einsum(
        "skgd,skdc->skgc", query_grid, cache_keys, preferred_element_type=jnp.float32
    ) * head_dim ** (-0.5)
    scores = scores + stick_bias.reshape(kv_local, groups)[None, :, :, None]
    visible = (jnp.arange(length)[None, :] < cache_lengths[:, None])[:, None, None, :]
    log_keep = jnp.where(visible, jax.nn.log_sigmoid(-scores), 0.0)
    later_sum = later_positions(log_keep)
    stick = jnp.where(visible, jnp.exp(jax.nn.log_sigmoid(scores) + later_sum), 0.0).astype(
        jnp.bfloat16
    )
    attended = jnp.einsum(
        "skgc,skdc->skgd", stick, cache_values, preferred_element_type=jnp.float32
    )
    attended = attended.reshape(sequences, heads_local * head_dim).astype(jnp.bfloat16)
    partial_proj = jnp.dot(attended, w_output, preferred_element_type=jnp.float32)
    projected = lax.psum(partial_proj, "tp")
    hidden = layer_norm(normed.astype(jnp.float32) + projected, norm_mid).astype(jnp.bfloat16)
    width = hidden.shape[1]
    topk = routes.shape[1]
    ep_count = lax.axis_size("ep")
    experts = ep_count * expert_gate.shape[0]
    capacity = max(2, (sequences * topk + ep_count - 1) // ep_count)
    flat_routes = routes.reshape(-1)
    onehot = (flat_routes[:, None] == jnp.arange(experts)[None, :]).astype(jnp.float32)
    flat_count = flat_routes.shape[0]
    row_index = jnp.arange(flat_count)
    earlier_table = (row_index[:, None] > row_index[None, :]).astype(jnp.float32)
    before = jnp.dot(earlier_table, onehot, precision=lax.Precision.HIGHEST)
    slot_index = jnp.sum(before * onehot, axis=1).astype(jnp.int32)
    target = flat_routes * capacity + slot_index
    placement = jnp.arange(experts * capacity)[:, None] == target[None, :]
    dispatch = jnp.any(placement.reshape(experts * capacity, sequences, topk), axis=2).astype(
        jnp.bfloat16
    )
    outgoing = jnp.dot(dispatch, hidden, preferred_element_type=jnp.float32).astype(jnp.bfloat16)
    outgoing = outgoing.reshape(ep_count, capacity, width)
    received = lax.all_to_all(outgoing, "ep", split_axis=0, concat_axis=0, tiled=True)
    token_rows = received.reshape(-1, width)
    gate_pre = jnp.dot(token_rows, expert_gate[0], preferred_element_type=jnp.float32)
    up_pre = jnp.dot(token_rows, expert_up[0], preferred_element_type=jnp.float32)
    act = (jax.nn.silu(gate_pre) * up_pre).astype(jnp.bfloat16)
    partial_out = jnp.dot(act, expert_down[0], preferred_element_type=jnp.float32).astype(
        jnp.bfloat16
    )
    expert_out = lax.psum(partial_out, "tp").astype(jnp.float32).astype(jnp.bfloat16)
    returned = lax.all_to_all(
        expert_out.reshape(ep_count, capacity, width), "ep", split_axis=0, concat_axis=0, tiled=True
    )
    selector = jnp.transpose(placement).astype(jnp.bfloat16)
    picked = jnp.dot(selector, returned.reshape(-1, width), preferred_element_type=jnp.float32)
    routed = jnp.sum(picked.reshape(sequences, topk, width) * route_weights[:, :, None], axis=1)
    share = dense_gate.shape[1] // lax.axis_size("tp")
    offset = lax.axis_index("tp") * share
    gate_share = lax.dynamic_slice_in_dim(dense_gate, offset, share, 1)
    up_share = lax.dynamic_slice_in_dim(dense_up, offset, share, 1)
    down_share = lax.dynamic_slice_in_dim(dense_down, offset, share, 0)
    dense_pre = jnp.dot(
        hidden,
        lax.all_gather(gate_share, "ep", axis=0, tiled=True),
        preferred_element_type=jnp.float32,
    )
    dense_lin = jnp.dot(
        hidden,
        lax.all_gather(up_share, "ep", axis=0, tiled=True),
        preferred_element_type=jnp.float32,
    )
    dense_act = (jax.nn.silu(dense_pre) * dense_lin).astype(jnp.bfloat16)
    dense_part = jnp.dot(
        dense_act,
        lax.all_gather(down_share, "ep", axis=1, tiled=True),
        preferred_element_type=jnp.float32,
    )
    dense_out = lax.psum(dense_part.astype(jnp.bfloat16), "tp").astype(jnp.float32)
    mix_weight = jax.nn.sigmoid(
        jnp.dot(hidden.astype(jnp.float32), mix_gate, precision=lax.Precision.HIGHEST)
    )
    combined_rows = hidden.astype(jnp.float32) + routed + mix_weight[:, None] * dense_out
    mixed_rows = layer_norm(combined_rows, norm_out).astype(jnp.bfloat16)
    return (mixed_rows, fresh_keys, fresh_values)


def solution(mesh):
    in_specs = (
        P("ep", None),
        P("ep", "tp", None, None),
        P("ep", "tp", None, None),
        P("ep"),
        P(),
        P(None, "tp"),
        P(None, "tp"),
        P(None, "tp"),
        P("tp"),
        P("tp", None),
        P(),
        P("ep", None),
        P("ep", None),
        P("ep", None, "tp"),
        P("ep", None, "tp"),
        P("ep", "tp", None),
        P("ep", None),
        P("ep", None),
        P(None, "ep"),
        P(),
        P(),
    )
    out_specs = (P("ep", None), P("ep", "tp"), P("ep", "tp"))
    return jax.shard_map(shards, mesh=mesh, in_specs=in_specs, out_specs=out_specs, check_vma=False)
```

profile of v0, /device:TPU:0, one launch (start us, length us, event | category | flops | bytes accessed | tf_op | source)
XLA Modules:
  0.0 213.7 jit_solution(13085332007921850898)
XLA Ops:
  9.1 1.0 fusion.36
  10.1 1.6 convolution_convert_fusion.3
  11.8 1.9 fusion.32
  14.3 1.0 convolution_add_fusion
  15.3 1.0 reshape.200
  16.3 2.4 %fusion.12 = bf16[16,4,64]{2,1,0:T(4,128)(2,1)S(1)} fusion(bf16[16,1,64,1024]{3,2,1,0:T(8,128)(2,1)} %param.23, f32[16,4,1024]{2,1,0:T(4,128)S(1)} %reshape.200, f32[16,4,1024]{2,1,0:T(4,128)} %get-tuple-element.8, pred[16,1024]{1,0:T(8,128)(4,1)S(1)} %iota_compare_fusion.1), kind=kOutput, calls=%fused_computation.14 | convolution fusion | flops 9113600 | bytes 2646016 | tf_op jit(solution)/shard_map/skgc,skdc->skgd/dot_general | solution.py:74
  20.5 45.3 %all_gather.11 = bf16[128,2048]{1,0:T(8,128)(2,1)S(1)} all-gather(bf16[128,128]{1,0:T(8,128)(2,1)S(1)} %constant_dynamic-slice_fusion), channel_id=1, replica_groups=mesh['ep'=16,'tp'=2] {'ep'}, dimensions={1}, use_global_device_ids=true | all-gather | bytes 557056 | tf_op jit(solution)/shard_map/all_gather | solution.py:133
  66.6 38.5 %all_gather.10 = bf16[2048,128]{1,0:T(8,128)(2,1)S(1)} all-gather(bf16[128,128]{1,0:T(8,128)(2,1)S(1)} %constant_dynamic-slice_fusion.1), channel_id=1, replica_groups=mesh['ep'=16,'tp'=2] {'ep'}, dimensions={0}, use_global_device_ids=true | all-gather | bytes 557056 | tf_op jit(solution)/shard_map/all_gather | solution.py:127
  105.8 1.1 fusion.48
  106.9 1.1 multiply_reduce_fusion.1
  108.1 1.0 multiply_convert_fusion.1
  109.1 1.1 convolution_convert_fusion.1
  110.2 1.9 reshape.203
  112.1 4.2 %all-to-all-start = ((bf16[16,6,2048]{2,1,0:T(8,128)(2,1)}), bf16[16,6,2048]{2,1,0:T(8,128)(2,1)}, u32[]{:S(2)}, u32[]{:S(2)}) async-start(bf16[16,6,2048]{2,1,0:T(8,128)(2,1)} %reshape.203), calls=%async_computation | async-start | bytes 1048576 | tf_op jit(solution)/shard_map/all_to_all | solution.py:100
  116.4 44.2 %all_gather.9 = bf16[2048,128]{1,0:T(8,128)(2,1)S(1)} all-gather(bf16[128,128]{1,0:T(8,128)(2,1)S(1)} %constant_dynamic-slice_fusion.2), channel_id=1, replica_groups=mesh['ep'=16,'tp'=2] {'ep'}, dimensions={0}, use_global_device_ids=true | all-gather | bytes 557056 | tf_op jit(solution)/shard_map/all_gather | solution.py:122
  160.8 1.0 convolution_convert_fusion.2
  161.8 1.2 reshape.204
  163.0 1.5 fusion.24
  164.5 2.3 %convolution_convert_fusion = bf16[96,2048]{1,0:T(8,128)(2,1)S(1)} fusion(bf16[96,2048]{1,0:T(8,128)(2,1)S(1)} %reshape.204, bf16[1,256,2048]{2,1,0:T(8,128)(2,1)} %param.36, bf16[1,2048,256]{2,1,0:T(8,128)(2,1)} %param.35, f32[96,256]{1,0:T(8,128)S(1)} %fusion.24), kind=kOutput, calls=%fused_computation.1 | convolution fusion | flops 201670656 | bytes 2981888 | tf_op jit(solution)/shard_map/dot_general | solution.py:105
  167.8 15.0 %all-reduce.6.cloned.1.call-done = (bf16[16,2048]{1,0:T(8,128)(2,1)}, bf16[16,6,2048]{2,1,0:T(8,128)(2,1)}) async-done(((bf16[16,2048]{1,0:T(8,128)(2,1)}, bf16[16,6,2048]{2,1,0:T(8,128)(2,1)}), (bf16[16,2048]{1,0:T(8,128)(2,1)}, bf16[16,6,2048]{2,1,0:T(8,128)(2,1)})) %all-reduce.6.cloned.1.call-update) | async-done | bytes 458768 | tf_op jit(solution)/shard_map/psum | solution.py:136
  182.8 7.0 %all-to-all-start.1 = ((bf16[16,6,2048]{2,1,0:T(8,128)(2,1)}), bf16[16,6,2048]{2,1,0:T(8,128)(2,1)S(1)}, u32[]{:S(2)}, u32[]{:S(2)}) async-start(bf16[16,6,2048]{2,1,0:T(8,128)(2,1)} %get-tuple-element.4), calls=%async_computation.1 | async-start | bytes 1048576 | tf_op jit(solution)/shard_map/all_to_all | solution.py:109
  189.9 1.8 convolution_convert_fusion.5
  191.7 1.8 convolution_convert_fusion.4
  193.6 11.7 %all-to-all-done.1 = bf16[16,6,2048]{2,1,0:T(8,128)(2,1)S(1)} async-done(((bf16[16,6,2048]{2,1,0:T(8,128)(2,1)}), bf16[16,6,2048]{2,1,0:T(8,128)(2,1)S(1)}, u32[]{:S(2)}, u32[]{:S(2)}) %all-to-all-start.1) | async-done | bytes 393248 | tf_op jit(solution)/shard_map/all_to_all | solution.py:109
  (65 shorter events, 8.7 us)
Async XLA Ops:
  7.2 4.6 %copy-start = (bf16[16,1,64,1024]{3,2,1,0:T(8,128)(2,1)S(1)}, bf16[16,1,64,1024]{3,2,1,0:T(8,128)(2,1)}, u32[]{:S(2)}) copy-start(bf16[16,1,64,1024]{3,2,1,0:T(8,128)(2,1)} %param.22) | copy-start | bytes 6291460
  7.2 98.6 %all-reduce.4.cloned.1.call-start = ((), (), s32[]{:S(2)}) async-start(), calls=%async_computation.2 | async-start | bytes 262144 | tf_op jit(solution)/shard_map/psum | solution.py:79
  14.3 4.5 %copy-start.2 = (bf16[256,2048]{1,0:T(8,128)(2,1)S(1)}, bf16[256,2048]{1,0:T(8,128)(2,1)}, u32[]{:S(2)}) copy-start(bf16[256,2048]{1,0:T(8,128)(2,1)} %param.30) | copy-start | bytes 3145732
  16.3 88.8 %copy-start.5 = (s32[16,6]{0,1:T(8,128)S(1)}, s32[16,6]{0,1:T(8,128)}, u32[]{:S(2)}) copy-start(s32[16,6]{0,1:T(8,128)} %param.32) | copy-start | bytes 1156
  18.7 87.0 %copy-start.6 = (bf16[128,256]{1,0:T(8,128)(2,1)S(1)}, bf16[128,256]{1,0:T(8,128)(2,1)}, u32[]{:S(2)}) copy-start(bf16[128,256]{1,0:T(8,128)(2,1)} %param.37) | copy-start | bytes 196612
  18.7 87.1 %copy-start.1 = (bf16[16,2048]{1,0:T(8,128)(2,1)S(1)}, bf16[16,2048]{1,0:T(8,128)(2,1)}, u32[]{:S(2)}) copy-start(bf16[16,2048]{1,0:T(8,128)(2,1)} %param.21) | copy-start | bytes 196612
  18.7 87.1 %copy-start.3 = (f32[2048]{0:T(1024)S(1)}, f32[2048]{0:T(1024)}, u32[]{:S(2)}) copy-start(f32[2048]{0:T(1024)} %param.25) | copy-start | bytes 24580
  18.7 89.3 %copy-start.7 = (f32[2048]{0:T(1024)S(1)}, f32[2048]{0:T(1024)}, u32[]{:S(2)}) copy-start(f32[2048]{0:T(1024)} %param.31) | copy-start | bytes 24580
  112.1 49.7 %all-to-all-start = ((bf16[16,6,2048]{2,1,0:T(8,128)(2,1)}), bf16[16,6,2048]{2,1,0:T(8,128)(2,1)}, u32[]{:S(2)}, u32[]{:S(2)}) async-start(bf16[16,6,2048]{2,1,0:T(8,128)(2,1)} %reshape.203), calls=%async_computation | async-start | bytes 1048576 | tf_op jit(solution)/shard_map/all_to_all | solution.py:100
  116.3 66.5 %all-reduce.6.cloned.1.call-start = ((), (), s32[]{:S(2)}) async-start(), calls=%async_computation.3 | async-start | bytes 1179648 | tf_op jit(solution)/shard_map/psum | solution.py:136
  166.8 26.7 %copy-start.9 = (f32[2048]{0:T(1024)S(1)}, f32[2048]{0:T(1024)}, u32[]{:S(2)}) copy-start(f32[2048]{0:T(1024)} %param.40) | copy-start | bytes 24580
  166.8 38.6 %copy-start.10 = (f32[16,6]{0,1:T(8,128)S(1)}, f32[16,6]{0,1:T(8,128)}, u32[]{:S(2)}) copy-start(f32[16,6]{0,1:T(8,128)} %param.33) | copy-start | bytes 1156
  167.8 38.3 %copy-start.8 = (f32[2048]{0:T(1024)S(1)}, f32[2048]{0:T(1024)}, u32[]{:S(2)}) copy-start(f32[2048]{0:T(1024)} %param.41) | copy-start | bytes 24580
  182.8 22.9 %copy-start.4 = (bf16[16,2048]{1,0:T(8,128)(2,1)S(1)}, bf16[16,2048]{1,0:T(8,128)(2,1)}, u32[]{:S(2)}) copy-start(bf16[16,2048]{1,0:T(8,128)(2,1)} %get-tuple-element.3) | copy-start | bytes 196612
  182.8 22.5 %all-to-all-start.1 = ((bf16[16,6,2048]{2,1,0:T(8,128)(2,1)}), bf16[16,6,2048]{2,1,0:T(8,128)(2,1)S(1)}, u32[]{:S(2)}, u32[]{:S(2)}) async-start(bf16[16,6,2048]{2,1,0:T(8,128)(2,1)} %get-tuple-element.4), calls=%async_computation.1 | async-start | bytes 1048576 | tf_op jit(solution)/shard_map/all_to_all | solution.py:109
Sparse Core Ops, SparseCore 0:
  19.9 20.6 all-reduce.3
  167.9 14.8 all-reduce.5
where the time goes:
time: 215 us; the launch traced here: 214 us
  blocking collectives  128 us (60%)
  waiting for transfers between devices  26.7 us (12%)
  matrix products  18.1 us (8%)
  between operations  14.3 us (7%)
  starting transfers between devices  11.3 us (5%)
  other arithmetic  7.63 us (4%)
  local copies, waits for them, and re-layouts  7.53 us (4%)
    all_gather x1, blocking collectives, shards(): lax.all_gather(down_share, 'ep', axis=1, tiled=True)  45.3 us
    all_gather x1, blocking collectives, shards(): lax.all_gather(gate_share, 'ep', axis=0, tiled=True)  44.2 us
    all_gather x1, blocking collectives, shards(): lax.all_gather(up_share, 'ep', axis=0, tiled=True)  38.5 us
    psum x1, waiting for transfers between devices, shards(): lax.psum(dense_part.astype(jnp.bfloat16), 'tp').astype(jnp.float32)  15 us
    all_to_all x1, waiting for transfers between devices, shards(): lax.all_to_all(expert_out.reshape(ep_count, capacity, width), 'ep', split...  11.7 us
    all_to_all x1, starting transfers between devices, shards(): lax.all_to_all(expert_out.reshape(ep_count, capacity, width), 'ep', split...  6.96 us
  transfers between devices with their start and end apart: 4, of which 2 were waited for; matrix products, arithmetic and copies ran while one was open for 3% of the time, Pallas kernels for 0%

commit v1 on v0

--- a/solution.py
+++ b/solution.py
@@ -27,6 +27,16 @@
     return (within + carried[..., None]).reshape(lead + (length,))
 
 
+def swap_core(values):
+    return lax.ppermute(values, "tp", [(0, 1), (1, 0)])
+
+
+def join_halves(own, other, core):
+    low = jnp.where(core == 0, own, other)
+    high = jnp.where(core == 0, other, own)
+    return jnp.concatenate([low, high], axis=-1)
+
+
 def shards(
     tokens,
     cache_keys,
@@ -50,6 +60,22 @@
     mix_gate,
     norm_out,
 ):
+    share = dense_gate.shape[1] // lax.axis_size("tp")
+    rows = dense_gate.shape[0]
+    ep_count = lax.axis_size("ep")
+    offset = lax.axis_index("tp") * share
+    gate_share = lax.dynamic_slice_in_dim(dense_gate, offset, share, 1)
+    up_share = lax.dynamic_slice_in_dim(dense_up, offset, share, 1)
+    down_share = lax.dynamic_slice_in_dim(dense_down, offset, share, 0)
+    packed = jnp.concatenate(
+        [gate_share.reshape(-1), up_share.reshape(-1), down_share.reshape(-1)]
+    ).reshape(1, -1, 128)
+    packed = jnp.broadcast_to(packed, (ep_count,) + packed.shape[1:])
+    gathered = lax.all_to_all(packed, "ep", split_axis=0, concat_axis=0, tiled=True)
+    gathered = gathered.reshape(ep_count, 3, rows * share)
+    gate_full = gathered[:, 0].reshape(ep_count * rows, share)
+    up_full = gathered[:, 1].reshape(ep_count * rows, share)
+    down_full = jnp.moveaxis(gathered[:, 2].reshape(ep_count, share, -1), 0, 1).reshape(share, -1)
     normed = layer_norm(tokens, norm_in).astype(jnp.bfloat16)
     queries = jnp.dot(normed, w_query, preferred_element_type=jnp.float32).astype(jnp.bfloat16)
     fresh_keys = jnp.dot(normed, w_key, preferred_element_type=jnp.float32).astype(jnp.bfloat16)
@@ -76,11 +102,10 @@
     )
     attended = attended.reshape(sequences, heads_local * head_dim).astype(jnp.bfloat16)
     partial_proj = jnp.dot(attended, w_output, preferred_element_type=jnp.float32)
-    projected = lax.psum(partial_proj, "tp")
+    projected = partial_proj + swap_core(partial_proj)
     hidden = layer_norm(normed.astype(jnp.float32) + projected, norm_mid).astype(jnp.bfloat16)
     width = hidden.shape[1]
     topk = routes.shape[1]
-    ep_count = lax.axis_size("ep")
     experts = ep_count * expert_gate.shape[0]
     capacity = max(2, (sequences * topk + ep_count - 1) // ep_count)
     flat_routes = routes.reshape(-1)
@@ -96,44 +121,36 @@
         jnp.bfloat16
     )
     outgoing = jnp.dot(dispatch, hidden, preferred_element_type=jnp.float32).astype(jnp.bfloat16)
-    outgoing = outgoing.reshape(ep_count, capacity, width)
-    received = lax.all_to_all(outgoing, "ep", split_axis=0, concat_axis=0, tiled=True)
-    token_rows = received.reshape(-1, width)
+    half = width // lax.axis_size("tp")
+    core = lax.axis_index("tp")
+    mine = lax.dynamic_slice_in_dim(outgoing, core * half, half, 1)
+    received = lax.all_to_all(
+        mine.reshape(ep_count, capacity, half), "ep", split_axis=0, concat_axis=0, tiled=True
+    ).reshape(-1, half)
+    token_rows = join_halves(received, swap_core(received), core)
     gate_pre = jnp.dot(token_rows, expert_gate[0], preferred_element_type=jnp.float32)
     up_pre = jnp.dot(token_rows, expert_up[0], preferred_element_type=jnp.float32)
     act = (jax.nn.silu(gate_pre) * up_pre).astype(jnp.bfloat16)
     partial_out = jnp.dot(act, expert_down[0], preferred_element_type=jnp.float32).astype(
         jnp.bfloat16
     )
-    expert_out = lax.psum(partial_out, "tp").astype(jnp.float32).astype(jnp.bfloat16)
+    kept = lax.dynamic_slice_in_dim(partial_out, core * half, half, 1)
+    sent = lax.dynamic_slice_in_dim(partial_out, (1 - core) * half, half, 1)
+    expert_out = (kept.astype(jnp.float32) + swap_core(sent).astype(jnp.float32)).astype(
+        jnp.bfloat16
+    )
     returned = lax.all_to_all(
-        expert_out.reshape(ep_count, capacity, width), "ep", split_axis=0, concat_axis=0, tiled=True
-    )
+        expert_out.reshape(ep_count, capacity, half), "ep", split_axis=0, concat_axis=0, tiled=True
+    ).reshape(-1, half)
     selector = jnp.transpose(placement).astype(jnp.bfloat16)
-    picked = jnp.dot(selector, returned.reshape(-1, width), preferred_element_type=jnp.float32)
-    routed = jnp.sum(picked.reshape(sequences, topk, width) * route_weights[:, :, None], axis=1)
-    share = dense_gate.shape[1] // lax.axis_size("tp")
-    offset = lax.axis_index("tp") * share
-    gate_share = lax.dynamic_slice_in_dim(dense_gate, offset, share, 1)
-    up_share = lax.dynamic_slice_in_dim(dense_up, offset, share, 1)
-    down_share = lax.dynamic_slice_in_dim(dense_down, offset, share, 0)
-    dense_pre = jnp.dot(
-        hidden,
-        lax.all_gather(gate_share, "ep", axis=0, tiled=True),
-        preferred_element_type=jnp.float32,
-    )
-    dense_lin = jnp.dot(
-        hidden,
-        lax.all_gather(up_share, "ep", axis=0, tiled=True),
-        preferred_element_type=jnp.float32,
-    )
+    picked = jnp.dot(selector, returned, preferred_element_type=jnp.float32)
+    routed = jnp.sum(picked.reshape(sequences, topk, half) * route_weights[:, :, None], axis=1)
+    routed = join_halves(routed, swap_core(routed), core)
+    dense_pre = jnp.dot(hidden, gate_full, preferred_element_type=jnp.float32)
+    dense_lin = jnp.dot(hidden, up_full, preferred_element_type=jnp.float32)
     dense_act = (jax.nn.silu(dense_pre) * dense_lin).astype(jnp.bfloat16)
-    dense_part = jnp.dot(
-        dense_act,
-        lax.all_gather(down_share, "ep", axis=1, tiled=True),
-        preferred_element_type=jnp.float32,
-    )
-    dense_out = lax.psum(dense_part.astype(jnp.bfloat16), "tp").astype(jnp.float32)
+    dense_part = jnp.dot(dense_act, down_full, preferred_element_type=jnp.float32)
+    dense_out = dense_part + swap_core(dense_part)
     mix_weight = jax.nn.sigmoid(
         jnp.dot(hidden.astype(jnp.float32), mix_gate, precision=lax.Precision.HIGHEST)
     )

time: 215 us -> 122 us (0.57)
  the two profiles are of different devices: /device:TPU:0 before, /device:TPU:13 now
where the time goes in v1:
time: 122 us; the launch traced here: 121 us
  waiting for transfers between devices  43.4 us (36%)
  local copies, waits for them, and re-layouts  24.7 us (20%)
  starting transfers between devices  18 us (15%)
  matrix products  15.5 us (13%)
  blocking collectives  13.5 us (11%)
  other arithmetic  5.03 us (4%)
    all_to_all x1, waiting for transfers between devices, shards(): lax.all_to_all(packed, 'ep', split_axis=0, concat_axis=0, tiled=True)  32.7 us
    all_to_all x1, blocking collectives, shards(): lax.all_to_all(mine.reshape(ep_count, capacity, half), 'ep', split_axis=0...  13.5 us
    slice x1, local copies, waits for them, and re-layouts, shards(): gate_full = gathered[:, 0].reshape(ep_count * rows, share)  10.1 us
    ppermute x5, starting transfers between devices, swap_core(): return lax.ppermute(values, 'tp', [(0, 1), (1, 0)])  7.33 us
    all_to_all x1, waiting for transfers between devices, shards(): lax.all_to_all(expert_out.reshape(ep_count, capacity, half), 'ep', split_...  7.18 us
    all_to_all x1, starting transfers between devices, shards(): lax.all_to_all(packed, 'ep', split_axis=0, concat_axis=0, tiled=True)  5.96 us
    reshape x1, local copies, waits for them, and re-layouts, shards(): gathered = gathered.reshape(ep_count, 3, rows * share)  5.17 us
    all_to_all x1, starting transfers between devices, shards(): lax.all_to_all(expert_out.reshape(ep_count, capacity, half), 'ep', split_...  4.73 us
  transfers between devices with their start and end apart: 7, of which 6 were waited for; matrix products, arithmetic and copies ran while one was open for 20% of the time, Pallas kernels for 0%

profile of v1, /device:TPU:13, one launch (start us, length us, event | category | flops | bytes accessed | tf_op | source)
XLA Modules:
  0.0 121.3 jit_solution(2685029397561318659)
XLA Ops:
  1.5 1.0 convert_reduce_fusion
  2.5 1.0 fusion.36
  3.6 1.6 %convolution_convert_fusion.1 = bf16[16,256]{1,0:T(8,128)(2,1)S(1)} fusion(bf16[2048,256]{1,0:T(8,128)(2,1)} %param.26, bf16[16,2048]{1,0:T(8,128)(2,1)} %param.21, f32[2048]{0:T(1024)} %param.25, f32[16]{0:T(128)S(1)} %add_rsqrt_fusion.2, f32[16]{0:T(128)S(1)} %broadcast_multiply_fusion.2), kind=kOutput, calls=%fused_computation.11 | convolution fusion | flops 16945152 | bytes 1130624 | tf_op jit(solution)/shard_map/dot_general | solution.py:80
  5.2 1.9 %fusion.32 = (f32[16,4,1024]{2,1,0:T(4,128)S(1)}, f32[16,4,1024]{2,1,0:T(4,128)}) fusion(pred[16,1024]{1,0:T(8,128)(4,1)S(1)} %iota_compare_fusion.1, f32[4]{0:T(128)} %param.29, bf16[16,4,64]{2,1,0:T(4,128)(2,1)S(1)} %reshape.214, bf16[16,1,64,1024]{3,2,1,0:T(8,128)(2,1)S(1)} %copy-done), kind=kOutput, calls=%fused_computation.43 | convolution fusion | flops 9043968 | bytes 2646032 | tf_op jit(solution)/shard_map/skgd,skdc->skgc/dot_general | solution.py:90
  8.7 1.7 %reshape.217 = f32[16,4,1024]{2,1,0:T(4,128)} reshape(f32[16,4,8,128]{3,2,1,0:T(8,128)} %convolution_add_fusion) | data formatting | bytes 524288 | tf_op jit(solution)/shard_map/reshape | solution.py:27
  10.5 2.5 %fusion.11 = bf16[16,4,64]{2,1,0:T(4,128)(2,1)S(1)} fusion(bf16[16,1,64,1024]{3,2,1,0:T(8,128)(2,1)} %param.23, f32[16,4,1024]{2,1,0:T(4,128)} %reshape.217, f32[16,4,1024]{2,1,0:T(4,128)} %get-tuple-element.15, pred[16,1024]{1,0:T(8,128)(4,1)S(1)} %iota_compare_fusion.1), kind=kOutput, calls=%fused_computation.10 | convolution fusion | flops 9113600 | bytes 2646016 | tf_op jit(solution)/shard_map/skgc,skdc->skgd/dot_general | solution.py:100
  16.0 13.5 %all_to_all.15 = bf16[16,6,1024]{2,1,0:T(8,128)(2,1)S(1)} all-to-all(bf16[16,6,1024]{2,1,0:T(8,128)(2,1)S(1)} %reshape.220), channel_id=1, replica_groups=mesh['ep'=16,'tp'=2] {'ep'}, dimensions={0} | all-to-all | bytes 393216 | tf_op jit(solution)/shard_map/all_to_all | solution.py:127
  29.6 2.5 %collective-permute-start.1 = (bf16[96,1024]{1,0:T(8,128)(2,1)S(1)}, bf16[96,1024]{1,0:T(8,128)(2,1)S(1)}, u32[]{:S(2)}, u32[]{:S(2)}) collective-permute-start(bf16[96,1024]{1,0:T(8,128)(2,1)S(1)} %reshape.221), channel_id=1, source_target_pairs={{0,1},{1,0},{2,3},{3,2},{4,5},{5,4},{6,7},{7,6},{8,9},{9,8},{10,11... | collective-permute-start | bytes 589832 | tf_op jit(solution)/shard_map/ppermute | solution.py:31
  32.1 1.1 collective-permute-done.1
  33.2 1.5 %fusion.22 = f32[96,256]{1,0:T(8,128)S(1)} fusion(bf16[1,2048,256]{2,1,0:T(8,128)(2,1)} %param.35, bf16[96,1024]{1,0:T(8,128)(2,1)S(1)} %get-tuple-element.11, bf16[96,1024]{1,0:T(8,128)(2,1)S(1)} %get-tuple-element.10), kind=kOutput, calls=%fused_computation.28 | convolution fusion | flops 101449728 | bytes 1540096 | tf_op jit(solution)/shard_map/dot_general | solution.py:132
  34.8 2.4 %convolution_convert_fusion = bf16[96,2048]{1,0:T(8,128)(2,1)S(1)} fusion(bf16[1,256,2048]{2,1,0:T(8,128)(2,1)} %param.36, f32[96,256]{1,0:T(8,128)S(1)} %fusion.22, bf16[1,2048,256]{2,1,0:T(8,128)(2,1)} %param.34, bf16[96,1024]{1,0:T(8,128)(2,1)S(1)} %get-tuple-element.11, bf16[96,1024]{1,0:T(8,128)(2,1)S(1)} %get-tuple-element.10), kind=kOutput, calls=%fused_computation | convolution fusion | flops 202457088 | bytes 2981888 | tf_op jit(solution)/shard_map/dot_general | solution.py:134
  37.6 1.1 collective-permute-done.2
  39.5 4.7 %all-to-all-start.1 = ((bf16[16,6,1024]{2,1,0:T(8,128)(2,1)}), bf16[16,6,1024]{2,1,0:T(8,128)(2,1)S(1)}, u32[]{:S(2)}, u32[]{:S(2)}) async-start(bf16[16,6,1024]{2,1,0:T(8,128)(2,1)} %reshape.222), calls=%async_computation.1 | async-start | bytes 524288 | tf_op jit(solution)/shard_map/all_to_all | solution.py:142
  44.4 7.2 %all-to-all-done.1 = bf16[16,6,1024]{2,1,0:T(8,128)(2,1)S(1)} async-done(((bf16[16,6,1024]{2,1,0:T(8,128)(2,1)}), bf16[16,6,1024]{2,1,0:T(8,128)(2,1)S(1)}, u32[]{:S(2)}, u32[]{:S(2)}) %all-to-all-start.1) | async-done | bytes 196640 | tf_op jit(solution)/shard_map/all_to_all | solution.py:142
  51.6 1.5 %broadcast_in_dim.17 = bf16[16,384,128]{2,1,0:T(8,128)(2,1)} broadcast(bf16[384,128]{1,0:T(8,128)(2,1)S(1)} %pad_maximum_fusion.3), dimensions={1,2} | broadcast | bytes 1671168 | tf_op jit(solution)/shard_map/broadcast_in_dim | solution.py:73
  53.1 6.0 %all-to-all-start.2 = ((bf16[16,384,128]{2,1,0:T(8,128)(2,1)}), bf16[16,384,128]{2,1,0:T(8,128)(2,1)}, u32[]{:S(2)}, u32[]{:S(2)}) async-start(bf16[16,384,128]{2,1,0:T(8,128)(2,1)} %broadcast_in_dim.17), calls=%async_computation.2 | async-start | bytes 3145728 | tf_op jit(solution)/shard_map/all_to_all | solution.py:74
  61.4 2.3 %collective-permute-start.3 = (f32[16,1024]{1,0:T(8,128)S(1)}, f32[16,1024]{1,0:T(8,128)S(1)}, u32[]{:S(2)}, u32[]{:S(2)}) collective-permute-start(f32[16,1024]{1,0:T(8,128)S(1)} %fusion.10), channel_id=1, source_target_pairs={{0,1},{1,0},{2,3},{3,2},{4,5},{5,4},{6,7},{7,6},{8,9},{9,8},{10,11... | collective-permute-start | bytes 196616 | tf_op jit(solution)/shard_map/ppermute | solution.py:31
  63.7 32.7 %all-to-all-done.2 = bf16[16,384,128]{2,1,0:T(8,128)(2,1)} async-done(((bf16[16,384,128]{2,1,0:T(8,128)(2,1)}), bf16[16,384,128]{2,1,0:T(8,128)(2,1)}, u32[]{:S(2)}, u32[]{:S(2)}) %all-to-all-start.2) | async-done | bytes 1572896 | tf_op jit(solution)/shard_map/all_to_all | solution.py:74
  96.4 5.2 %reshape.224 = bf16[16,3,16384]{2,1,0:T(4,128)(2,1)} reshape(bf16[16,384,128]{2,1,0:T(8,128)(2,1)} %all-to-all-done.2) | data formatting | bytes 3145728 | tf_op jit(solution)/shard_map/reshape | solution.py:75
  101.6 10.1 %slice_reduce_fusion.2 = (bf16[16,16384]{1,0:T(8,128)(2,1)S(1)}, bf16[16,16384]{1,0:T(8,128)(2,1)S(1)}, bf16[16,16384]{1,0:T(8,128)(2,1)S(1)}) fusion(bf16[16,3,16384]{2,1,0:T(4,128)(2,1)} %reshape.224), kind=kLoop, calls=%fused_computation.26 | loop fusion | bytes 3145728 | tf_op jit(solution)/shard_map/slice | solution.py:76
  112.6 2.0 %copy.50 = bf16[128,16,128]{0,2,1:T(8,128)(2,1)} copy(bf16[128,16,128]{2,0,1:T(8,128)(2,1)} %bitcast.72) | data formatting | bytes 1048576 | tf_op jit(solution)/shard_map/transpose | solution.py:78
  114.7 1.0 reshape_squeeze.10
  116.1 1.6 %fusion.16 = f32[16,2048]{1,0:T(8,128)S(1)} fusion(bf16[128,2048]{0,1:T(8,128)(2,1)} %bitcast.71, bf16[16,2048]{1,0:T(8,128)(2,1)S(1)} %multiply_convert_fusion.1, bf16[2048,128]{1,0:T(8,128)(2,1)} %reshape_squeeze.10, f32[16,128]{1,0:T(8,128)S(1)} %fusion.76), kind=kOutput, calls=%fused_computation.18 | convolution fusion | flops 16789504 | bytes 1253376 | tf_op jit(solution)/shard_map/dot_general | solution.py:152
  117.7 1.4 %collective-permute-start.4 = (f32[16,2048]{1,0:T(8,128)S(1)}, f32[16,2048]{1,0:T(8,128)S(1)}, u32[]{:S(2)}, u32[]{:S(2)}) collective-permute-start(f32[16,2048]{1,0:T(8,128)S(1)} %fusion.16), channel_id=1, source_target_pairs={{0,1},{1,0},{2,3},{3,2},{4,5},{5,4},{6,7},{7,6},{8,9},{9,8},{10,11... | collective-permute-start | bytes 393224 | tf_op jit(solution)/shard_map/ppermute | solution.py:31
  (113 shorter events, 12.6 us)
Async XLA Ops:
  7.7 5.3 %copy-start.1 = (bf16[256,2048]{1,0:T(8,128)(2,1)S(1)}, bf16[256,2048]{1,0:T(8,128)(2,1)}, u32[]{:S(2)}) copy-start(bf16[256,2048]{1,0:T(8,128)(2,1)} %param.30) | copy-start | bytes 3145732
  10.5 5.0 %copy-start.4 = (f32[2048]{0:T(1024)S(1)}, f32[2048]{0:T(1024)}, u32[]{:S(2)}) copy-start(f32[2048]{0:T(1024)} %param.31) | copy-start | bytes 24580
  13.3 1.7 %collective-permute-start = (f32[16,2048]{1,0:T(8,128)S(1)}, f32[16,2048]{1,0:T(8,128)S(1)}, u32[]{:S(2)}, u32[]{:S(2)}) collective-permute-start(f32[16,2048]{1,0:T(8,128)S(1)} %fusion.74), channel_id=1, source_target_pairs={{0,1},{1,0},{2,3},{3,2},{4,5},{5,4},{6,7},{7,6},{8,9},{9,8},{10,11... | collective-permute-start | bytes 393224 | tf_op jit(solution)/shard_map/ppermute | solution.py:31
  15.2 18.0 %copy-start.13 = (f32[16]{0:T(128)}, f32[16]{0:T(128)S(1)}, u32[]{:S(2)}) copy-start(f32[16]{0:T(128)S(1)} %broadcast_multiply_fusion.1) | copy-start | bytes 196
  15.5 17.7 %copy-start.18 = (f32[16]{0:T(128)}, f32[16]{0:T(128)S(1)}, u32[]{:S(2)}) copy-start(f32[16]{0:T(128)S(1)} %add_rsqrt_fusion.1) | copy-start | bytes 196
  29.6 3.5 %collective-permute-start.1 = (bf16[96,1024]{1,0:T(8,128)(2,1)S(1)}, bf16[96,1024]{1,0:T(8,128)(2,1)S(1)}, u32[]{:S(2)}, u32[]{:S(2)}) collective-permute-start(bf16[96,1024]{1,0:T(8,128)(2,1)S(1)} %reshape.221), channel_id=1, source_target_pairs={{0,1},{1,0},{2,3},{3,2},{4,5},{5,4},{6,7},{7,6},{8,9},{9,8},{10,11... | collective-permute-start | bytes 589832 | tf_op jit(solution)/shard_map/ppermute | solution.py:31
  34.8 9.5 %copy-start.6 = (bf16[128,256]{1,0:T(8,128)(2,1)S(1)}, bf16[128,256]{1,0:T(8,128)(2,1)}, u32[]{:S(2)}) copy-start(bf16[128,256]{1,0:T(8,128)(2,1)} %param.37) | copy-start | bytes 196612
  34.8 9.5 %copy-start.7 = (bf16[256,128]{1,0:T(8,128)(2,1)S(1)}, bf16[256,128]{1,0:T(8,128)(2,1)}, u32[]{:S(2)}) copy-start(bf16[256,128]{1,0:T(8,128)(2,1)} %param.39) | copy-start | bytes 196612
  34.8 9.5 %copy-start.8 = (bf16[128,256]{1,0:T(8,128)(2,1)S(1)}, bf16[128,256]{1,0:T(8,128)(2,1)}, u32[]{:S(2)}) copy-start(bf16[128,256]{1,0:T(8,128)(2,1)} %param.38) | copy-start | bytes 196612
  37.2 1.5 %collective-permute-start.2 = (bf16[96,1024]{1,0:T(8,128)(2,1)S(1)}, bf16[96,1024]{1,0:T(8,128)(2,1)S(1)}, u32[]{:S(2)}, u32[]{:S(2)}) collective-permute-start(bf16[96,1024]{1,0:T(8,128)(2,1)S(1)} %constant_dynamic-slice_fusion.3), channel_id=1, source_target_pairs={{0,1},{1,0},{2,3},{3,2},{4,5},{5,4},{6,7},{7,6},{8,9},{9,8},{10,11... | collective-permute-start | bytes 589832 | tf_op jit(solution)/shard_map/ppermute | solution.py:31
  39.5 12.1 %all-to-all-start.1 = ((bf16[16,6,1024]{2,1,0:T(8,128)(2,1)}), bf16[16,6,1024]{2,1,0:T(8,128)(2,1)S(1)}, u32[]{:S(2)}, u32[]{:S(2)}) async-start(bf16[16,6,1024]{2,1,0:T(8,128)(2,1)} %reshape.222), calls=%async_computation.1 | async-start | bytes 524288 | tf_op jit(solution)/shard_map/all_to_all | solution.py:142
  44.4 14.7 %copy-start.21 = (s32[96]{0:T(128)S(1)}, s32[96]{0:T(128)}, u32[]{:S(2)}) copy-start(s32[96]{0:T(128)} %copy-done.20) | copy-start | bytes 1156
  44.4 14.7 %copy-start.27 = (f32[96]{0:T(128)S(1)}, f32[96]{0:T(128)}, u32[]{:S(2)}) copy-start(f32[96]{0:T(128)} %copy-done.26) | copy-start | bytes 1156
  44.4 14.8 %copy-start.12 = (f32[16]{0:T(128)S(1)}, f32[16]{0:T(128)}, u32[]{:S(2)}) copy-start(f32[16]{0:T(128)} %copy-done.10) | copy-start | bytes 196
  44.4 14.8 %copy-start.17 = (f32[16]{0:T(128)S(1)}, f32[16]{0:T(128)}, u32[]{:S(2)}) copy-start(f32[16]{0:T(128)} %copy-done.15) | copy-start | bytes 196
  44.4 14.8 %copy-start.22 = (bf16[2048,64]{0,1:T(8,128)(2,1)S(1)}, bf16[2048,64]{0,1:T(8,128)(2,1)}, u32[]{:S(2)}) copy-start(bf16[2048,64]{0,1:T(8,128)(2,1)} %param.27) | copy-start | bytes 786436
  53.1 7.0 %copy-start.23 = (bf16[2048,64]{0,1:T(8,128)(2,1)S(1)}, bf16[2048,64]{0,1:T(8,128)(2,1)}, u32[]{:S(2)}) copy-start(bf16[2048,64]{0,1:T(8,128)(2,1)} %param.28) | copy-start | bytes 786436
  53.1 7.8 %copy-start.24 = (f32[2048]{0:T(1024)S(1)}, f32[2048]{0:T(1024)}, u32[]{:S(2)}) copy-start(f32[2048]{0:T(1024)} %param.40) | copy-start | bytes 24580
  53.1 8.1 %copy-start.25 = (f32[16,6]{0,1:T(8,128)S(1)}, f32[16,6]{0,1:T(8,128)}, u32[]{:S(2)}) copy-start(f32[16,6]{0,1:T(8,128)} %param.33) | copy-start | bytes 1156
  53.1 43.3 %all-to-all-start.2 = ((bf16[16,384,128]{2,1,0:T(8,128)(2,1)}), bf16[16,384,128]{2,1,0:T(8,128)(2,1)}, u32[]{:S(2)}, u32[]{:S(2)}) async-start(bf16[16,384,128]{2,1,0:T(8,128)(2,1)} %broadcast_in_dim.17), calls=%async_computation.2 | async-start | bytes 3145728 | tf_op jit(solution)/shard_map/all_to_all | solution.py:74
  61.4 57.8 %collective-permute-start.3 = (f32[16,1024]{1,0:T(8,128)S(1)}, f32[16,1024]{1,0:T(8,128)S(1)}, u32[]{:S(2)}, u32[]{:S(2)}) collective-permute-start(f32[16,1024]{1,0:T(8,128)S(1)} %fusion.10), channel_id=1, source_target_pairs={{0,1},{1,0},{2,3},{3,2},{4,5},{5,4},{6,7},{7,6},{8,9},{9,8},{10,11... | collective-permute-start | bytes 196616 | tf_op jit(solution)/shard_map/ppermute | solution.py:31
  114.7 5.5 %copy-start.14 = (f32[16]{0:T(128)S(1)}, f32[16]{0:T(128)}, u32[]{:S(2)}) copy-start(f32[16]{0:T(128)} %copy-done.13) | copy-start | bytes 196
  114.7 5.5 %copy-start.19 = (f32[16]{0:T(128)S(1)}, f32[16]{0:T(128)}, u32[]{:S(2)}) copy-start(f32[16]{0:T(128)} %copy-done.18) | copy-start | bytes 196
  117.7 2.4 %collective-permute-start.4 = (f32[16,2048]{1,0:T(8,128)S(1)}, f32[16,2048]{1,0:T(8,128)S(1)}, u32[]{:S(2)}, u32[]{:S(2)}) collective-permute-start(f32[16,2048]{1,0:T(8,128)S(1)} %fusion.16), channel_id=1, source_target_pairs={{0,1},{1,0},{2,3},{3,2},{4,5},{5,4},{6,7},{7,6},{8,9},{9,8},{10,11... | collective-permute-start | bytes 393224 | tf_op jit(solution)/shard_map/ppermute | solution.py:31
  (11 other events, 37.8 us)

commit v2 on v0

v2 whole, which is shorter than its diff:
```python
import functools

import jax
import jax.numpy as jnp
from jax import lax
from jax.experimental import pallas as pl
from jax.experimental.pallas import tpu as pltpu
from jax.sharding import PartitionSpec as P

LANES = 128
F32 = jnp.float32
BF16 = jnp.bfloat16
VMEM = pltpu.VMEM
SMEM = pltpu.SMEM
HBM = pltpu.MemorySpace.HBM


def in_vmem():
    return pl.BlockSpec(memory_space=VMEM)


def in_smem():
    return pl.BlockSpec(memory_space=SMEM)


def in_hbm():
    return pl.BlockSpec(memory_space=HBM)


def params(mib):
    return pltpu.CompilerParams(vmem_limit_bytes=mib << 20)


def cost(flops, moved):
    return pl.CostEstimate(flops=flops, bytes_accessed=moved, transcendentals=0)


def iota(shape, dim):
    return lax.broadcasted_iota(jnp.int32, shape, dim)


def dot(a, b):
    return jnp.dot(a, b, preferred_element_type=F32)


def dot_last(a, b):
    return lax.dot_general(a, b, (((1,), (1,)), ((), ())), preferred_element_type=F32)


def dot_first(a, b):
    return lax.dot_general(a, b, (((0,), (0,)), ((), ())), preferred_element_type=F32)


def norm_rows(floats, gain):
    center = jnp.mean(floats, -1, keepdims=True)
    shifted = floats - center
    spread = jnp.mean(jnp.square(shifted), -1, keepdims=True)
    return shifted * lax.rsqrt(spread + 1e-05) * gain


def split_high(values):
    high = values.astype(BF16)
    return high, values - high.astype(F32)


def attention_kernel(
    lengths, bias, tokens, gain, wq_hbm, k_hbm, v_hbm, wo_hbm, partial, normed, wq, k, v, wo, sems
):
    copies = [
        pltpu.make_async_copy(src, dst, sems.at[i])
        for i, (src, dst) in enumerate(((wq_hbm, wq), (k_hbm, k), (v_hbm, v), (wo_hbm, wo)))
    ]
    for copy in copies:
        copy.start()
    sequences = tokens.shape[0]
    heads = wq.shape[1] * 2 // LANES
    head_dim = LANES // 2
    length = k.shape[1]
    rows = heads * sequences
    wide = sequences * head_dim
    rounded = norm_rows(tokens[...].astype(F32), gain[...]).astype(BF16)
    normed[...] = rounded
    copies[0].wait()
    queries = dot(rounded, wq[...]).astype(BF16).astype(F32) * head_dim ** (-0.5)
    low_lane = iota((sequences, LANES), 1) < head_dim
    own_block = iota((sequences, wide), 1) // head_dim == iota((sequences, wide), 0)
    blocks = []
    for h in range(heads):
        slab = queries[:, h // 2 * LANES : (h // 2 + 1) * LANES]
        turned = pltpu.roll(slab, head_dim, 1)
        both = jnp.where(low_lane, slab, turned) if h % 2 == 0 else jnp.where(low_lane, turned, slab)
        blocks.append(jnp.where(own_block, jnp.concatenate([both] * (wide // LANES), axis=1), 0.0))
    spread_queries = jnp.concatenate(blocks, axis=0).astype(BF16)

    row = iota((rows, 1), 0)
    limit = jnp.zeros((rows, 1), jnp.int32)
    for s in range(sequences):
        limit = jnp.where(row % sequences == s, lengths[s], limit)
    offset = jnp.zeros((rows, 1), F32)
    for h in range(heads):
        offset = jnp.where(row // sequences == h, bias[h], offset)
    visible = iota((rows, length), 1) < limit

    copies[1].wait()
    scores = dot(spread_queries, k[...]) + offset
    tail = jnp.log1p(jnp.exp(-jnp.abs(scores)))
    keep = jnp.where(visible, -(jnp.maximum(scores, 0.0) + tail), 0.0)
    high, rest = split_high(keep)
    middle, rest = split_high(rest)
    low = rest.astype(BF16)
    span = 2 * LANES
    count = length // span
    pieces = [part[:, n * span : (n + 1) * span] for part in (high, middle, low) for n in range(count)]
    after = (iota((span, span), 0) > iota((span, span), 1)).astype(BF16)
    sums = dot(jnp.concatenate(pieces, axis=0), after)
    carry = jnp.zeros((rows, 1), F32)
    later = [None] * count
    for n in reversed(range(count)):
        within = (
            sums[n * rows : (n + 1) * rows]
            + sums[(count + n) * rows : (count + n + 1) * rows]
            + sums[(2 * count + n) * rows : (2 * count + n + 1) * rows]
        )
        later[n] = within + carry
        carry = carry + within[:, 0:1] + keep[:, n * span : n * span + 1]
    later_sum = jnp.concatenate(later, axis=1)
    stick = jnp.where(visible, jnp.exp(jnp.minimum(scores, 0.0) - tail + later_sum), 0.0).astype(BF16)

    copies[2].wait()
    mixed = dot_last(stick, v[...])
    own_rows = iota((rows, wide), 1) // head_dim == iota((rows, wide), 0) % sequences
    mixed = jnp.where(own_rows, mixed, 0.0)
    folded = mixed[:, 0:LANES]
    for j in range(1, wide // LANES):
        folded = folded + mixed[:, j * LANES : (j + 1) * LANES]
    folded = folded + pltpu.roll(folded, head_dim, 1)
    slabs = [
        jnp.where(
            low_lane,
            folded[h * sequences : (h + 1) * sequences],
            folded[(h + 1) * sequences : (h + 2) * sequences],
        )
        for h in range(0, heads, 2)
    ]
    attended = jnp.concatenate(slabs, axis=1).astype(BF16)
    copies[3].wait()
    partial[...] = dot(attended, wo[...])


def attention(tokens, gain, w_query, keys, values, lengths, bias, w_output):
    sequences, kv_local, head_dim, length = keys.shape
    assert kv_local == 1 and head_dim * 2 == LANES
    width = tokens.shape[1]
    wide = sequences * head_dim
    flat = (wide, length)
    return pl.pallas_call(
        attention_kernel,
        out_shape=(
            jax.ShapeDtypeStruct((sequences, width), F32),
            jax.ShapeDtypeStruct((sequences, width), BF16),
        ),
        in_specs=[in_smem(), in_smem(), in_vmem(), in_vmem()] + [in_hbm()] * 4,
        out_specs=(in_vmem(), in_vmem()),
        scratch_shapes=[
            VMEM(w_query.shape, BF16),
            VMEM(flat, BF16),
            VMEM(flat, BF16),
            VMEM(w_output.shape, BF16),
            pltpu.SemaphoreType.DMA((4,)),
        ],
        compiler_params=params(58),
        cost_estimate=cost(1 << 32, 7 << 20),
        name="attention",
    )(lengths, bias, tokens, gain.reshape(1, -1), w_query, keys.reshape(flat), values.reshape(flat), w_output)


def plan_kernel(capacity, routes, weights, place, share):
    topk, sequences = routes.shape
    slots = place.shape[0]
    expert = iota((slots, sequences), 0) // capacity
    hit = jnp.zeros((slots, sequences), F32)
    weight = jnp.zeros((slots, sequences), F32)
    for j in range(topk):
        match = routes[j : j + 1, :] == expert
        hit = jnp.where(match, 1.0, hit)
        weight = jnp.where(match, weights[j : j + 1, :], weight)
    earlier = (iota((sequences, sequences), 0) < iota((sequences, sequences), 1)).astype(BF16)
    rank = dot(hit.astype(BF16), earlier)
    turn = (iota((slots, sequences), 0) % capacity).astype(F32)
    chosen = (hit > 0.0) & (rank == turn)
    place[...] = jnp.where(chosen, 1.0, 0.0).astype(BF16)
    share[...] = jnp.where(chosen, weight, 0.0)


def plan(routes, route_weights, slots, capacity):
    sequences = routes.shape[0]
    return pl.pallas_call(
        functools.partial(plan_kernel, capacity),
        out_shape=(
            jax.ShapeDtypeStruct((slots, sequences), BF16),
            jax.ShapeDtypeStruct((slots, sequences), F32),
        ),
        in_specs=[in_vmem(), in_vmem()],
        out_specs=(in_vmem(), in_vmem()),
        compiler_params=params(8),
        cost_estimate=cost(1 << 20, 1 << 16),
        name="plan",
    )(jnp.transpose(routes), jnp.transpose(route_weights))


def store_rows(scratch, values):
    count, width = values.shape
    parts = width // LANES
    for j in range(parts):
        scratch[pl.ds(j, count, stride=parts), :] = values[:, j * LANES : (j + 1) * LANES]


def load_rows(scratch, count):
    parts = scratch.shape[0] // count
    return jnp.concatenate(
        [scratch[pl.ds(j, count, stride=parts), :] for j in range(parts)], axis=1
    )


def half_of(ref, core, half):
    return ref[:, pl.ds(pl.multiple_of(core * half, half), half)]


def middle_kernel(partial, other, normed, gain, place, hidden, outgoing, scratch):
    _, width = partial.shape
    half = width // 2
    floats = normed[...].astype(F32) + (partial[...] + other[...])
    hidden[...] = norm_rows(floats, gain[...]).astype(BF16)
    mine = half_of(hidden, lax.axis_index("tp"), half)
    store_rows(scratch, dot(place[...], mine))
    outgoing[...] = scratch[...].astype(BF16)


def middle(partial, other, normed, gain, place):
    sequences, width = partial.shape
    packed = (place.shape[0] * (width // 2) // LANES, LANES)
    return pl.pallas_call(
        middle_kernel,
        out_shape=(
            jax.ShapeDtypeStruct((sequences, width), BF16),
            jax.ShapeDtypeStruct(packed, BF16),
        ),
        in_specs=[in_vmem()] * 5,
        out_specs=(in_vmem(), in_vmem()),
        scratch_shapes=[VMEM(packed, F32)],
        compiler_params=params(12),
        cost_estimate=cost(1 << 28, 1 << 20),
        name="middle",
    )(partial, other, normed, gain.reshape(1, -1), place)


def expert_kernel(own, other, gate, up, down, kept, sent, scratch, rows):
    core = lax.axis_index("tp")
    packed = own.shape[0]
    width = gate.shape[0]
    half = width // 2
    count = packed * LANES // half
    scratch[...] = own[...].astype(F32)
    own_rows = load_rows(scratch, count).astype(BF16)
    scratch[...] = other[...].astype(F32)
    other_rows = load_rows(scratch, count).astype(BF16)
    rows[:, pl.ds(pl.multiple_of(core * half, half), half)] = own_rows
    rows[:, pl.ds(pl.multiple_of((1 - core) * half, half), half)] = other_rows
    inputs = rows[...]
    gate_pre = dot(inputs, gate[...])
    up_pre = dot(inputs, up[...])
    act = (jax.nn.silu(gate_pre) * up_pre).astype(BF16)
    store_rows(scratch, dot(act, half_of(down, core, half)))
    kept[...] = scratch[...].astype(BF16)
    store_rows(scratch, dot(act, half_of(down, 1 - core, half)))
    sent[...] = scratch[...].astype(BF16)


def expert(own, other, gate, up, down):
    packed = own.shape
    width = gate.shape[0]
    count = packed[0] * LANES * 2 // width
    return pl.pallas_call(
        expert_kernel,
        out_shape=(jax.ShapeDtypeStruct(packed, BF16), jax.ShapeDtypeStruct(packed, BF16)),
        in_specs=[in_vmem()] * 5,
        out_specs=(in_vmem(), in_vmem()),
        scratch_shapes=[VMEM(packed, F32), VMEM((count, width), BF16)],
        compiler_params=params(24),
        cost_estimate=cost(1 << 30, 4 << 20),
        name="expert",
    )(own, other, gate, up, down)


def add_kernel(a, b, out):
    out[...] = (a[...].astype(F32) + b[...].astype(F32)).astype(BF16)


def add_rounded(a, b):
    return pl.pallas_call(
        add_kernel,
        out_shape=jax.ShapeDtypeStruct(a.shape, BF16),
        in_specs=[in_vmem()] * 2,
        out_specs=in_vmem(),
        compiler_params=params(4),
        cost_estimate=cost(1 << 18, 1 << 19),
        name="add_parts",
    )(a, b)


def combine_kernel(returned, share, out, scratch):
    scratch[...] = returned[...].astype(F32)
    rows = load_rows(scratch, share.shape[0]).astype(BF16)
    high, rest = split_high(share[...])
    out[...] = dot_first(high, rows) + dot_first(rest.astype(BF16), rows)


def combine(returned, share):
    half = returned.shape[0] * LANES // share.shape[0]
    return pl.pallas_call(
        combine_kernel,
        out_shape=jax.ShapeDtypeStruct((share.shape[1], half), F32),
        in_specs=[in_vmem()] * 2,
        out_specs=in_vmem(),
        scratch_shapes=[VMEM(returned.shape, F32)],
        compiler_params=params(8),
        cost_estimate=cost(1 << 24, 1 << 19),
        name="combine",
    )(returned, share)


def last_kernel(own, other, dense, dense_other, hidden, mix_gate, gain, mixed, total):
    core = lax.axis_index("tp")
    half = own.shape[1]
    floats = hidden[...].astype(F32)
    mix = jax.nn.sigmoid(jnp.sum(floats * mix_gate[...], axis=-1, keepdims=True))
    total[...] = floats + mix * (dense[...] + dense_other[...])
    mine = pl.ds(pl.multiple_of(core * half, half), half)
    theirs = pl.ds(pl.multiple_of((1 - core) * half, half), half)
    total[:, mine] = total[:, mine] + own[...]
    total[:, theirs] = total[:, theirs] + other[...]
    mixed[...] = norm_rows(total[...], gain[...]).astype(BF16)


def last(own, other, dense, dense_other, hidden, mix_gate, gain):
    return pl.pallas_call(
        last_kernel,
        out_shape=jax.ShapeDtypeStruct(hidden.shape, BF16),
        in_specs=[in_vmem()] * 7,
        out_specs=in_vmem(),
        scratch_shapes=[VMEM(hidden.shape, F32)],
        compiler_params=params(8),
        cost_estimate=cost(1 << 20, 1 << 20),
        name="last",
    )(own, other, dense, dense_other, hidden, mix_gate.reshape(1, -1), gain.reshape(1, -1))


def fresh_kernel(normed, w_key, w_value, keys, values):
    rows = normed[...]
    keys[...] = dot_last(rows, w_key[...]).astype(BF16)
    values[...] = dot_last(rows, w_value[...]).astype(BF16)


def fresh(normed, w_key, w_value):
    shape = jax.ShapeDtypeStruct((normed.shape[0], w_key.shape[1]), BF16)
    return pl.pallas_call(
        fresh_kernel,
        out_shape=(shape, shape),
        in_specs=[in_vmem()] * 3,
        out_specs=(in_vmem(), in_vmem()),
        compiler_params=params(8),
        cost_estimate=cost(1 << 24, 1 << 19),
        name="fresh",
    )(normed, jnp.transpose(w_key), jnp.transpose(w_value))


def swap_core(values):
    return lax.ppermute(values, "tp", [(0, 1), (1, 0)])


def exchange(packed, ep_count):
    blocks = packed.reshape(ep_count, -1, LANES)
    moved = lax.all_to_all(blocks, "ep", split_axis=0, concat_axis=0, tiled=True)
    return moved.reshape(packed.shape)


def swap_far(values, bit):
    count = lax.axis_size("ep")
    return lax.ppermute(values, "ep", [(i, i ^ bit) for i in range(count)])


def pack_kernel(gate, up, down, packed):
    core = lax.axis_index("tp")
    rows, units = gate.shape
    share = units // 2
    packed[0:rows, 0:share] = half_of(gate, core, share)
    packed[0:rows, share:units] = half_of(up, core, share)
    mine = down[pl.ds(pl.multiple_of(core * share, share), share), :]
    packed[rows:, 0:share] = mine[0 : share // 2]
    packed[rows:, share:units] = mine[share // 2 : share]


def pack(gate, up, down):
    rows, units = gate.shape
    return pl.pallas_call(
        pack_kernel,
        out_shape=jax.ShapeDtypeStruct((rows + units // 4, units), BF16),
        in_specs=[in_vmem()] * 3,
        out_specs=in_vmem(),
        compiler_params=params(8),
        cost_estimate=cost(1 << 18, 1 << 18),
        name="pack",
    )(gate, up, down)


def join_kernel(*refs):
    out, at = refs[-1], 0
    for ref in refs[:-1]:
        out[at : at + ref.shape[0], :] = ref[...]
        at += ref.shape[0]


def join(*blocks):
    rows = sum(block.shape[0] for block in blocks)
    return pl.pallas_call(
        join_kernel,
        out_shape=jax.ShapeDtypeStruct((rows, blocks[0].shape[1]), BF16),
        in_specs=[in_vmem()] * len(blocks),
        out_specs=in_vmem(),
        compiler_params=params(8),
        cost_estimate=cost(1 << 18, 1 << 19),
        name="join",
    )(*blocks)


def dense_kernel(offsets, hidden, *refs):
    sources, out = refs[:-1], refs[-1]
    units = sources[0].shape[1]
    share = units // 2
    rows = LANES
    height = rows + share // 2
    me = lax.axis_index("ep")
    blocks = []
    for ref, group in zip(sources, offsets):
        for n, offset in enumerate(group):
            blocks.append((ref, n * height, (me ^ offset) * rows))
    pre = jnp.zeros((hidden.shape[0], units), F32)
    for j in range(0, len(blocks), 2):
        left = [hidden[:, pl.ds(pl.multiple_of(at, rows), rows)] for _, _, at in blocks[j : j + 2]]
        right = [ref[start : start + rows, :] for ref, start, _ in blocks[j : j + 2]]
        pre = pre + dot(jnp.concatenate(left, axis=1), jnp.concatenate(right, axis=0))
    act = (jax.nn.silu(pre[:, 0:share]) * pre[:, share:units]).astype(BF16)
    for ref, start, at in blocks:
        tail = ref[start + rows : start + height, :]
        down = jnp.concatenate([tail[:, 0:share], tail[:, share:units]], axis=0)
        out[:, pl.ds(pl.multiple_of(at, rows), rows)] = dot(act, down)


def dense(hidden, sources, offsets):
    return pl.pallas_call(
        functools.partial(dense_kernel, offsets),
        out_shape=jax.ShapeDtypeStruct(hidden.shape, F32),
        in_specs=[in_vmem()] * (1 + len(sources)),
        out_specs=in_vmem(),
        compiler_params=params(8),
        cost_estimate=cost(1 << 28, 2 << 20),
        name="dense",
    )(hidden, *sources)


def dense_weights(dense_gate, dense_up, dense_down):
    share = dense_gate.shape[1] // lax.axis_size("tp")
    offset = lax.axis_index("tp") * share
    gate = lax.dynamic_slice_in_dim(dense_gate, offset, share, 1)
    up = lax.dynamic_slice_in_dim(dense_up, offset, share, 1)
    down = lax.dynamic_slice_in_dim(dense_down, offset, share, 0)
    return jnp.concatenate(
        [gate.reshape(-1, LANES), up.reshape(-1, LANES), down.reshape(-1, LANES)]
    )


def dense_narrow(hidden, packed, rows, share):
    count = lax.axis_size("ep")
    packed = packed[None]
    bits = [count >> (n + 1) for n in range(count.bit_length() - 1)]
    for bit in bits:
        packed = jnp.concatenate([packed, swap_far(packed, bit)])
    order = [0] * count
    for j in range(count):
        order[sum(bit for n, bit in enumerate(bits) if j >> n & 1)] = j
    packed = jnp.take(packed[jnp.array(order)], lax.axis_index("ep") ^ jnp.arange(count), axis=0)
    packed = packed.reshape(count, 3, rows * share)
    gate = packed[:, 0].reshape(count * rows, share)
    up = packed[:, 1].reshape(count * rows, share)
    down = jnp.moveaxis(packed[:, 2].reshape(count, share, rows), 0, 1).reshape(share, -1)
    act = (jax.nn.silu(dot(hidden, gate)) * dot(hidden, up)).astype(BF16)
    return dot(act, down)


def shards(
    tokens,
    cache_keys,
    cache_values,
    cache_lengths,
    norm_in,
    w_query,
    w_key,
    w_value,
    stick_bias,
    w_output,
    norm_mid,
    routes,
    route_weights,
    expert_gate,
    expert_up,
    expert_down,
    dense_gate,
    dense_up,
    dense_down,
    mix_gate,
    norm_out,
):
    sequences, topk = routes.shape
    ep_count = lax.axis_size("ep")
    experts = ep_count * expert_gate.shape[0]
    capacity = max(2, (sequences * topk + ep_count - 1) // ep_count)
    slots = experts * capacity
    rows = dense_gate.shape[0]
    share = dense_gate.shape[1] // lax.axis_size("tp")
    wide = rows == LANES and share == LANES
    if wide:
        block = pack(dense_gate, dense_up, dense_down)
        columns = [0]
        bit = ep_count // 2
        far = []
        while bit > 2:
            far.append(swap_far(block, bit))
            columns = columns + [c ^ bit for c in columns]
            if bit > 4 or bit == 4:
                block = join(block, far[-1])
            bit //= 2
    partial, normed = attention(
        tokens, norm_in, w_query, cache_keys, cache_values, cache_lengths, stick_bias, w_output
    )
    place, portion = plan(routes, route_weights, slots, capacity)
    partial_other = swap_core(partial)
    hidden, outgoing = middle(partial, partial_other, normed, norm_mid, place)
    received = exchange(outgoing, ep_count)
    received_other = swap_core(received)
    kept, sent = expert(received, received_other, expert_gate[0], expert_up[0], expert_down[0])
    sent_other = swap_core(sent)
    summed = add_rounded(kept, sent_other)
    returned = exchange(summed, ep_count)
    fresh_keys, fresh_values = fresh(normed, w_key, w_value)
    if wide:
        from_x = swap_far(block, 1)
        from_y = swap_far(block, 2)
        part = block.shape[0] // 2
        diagonal_low = swap_far(from_y[:part], 1)
        diagonal_high = swap_far(from_x[part:], 2)
        count = len(columns) // 2
        offsets = (
            tuple(columns),
            tuple(c ^ 1 for c in columns),
            tuple(c ^ 2 for c in columns),
            tuple(c ^ 3 for c in columns[:count]),
            tuple(c ^ 3 for c in columns[count:]),
        )
        dense_out = dense(hidden, (block, from_x, from_y, diagonal_low, diagonal_high), offsets)
    else:
        packed = dense_weights(dense_gate, dense_up, dense_down)
        dense_out = dense_narrow(hidden, packed, rows, share)
    dense_other = swap_core(dense_out)
    own = combine(returned, portion)
    own_other = swap_core(own)
    mixed = last(own, own_other, dense_out, dense_other, hidden, mix_gate, norm_out)
    return (mixed, fresh_keys, fresh_values)


def solution(mesh):
    in_specs = (
        P("ep", None),
        P("ep", "tp", None, None),
        P("ep", "tp", None, None),
        P("ep"),
        P(),
        P(None, "tp"),
        P(None, "tp"),
        P(None, "tp"),
        P("tp"),
        P("tp", None),
        P(),
        P("ep", None),
        P("ep", None),
        P("ep", None, "tp"),
        P("ep", None, "tp"),
        P("ep", "tp", None),
        P("ep", None),
        P("ep", None),
        P(None, "ep"),
        P(),
        P(),
    )
    out_specs = (P("ep", None), P("ep", "tp"), P("ep", "tp"))
    return jax.shard_map(shards, mesh=mesh, in_specs=in_specs, out_specs=out_specs, check_vma=False)
```

time: 215 us -> 63.1 us (0.29)
  blocking collectives: 128 us -> 0 us
  matrix products: 18.1 us -> 0 us
  between operations: 14.3 us -> 0.88 us
  Pallas kernels: 0 us -> 11.4 us
  starting transfers between devices: 11.3 us -> 22.3 us
  other arithmetic: 7.63 us -> 0 us
  local copies, waits for them, and re-layouts: 7.53 us -> 4.28 us
  waiting for transfers between devices: 26.7 us -> 23.7 us
    all_gather x3 -> x0, blocking collectives: 128 us -> none  [the longest x1 45.3 us: shards(): lax.all_gather(down_share, 'ep', axis=1, tiled=True)]
    ppermute x0 -> x11, waiting for transfers between devices: none -> 23.7 us  [the longest x6 21.2 us: swap_far(): return lax.ppermute(values, 'ep', [(i, i ^ bit) for i in range(count)])]
    dot_general x16 -> x0, matrix products: 18.1 us -> none  [the longest x1 2.36 us: shards(): jnp.einsum('skgc,skdc->skgd', stick, cache_values, preferred_element_type...]
    psum x2 -> x0, waiting for transfers between devices: 15 us -> none  [the longest x1 15 us: shards(): lax.psum(dense_part.astype(jnp.bfloat16), 'tp').astype(jnp.float32)]
    all_to_all x2, waiting for transfers between devices: 11.7 us -> 0.01 us  [exchange(): lax.all_to_all(blocks, 'ep', split_axis=0, concat_axis=0, tiled=True)]
    pallas_call x0 -> x12, Pallas kernels: none -> 11.4 us  [the longest x1 5.7 us: attention(): pl.pallas_call(attention_kernel, out_shape=(jax.ShapeDtypeStruct((sequenc...]
    ppermute x0 -> x11, starting transfers between devices: none -> 10.6 us  [the longest x6 9.39 us: swap_far(): return lax.ppermute(values, 'ep', [(i, i ^ bit) for i in range(count)])]
    reshape x6 -> x0, local copies, waits for them, and re-layouts: 5.29 us -> none  [the longest x1 1.92 us: shards(): outgoing = outgoing.reshape(ep_count, capacity, width)]
  transfers between devices with their start and end apart: 4 -> 13, of which waited for: 2 -> 6; matrix products, arithmetic and copies ran while one was open for 3% -> 0% of each run, Pallas kernels for 0% -> 6%
where the time goes in v2:
time: 63.1 us; the launch traced here: 62.7 us
  waiting for transfers between devices  23.7 us (38%)
  starting transfers between devices  22.3 us (35%)
  Pallas kernels  11.4 us (18%)
  local copies, waits for them, and re-layouts  4.28 us (7%)
  between operations  0.88 us (1%)
    ppermute x6, waiting for transfers between devices, swap_far(): return lax.ppermute(values, 'ep', [(i, i ^ bit) for i in range(count)])  21.2 us
    all_to_all x2, starting transfers between devices, exchange(): lax.all_to_all(blocks, 'ep', split_axis=0, concat_axis=0, tiled=True)  11.7 us
    ppermute x6, starting transfers between devices, swap_far(): return lax.ppermute(values, 'ep', [(i, i ^ bit) for i in range(count)])  9.39 us
    pallas_call x1, Pallas kernels, attention(): pl.pallas_call(attention_kernel, out_shape=(jax.ShapeDtypeStruct((sequenc...  5.7 us
    unnamed x32, local copies, waits for them, and re-layouts  4.25 us
    ppermute x5, waiting for transfers between devices, swap_core(): return lax.ppermute(values, 'tp', [(0, 1), (1, 0)])  2.51 us
  transfers between devices with their start and end apart: 13, of which 6 were waited for; matrix products, arithmetic and copies ran while one was open for 0% of the time, Pallas kernels for 6%

profile of v2, /device:TPU:0, one launch (start us, length us, event | category | flops | bytes accessed | tf_op | source)
XLA Modules:
  0.0 62.7 jit_solution(13601087440295819008)
XLA Ops:
  0.7 5.7 %attention.1 = (f32[16,2048]{1,0:T(8,128)}, bf16[16,2048]{1,0:T(8,128)(2,1)}) custom-call(s32[16]{0:T(128)} %lengths.1, f32[4]{0:T(128)} %bias.1, bf16[16,2048]{1,0:T(8,128)(2,1)} %tokens.1, f32[1,2048]{1,0:T(1,128)} %bitcast.32, bf16[2048,256]{1,0:T(8,128)(2,1)} %wq_hbm.1, bf16[1024,1024]{1,0:T(8,128)(2,1)} %bitcast.30, bf16[1024,1024]{1,0:T(8,128)(2,1)} %bitcast.31, ...), custom_call_target="tpu_custom_call" | custom-call | flops 4294967296 | bytes 7340032 | tf_op jit(solution)/shard_map/attention/pallas_call | solution.py:156
  7.1 1.0 %collective-permute-done.other = f32[16,2048]{1,0:T(8,128)S(1)} collective-permute-done((f32[16,2048]{1,0:T(8,128)}, f32[16,2048]{1,0:T(8,128)S(1)}, u32[]{:S(2)}, u32[]{:S(2)}) %collective-permute-start) | collective-permute-done | bytes 131104 | tf_op jit(solution)/shard_map/ppermute | solution.py:378
  8.2 0.8 %copy-done.2 = bf16[16,2048]{1,0:T(8,128)(2,1)S(1)} copy-done((bf16[16,2048]{1,0:T(8,128)(2,1)S(1)}, bf16[16,2048]{1,0:T(8,128)(2,1)}, u32[]{:S(2)}) %copy-start.2) | copy-done | bytes 65560
  9.0 0.9 %copy-done.14 = f32[16,2048]{1,0:T(8,128)S(1)} copy-done((f32[16,2048]{1,0:T(8,128)S(1)}, f32[16,2048]{1,0:T(8,128)}, u32[]{:S(2)}) %copy-start.14) | copy-done | bytes 131096
  9.9 1.1 %middle.1 = (bf16[16,2048]{1,0:T(8,128)(2,1)S(1)}, bf16[768,128]{1,0:T(8,128)(2,1)}) custom-call(f32[16,2048]{1,0:T(8,128)S(1)} %copy-done.14, f32[16,2048]{1,0:T(8,128)S(1)} %collective-permute-done.other, bf16[16,2048]{1,0:T(8,128)(2,1)S(1)} %copy-done.2, f32[1,2048]{1,0:T(1,128)S(1)} %bitcast.29, bf16[96,16]{1,0:T(8,128)(2,1)S(1)} %get-tuple-element.15.place), custom_call_target="tpu_custom_call" | custom-call | flops 268435456 | bytes 1048576 | tf_op jit(solution)/shard_map/middle/pallas_call | solution.py:242
  11.0 8.2 %all-to-all-start = ((bf16[16,48,128]{2,1,0:T(8,128)(2,1)}), bf16[16,48,128]{2,1,0:T(8,128)(2,1)S(1)}, u32[]{:S(2)}, u32[]{:S(2)}) async-start(bf16[16,48,128]{2,1,0:T(8,128)(2,1)} %bitcast.6), calls=%async_computation | async-start | bytes 393216 | tf_op jit(solution)/shard_map/all_to_all | solution.py:383
  19.3 2.9 %collective-permute-start.4 = (bf16[192,256]{1,0:T(8,128)(2,1)S(1)}, bf16[192,256]{1,0:T(8,128)(2,1)S(1)}, u32[]{:S(2)}, u32[]{:S(2)}) collective-permute-start(bf16[192,256]{1,0:T(8,128)(2,1)S(1)} %pack.1.refs_0_), channel_id=1, source_target_pairs={{0,16},{2,18},{4,20},{6,22},{8,24},{10,26},{12,28},{14,30},{16,0},... | collective-permute-start | bytes 294920 | tf_op jit(solution)/shard_map/ppermute | solution.py:389
  22.2 8.9 %collective-permute-done.4.refs_1_ = bf16[192,256]{1,0:T(8,128)(2,1)S(1)} collective-permute-done((bf16[192,256]{1,0:T(8,128)(2,1)S(1)}, bf16[192,256]{1,0:T(8,128)(2,1)S(1)}, u32[]{:S(2)}, u32[]{:S(2)}) %collective-permute-start.4) | collective-permute-done | bytes 98336 | tf_op jit(solution)/shard_map/ppermute | solution.py:389
  31.3 5.8 %collective-permute-done.5.refs_1_ = bf16[384,256]{1,0:T(8,128)(2,1)S(1)} collective-permute-done((bf16[384,256]{1,0:T(8,128)(2,1)S(1)}, bf16[384,256]{1,0:T(8,128)(2,1)S(1)}, u32[]{:S(2)}, u32[]{:S(2)}) %collective-permute-start.5) | collective-permute-done | bytes 196640 | tf_op jit(solution)/shard_map/ppermute | solution.py:389
  37.2 1.5 %collective-permute-start.7 = (bf16[768,256]{1,0:T(8,128)(2,1)S(1)}, bf16[768,256]{1,0:T(8,128)(2,1)S(1)}, u32[]{:S(2)}, u32[]{:S(2)}) collective-permute-start(bf16[768,256]{1,0:T(8,128)(2,1)S(1)} %join.3.refs_0_), channel_id=1, source_target_pairs={{0,4},{2,6},{4,0},{6,2},{8,12},{10,14},{12,8},{14,10},{16,20},{18,... | collective-permute-start | bytes 1179656 | tf_op jit(solution)/shard_map/ppermute | solution.py:389
  38.7 1.5 %collective-permute-start.6 = (bf16[768,256]{1,0:T(8,128)(2,1)S(1)}, bf16[768,256]{1,0:T(8,128)(2,1)S(1)}, u32[]{:S(2)}, u32[]{:S(2)}) collective-permute-start(bf16[768,256]{1,0:T(8,128)(2,1)S(1)} %join.3.refs_0_), channel_id=1, source_target_pairs={{0,2},{2,0},{4,6},{6,4},{8,10},{10,8},{12,14},{14,12},{16,18},{18,... | collective-permute-start | bytes 1179656 | tf_op jit(solution)/shard_map/ppermute | solution.py:389
  40.2 1.2 %copy-done.12 = bf16[1,2048,256]{2,1,0:T(8,128)(2,1)S(1)} copy-done((bf16[1,2048,256]{2,1,0:T(8,128)(2,1)S(1)}, bf16[1,2048,256]{2,1,0:T(8,128)(2,1)}, u32[]{:S(2)}) %copy-start.12) | copy-done | bytes 1048600
  41.4 1.2 %copy-done.13 = bf16[1,256,2048]{2,1,0:T(8,128)(2,1)S(1)} copy-done((bf16[1,256,2048]{2,1,0:T(8,128)(2,1)S(1)}, bf16[1,256,2048]{2,1,0:T(8,128)(2,1)}, u32[]{:S(2)}) %copy-start.13) | copy-done | bytes 1048600
  42.6 0.9 %expert.1 = (bf16[768,128]{1,0:T(8,128)(2,1)S(1)}, bf16[768,128]{1,0:T(8,128)(2,1)S(1)}) custom-call(bf16[768,128]{1,0:T(8,128)(2,1)S(1)} %bitcast.21, bf16[768,128]{1,0:T(8,128)(2,1)S(1)} %collective-permute-done.1.other, bf16[2048,256]{1,0:T(8,128)(2,1)S(1)} %bitcast.26, bf16[2048,256]{1,0:T(8,128)(2,1)S(1)} %bitcast.27, bf16[256,2048]{1,0:T(8,128)(2,1)S(1)} %bitcast.28), custom_call_target="tpu_custom_call" | custom-call | flops 1073741824 | bytes 4194304 | tf_op jit(solution)/shard_map/expert/pallas_call | solution.py:283
  43.6 1.4 %collective-permute-done.2.b = bf16[768,128]{1,0:T(8,128)(2,1)S(1)} collective-permute-done((bf16[768,128]{1,0:T(8,128)(2,1)S(1)}, bf16[768,128]{1,0:T(8,128)(2,1)S(1)}, u32[]{:S(2)}, u32[]{:S(2)}) %collective-permute-start.2) | collective-permute-done | bytes 196640 | tf_op jit(solution)/shard_map/ppermute | solution.py:378
  45.1 0.7 %add_parts.1 = bf16[768,128]{1,0:T(8,128)(2,1)} custom-call(bf16[768,128]{1,0:T(8,128)(2,1)S(1)} %get-tuple-element.17.a, bf16[768,128]{1,0:T(8,128)(2,1)S(1)} %collective-permute-done.2.b), custom_call_target="tpu_custom_call" | custom-call | flops 262144 | bytes 524288 | tf_op jit(solution)/shard_map/add_parts/pallas_call | solution.py:300
  45.8 3.5 %all-to-all-start.1 = ((bf16[16,48,128]{2,1,0:T(8,128)(2,1)}), bf16[16,48,128]{2,1,0:T(8,128)(2,1)S(1)}, u32[]{:S(2)}, u32[]{:S(2)}) async-start(bf16[16,48,128]{2,1,0:T(8,128)(2,1)} %bitcast.11), calls=%async_computation.1 | async-start | bytes 393216 | tf_op jit(solution)/shard_map/all_to_all | solution.py:383
  49.3 1.9 %collective-permute-start.8 = (bf16[384,256]{1,0:T(8,128)(2,1)S(1)}, bf16[384,256]{1,0:T(8,128)(2,1)S(1)}, u32[]{:S(2)}, u32[]{:S(2)}) collective-permute-start(bf16[384,256]{1,0:T(8,128)(2,1)S(1)} %slice.8), channel_id=1, source_target_pairs={{0,2},{2,0},{4,6},{6,4},{8,10},{10,8},{12,14},{14,12},{16,18},{18,... | collective-permute-start | bytes 589832 | tf_op jit(solution)/shard_map/ppermute | solution.py:389
  51.3 1.5 %collective-permute-start.9 = (bf16[384,256]{1,0:T(8,128)(2,1)S(1)}, bf16[384,256]{1,0:T(8,128)(2,1)S(1)}, u32[]{:S(2)}, u32[]{:S(2)}) collective-permute-start(bf16[384,256]{1,0:T(8,128)(2,1)S(1)} %slice.9), channel_id=1, source_target_pairs={{0,4},{2,6},{4,0},{6,2},{8,12},{10,14},{12,8},{14,10},{16,20},{18,... | collective-permute-start | bytes 589832 | tf_op jit(solution)/shard_map/ppermute | solution.py:389
  52.8 5.5 %collective-permute-done.8.refs_3_ = bf16[384,256]{1,0:T(8,128)(2,1)S(1)} collective-permute-done((bf16[384,256]{1,0:T(8,128)(2,1)S(1)}, bf16[384,256]{1,0:T(8,128)(2,1)S(1)}, u32[]{:S(2)}, u32[]{:S(2)}) %collective-permute-start.8) | collective-permute-done | bytes 196640 | tf_op jit(solution)/shard_map/ppermute | solution.py:389
  58.4 0.9 %collective-permute-done.9.refs_4_ = bf16[384,256]{1,0:T(8,128)(2,1)S(1)} collective-permute-done((bf16[384,256]{1,0:T(8,128)(2,1)S(1)}, bf16[384,256]{1,0:T(8,128)(2,1)S(1)}, u32[]{:S(2)}, u32[]{:S(2)}) %collective-permute-start.9) | collective-permute-done | bytes 196640 | tf_op jit(solution)/shard_map/ppermute | solution.py:389
  59.3 0.7 %dense.1 = f32[16,2048]{1,0:T(8,128)S(1)} custom-call(bf16[16,2048]{1,0:T(8,128)(2,1)S(1)} %get-tuple-element.20.hidden, bf16[768,256]{1,0:T(8,128)(2,1)S(1)} %join.3.refs_0_, bf16[768,256]{1,0:T(8,128)(2,1)S(1)} %collective-permute-done.6.refs_1_, bf16[768,256]{1,0:T(8,128)(2,1)S(1)} %collective-permute-done.7.refs_2_, ...), custom_call_target="tpu_custom_call" | custom-call | flops 268435456 | bytes 2097152 | tf_op jit(solution)/shard_map/dense/pallas_call | solution.py:460
  60.8 0.9 %fresh.1 = (bf16[16,64]{1,0:T(8,128)(2,1)}, bf16[16,64]{1,0:T(8,128)(2,1)}) custom-call(bf16[16,2048]{1,0:T(8,128)(2,1)S(1)} %copy-done.3, bf16[64,2048]{1,0:T(8,128)(2,1)S(1)} %bitcast.18, bf16[64,2048]{1,0:T(8,128)(2,1)S(1)} %bitcast.19), custom_call_target="tpu_custom_call" | custom-call | flops 16777216 | bytes 524288 | tf_op jit(solution)/shard_map/fresh/pallas_call | solution.py:366
  61.7 1.0 %last.1 = bf16[16,2048]{1,0:T(8,128)(2,1)} custom-call(f32[16,1024]{1,0:T(8,128)S(1)} %combine.1.own, f32[16,1024]{1,0:T(8,128)S(1)} %collective-permute-done.3.other, f32[16,2048]{1,0:T(8,128)S(1)} %dense.1, f32[16,2048]{1,0:T(8,128)S(1)} %collective-permute-done.10.dense_other, bf16[16,2048]{1,0:T(8,128)(2,1)S(1)} %get-tuple-element.20.hidden, ...), custom_call_target="tpu_custom_call" | custom-call | flops 1048576 | bytes 1048576 | tf_op jit(solution)/shard_map/last/pallas_call | solution.py:346
  (48 shorter events, 1.9 us)
Async XLA Ops:
  0.6 6.3 %copy-start.9 = (s32[16,6]{0,1:T(8,128)S(1)}, s32[16,6]{0,1:T(8,128)}, u32[]{:S(2)}) copy-start(s32[16,6]{0,1:T(8,128)} %param.32) | copy-start | bytes 1156
  0.7 7.5 %copy-start.15 = (f32[2048]{0:T(1024)S(1)}, f32[2048]{0:T(1024)}, u32[]{:S(2)}) copy-start(f32[2048]{0:T(1024)} %param.31) | copy-start | bytes 24580
  0.7 18.6 %copy-start.4 = (bf16[128,256]{1,0:T(8,128)(2,1)S(1)}, bf16[128,256]{1,0:T(8,128)(2,1)}, u32[]{:S(2)}) copy-start(bf16[128,256]{1,0:T(8,128)(2,1)} %gate.1) | copy-start | bytes 196612
  0.7 18.6 %copy-start.5 = (bf16[128,256]{1,0:T(8,128)(2,1)S(1)}, bf16[128,256]{1,0:T(8,128)(2,1)}, u32[]{:S(2)}) copy-start(bf16[128,256]{1,0:T(8,128)(2,1)} %up.1) | copy-start | bytes 196612
  0.7 18.6 %copy-start.6 = (bf16[256,128]{1,0:T(8,128)(2,1)S(1)}, bf16[256,128]{1,0:T(8,128)(2,1)}, u32[]{:S(2)}) copy-start(bf16[256,128]{1,0:T(8,128)(2,1)} %down.1) | copy-start | bytes 196612
  0.7 39.5 %copy-start.11 = (bf16[1,2048,256]{2,1,0:T(8,128)(2,1)S(1)}, bf16[1,2048,256]{2,1,0:T(8,128)(2,1)}, u32[]{:S(2)}) copy-start(bf16[1,2048,256]{2,1,0:T(8,128)(2,1)} %param.34) | copy-start | bytes 3145732
  6.4 1.8 %collective-permute-start = (f32[16,2048]{1,0:T(8,128)}, f32[16,2048]{1,0:T(8,128)S(1)}, u32[]{:S(2)}, u32[]{:S(2)}) collective-permute-start(f32[16,2048]{1,0:T(8,128)} %get-tuple-element.13.partial), channel_id=1, source_target_pairs={{0,1},{1,0},{2,3},{3,2},{4,5},{5,4},{6,7},{7,6},{8,9},{9,8},{10,11... | collective-permute-start | bytes 393224 | tf_op jit(solution)/shard_map/ppermute | solution.py:378
  11.0 20.2 %all-to-all-start = ((bf16[16,48,128]{2,1,0:T(8,128)(2,1)}), bf16[16,48,128]{2,1,0:T(8,128)(2,1)S(1)}, u32[]{:S(2)}, u32[]{:S(2)}) async-start(bf16[16,48,128]{2,1,0:T(8,128)(2,1)} %bitcast.6), calls=%async_computation | async-start | bytes 393216 | tf_op jit(solution)/shard_map/all_to_all | solution.py:383
  19.3 11.8 %collective-permute-start.4 = (bf16[192,256]{1,0:T(8,128)(2,1)S(1)}, bf16[192,256]{1,0:T(8,128)(2,1)S(1)}, u32[]{:S(2)}, u32[]{:S(2)}) collective-permute-start(bf16[192,256]{1,0:T(8,128)(2,1)S(1)} %pack.1.refs_0_), channel_id=1, source_target_pairs={{0,16},{2,18},{4,20},{6,22},{8,24},{10,26},{12,28},{14,30},{16,0},... | collective-permute-start | bytes 294920 | tf_op jit(solution)/shard_map/ppermute | solution.py:389
  31.1 6.0 %collective-permute-start.5 = (bf16[384,256]{1,0:T(8,128)(2,1)S(1)}, bf16[384,256]{1,0:T(8,128)(2,1)S(1)}, u32[]{:S(2)}, u32[]{:S(2)}) collective-permute-start(bf16[384,256]{1,0:T(8,128)(2,1)S(1)} %join.2.refs_0_), channel_id=1, source_target_pairs={{0,8},{2,10},{4,12},{6,14},{8,0},{10,2},{12,4},{14,6},{16,24},{18,... | collective-permute-start | bytes 589832 | tf_op jit(solution)/shard_map/ppermute | solution.py:389
  31.2 8.9 %collective-permute-start.1 = (bf16[768,128]{1,0:T(8,128)(2,1)S(1)}, bf16[768,128]{1,0:T(8,128)(2,1)S(1)}, u32[]{:S(2)}, u32[]{:S(2)}) collective-permute-start(bf16[768,128]{1,0:T(8,128)(2,1)S(1)} %bitcast.20), channel_id=1, source_target_pairs={{0,1},{1,0},{2,3},{3,2},{4,5},{5,4},{6,7},{7,6},{8,9},{9,8},{10,11... | collective-permute-start | bytes 589832 | tf_op jit(solution)/shard_map/ppermute | solution.py:378
  37.2 12.2 %collective-permute-start.7 = (bf16[768,256]{1,0:T(8,128)(2,1)S(1)}, bf16[768,256]{1,0:T(8,128)(2,1)S(1)}, u32[]{:S(2)}, u32[]{:S(2)}) collective-permute-start(bf16[768,256]{1,0:T(8,128)(2,1)S(1)} %join.3.refs_0_), channel_id=1, source_target_pairs={{0,4},{2,6},{4,0},{6,2},{8,12},{10,14},{12,8},{14,10},{16,20},{18,... | collective-permute-start | bytes 1179656 | tf_op jit(solution)/shard_map/ppermute | solution.py:389
  38.7 12.6 %collective-permute-start.6 = (bf16[768,256]{1,0:T(8,128)(2,1)S(1)}, bf16[768,256]{1,0:T(8,128)(2,1)S(1)}, u32[]{:S(2)}, u32[]{:S(2)}) collective-permute-start(bf16[768,256]{1,0:T(8,128)(2,1)S(1)} %join.3.refs_0_), channel_id=1, source_target_pairs={{0,2},{2,0},{4,6},{6,4},{8,10},{10,8},{12,14},{14,12},{16,18},{18,... | collective-permute-start | bytes 1179656 | tf_op jit(solution)/shard_map/ppermute | solution.py:389
  43.5 17.3 %copy-start = (bf16[2048,64]{0,1:T(8,128)(2,1)S(1)}, bf16[2048,64]{0,1:T(8,128)(2,1)}, u32[]{:S(2)}) copy-start(bf16[2048,64]{0,1:T(8,128)(2,1)} %param.27) | copy-start | bytes 786436
  43.5 17.3 %copy-start.1 = (bf16[2048,64]{0,1:T(8,128)(2,1)S(1)}, bf16[2048,64]{0,1:T(8,128)(2,1)}, u32[]{:S(2)}) copy-start(bf16[2048,64]{0,1:T(8,128)(2,1)} %param.28) | copy-start | bytes 786436
  43.5 17.3 %copy-start.3 = (bf16[16,2048]{1,0:T(8,128)(2,1)S(1)}, bf16[16,2048]{1,0:T(8,128)(2,1)}, u32[]{:S(2)}) copy-start(bf16[16,2048]{1,0:T(8,128)(2,1)} %get-tuple-element.14.normed) | copy-start | bytes 196612
  43.6 1.5 %collective-permute-start.2 = (bf16[768,128]{1,0:T(8,128)(2,1)S(1)}, bf16[768,128]{1,0:T(8,128)(2,1)S(1)}, u32[]{:S(2)}, u32[]{:S(2)}) collective-permute-start(bf16[768,128]{1,0:T(8,128)(2,1)S(1)} %get-tuple-element.18), channel_id=1, source_target_pairs={{0,1},{1,0},{2,3},{3,2},{4,5},{5,4},{6,7},{7,6},{8,9},{9,8},{10,11... | collective-permute-start | bytes 589832 | tf_op jit(solution)/shard_map/ppermute | solution.py:378
  45.1 16.6 %copy-start.7 = (f32[2048]{0:T(1024)S(1)}, f32[2048]{0:T(1024)}, u32[]{:S(2)}) copy-start(f32[2048]{0:T(1024)} %param.40) | copy-start | bytes 24580
  45.1 16.6 %copy-start.8 = (f32[2048]{0:T(1024)S(1)}, f32[2048]{0:T(1024)}, u32[]{:S(2)}) copy-start(f32[2048]{0:T(1024)} %param.41) | copy-start | bytes 24580
  45.8 14.3 %all-to-all-start.1 = ((bf16[16,48,128]{2,1,0:T(8,128)(2,1)}), bf16[16,48,128]{2,1,0:T(8,128)(2,1)S(1)}, u32[]{:S(2)}, u32[]{:S(2)}) async-start(bf16[16,48,128]{2,1,0:T(8,128)(2,1)} %bitcast.11), calls=%async_computation.1 | async-start | bytes 393216 | tf_op jit(solution)/shard_map/all_to_all | solution.py:383
  49.3 9.0 %collective-permute-start.8 = (bf16[384,256]{1,0:T(8,128)(2,1)S(1)}, bf16[384,256]{1,0:T(8,128)(2,1)S(1)}, u32[]{:S(2)}, u32[]{:S(2)}) collective-permute-start(bf16[384,256]{1,0:T(8,128)(2,1)S(1)} %slice.8), channel_id=1, source_target_pairs={{0,2},{2,0},{4,6},{6,4},{8,10},{10,8},{12,14},{14,12},{16,18},{18,... | collective-permute-start | bytes 589832 | tf_op jit(solution)/shard_map/ppermute | solution.py:389
  51.3 8.0 %collective-permute-start.9 = (bf16[384,256]{1,0:T(8,128)(2,1)S(1)}, bf16[384,256]{1,0:T(8,128)(2,1)S(1)}, u32[]{:S(2)}, u32[]{:S(2)}) collective-permute-start(bf16[384,256]{1,0:T(8,128)(2,1)S(1)} %slice.9), channel_id=1, source_target_pairs={{0,4},{2,6},{4,0},{6,2},{8,12},{10,14},{12,8},{14,10},{16,20},{18,... | collective-permute-start | bytes 589832 | tf_op jit(solution)/shard_map/ppermute | solution.py:389
  60.0 1.6 %collective-permute-start.10 = (f32[16,2048]{1,0:T(8,128)S(1)}, f32[16,2048]{1,0:T(8,128)S(1)}, u32[]{:S(2)}, u32[]{:S(2)}) collective-permute-start(f32[16,2048]{1,0:T(8,128)S(1)} %dense.1), channel_id=1, source_target_pairs={{0,1},{1,0},{2,3},{3,2},{4,5},{5,4},{6,7},{7,6},{8,9},{9,8},{10,11... | collective-permute-start | bytes 393224 | tf_op jit(solution)/shard_map/ppermute | solution.py:378
  60.3 1.4 %collective-permute-start.3 = (f32[16,1024]{1,0:T(8,128)S(1)}, f32[16,1024]{1,0:T(8,128)S(1)}, u32[]{:S(2)}, u32[]{:S(2)}) collective-permute-start(f32[16,1024]{1,0:T(8,128)S(1)} %combine.1.own), channel_id=1, source_target_pairs={{0,1},{1,0},{2,3},{3,2},{4,5},{5,4},{6,7},{7,6},{8,9},{9,8},{10,11... | collective-permute-start | bytes 196616 | tf_op jit(solution)/shard_map/ppermute | solution.py:378
  (5 other events, 10.5 us)

commit v3 on v2

--- a/solution.py
+++ b/solution.py
@@ -7,7 +7,9 @@
 from jax.experimental.pallas import tpu as pltpu
 from jax.sharding import PartitionSpec as P
 
+
 LANES = 128
+CHUNKS = 4
 F32 = jnp.float32
 BF16 = jnp.bfloat16
 VMEM = pltpu.VMEM
@@ -63,15 +65,33 @@
     return high, values - high.astype(F32)
 
 
+def chunked(src, dst, sems, index):
+    size = dst.shape[0] // CHUNKS
+    return [
+        pltpu.make_async_copy(
+            src.at[pl.ds(c * size, size)], dst.at[pl.ds(c * size, size)], sems.at[index, c]
+        )
+        for c in range(CHUNKS)
+    ]
+
+
+def start_all(copies):
+    for copy in copies:
+        copy.start()
+
+
+def wait_all(copies):
+    for copy in copies:
+        copy.wait()
+
+
 def attention_kernel(
-    lengths, bias, tokens, gain, wq_hbm, k_hbm, v_hbm, wo_hbm, partial, normed, wq, k, v, wo, sems
+    lengths, bias, tokens, gain, wq_hbm, k_hbm, v_hbm, wo_hbm, partial, wq, k, v, wo, sems
 ):
     copies = [
-        pltpu.make_async_copy(src, dst, sems.at[i])
-        for i, (src, dst) in enumerate(((wq_hbm, wq), (k_hbm, k), (v_hbm, v), (wo_hbm, wo)))
+        chunked(src, dst, sems, i) for i, (src, dst) in enumerate(((wq_hbm, wq), (k_hbm, k), (v_hbm, v), (wo_hbm, wo)))
     ]
-    for copy in copies:
-        copy.start()
+    start_all(copies[0] + copies[1])
     sequences = tokens.shape[0]
     heads = wq.shape[1] * 2 // LANES
     head_dim = LANES // 2
@@ -79,8 +99,8 @@
     rows = heads * sequences
     wide = sequences * head_dim
     rounded = norm_rows(tokens[...].astype(F32), gain[...]).astype(BF16)
-    normed[...] = rounded
-    copies[0].wait()
+    wait_all(copies[0])
+    start_all(copies[2] + copies[3])
     queries = dot(rounded, wq[...]).astype(BF16).astype(F32) * head_dim ** (-0.5)
     low_lane = iota((sequences, LANES), 1) < head_dim
     own_block = iota((sequences, wide), 1) // head_dim == iota((sequences, wide), 0)
@@ -101,7 +121,7 @@
         offset = jnp.where(row // sequences == h, bias[h], offset)
     visible = iota((rows, length), 1) < limit
 
-    copies[1].wait()
+    wait_all(copies[1])
     scores = dot(spread_queries, k[...]) + offset
     tail = jnp.log1p(jnp.exp(-jnp.abs(scores)))
     keep = jnp.where(visible, -(jnp.maximum(scores, 0.0) + tail), 0.0)
@@ -126,7 +146,7 @@
     later_sum = jnp.concatenate(later, axis=1)
     stick = jnp.where(visible, jnp.exp(jnp.minimum(scores, 0.0) - tail + later_sum), 0.0).astype(BF16)
 
-    copies[2].wait()
+    wait_all(copies[2])
     mixed = dot_last(stick, v[...])
     own_rows = iota((rows, wide), 1) // head_dim == iota((rows, wide), 0) % sequences
     mixed = jnp.where(own_rows, mixed, 0.0)
@@ -143,7 +163,7 @@
         for h in range(0, heads, 2)
     ]
     attended = jnp.concatenate(slabs, axis=1).astype(BF16)
-    copies[3].wait()
+    wait_all(copies[3])
     partial[...] = dot(attended, wo[...])
 
 
@@ -155,26 +175,23 @@
     flat = (wide, length)
     return pl.pallas_call(
         attention_kernel,
-        out_shape=(
-            jax.ShapeDtypeStruct((sequences, width), F32),
-            jax.ShapeDtypeStruct((sequences, width), BF16),
-        ),
+        out_shape=jax.ShapeDtypeStruct((sequences, width), F32),
         in_specs=[in_smem(), in_smem(), in_vmem(), in_vmem()] + [in_hbm()] * 4,
-        out_specs=(in_vmem(), in_vmem()),
+        out_specs=in_vmem(),
         scratch_shapes=[
             VMEM(w_query.shape, BF16),
             VMEM(flat, BF16),
             VMEM(flat, BF16),
             VMEM(w_output.shape, BF16),
-            pltpu.SemaphoreType.DMA((4,)),
+            pltpu.SemaphoreType.DMA((4, CHUNKS)),
         ],
-        compiler_params=params(58),
+        compiler_params=params(53),
         cost_estimate=cost(1 << 32, 7 << 20),
         name="attention",
     )(lengths, bias, tokens, gain.reshape(1, -1), w_query, keys.reshape(flat), values.reshape(flat), w_output)
 
 
-def plan_kernel(capacity, routes, weights, place, share):
+def plan_kernel(capacity, routes, weights, partial, tokens, gain, place, share, base, normed):
     topk, sequences = routes.shape
     slots = place.shape[0]
     expert = iota((slots, sequences), 0) // capacity
@@ -190,22 +207,27 @@
     chosen = (hit > 0.0) & (rank == turn)
     place[...] = jnp.where(chosen, 1.0, 0.0).astype(BF16)
     share[...] = jnp.where(chosen, weight, 0.0)
-
-
-def plan(routes, route_weights, slots, capacity):
+    rounded = norm_rows(tokens[...].astype(F32), gain[...]).astype(BF16)
+    normed[...] = rounded
+    base[...] = rounded.astype(F32) + partial[...]
+
+
+def plan(routes, route_weights, partial, tokens, gain, slots, capacity):
     sequences = routes.shape[0]
     return pl.pallas_call(
         functools.partial(plan_kernel, capacity),
         out_shape=(
             jax.ShapeDtypeStruct((slots, sequences), BF16),
             jax.ShapeDtypeStruct((slots, sequences), F32),
+            jax.ShapeDtypeStruct(tokens.shape, F32),
+            jax.ShapeDtypeStruct(tokens.shape, BF16),
         ),
-        in_specs=[in_vmem(), in_vmem()],
-        out_specs=(in_vmem(), in_vmem()),
+        in_specs=[in_vmem()] * 5,
+        out_specs=(in_vmem(),) * 4,
         compiler_params=params(8),
         cost_estimate=cost(1 << 20, 1 << 16),
         name="plan",
-    )(jnp.transpose(routes), jnp.transpose(route_weights))
+    )(jnp.transpose(routes), jnp.transpose(route_weights), partial, tokens, gain.reshape(1, -1))
 
 
 def store_rows(scratch, values):
@@ -226,18 +248,16 @@
     return ref[:, pl.ds(pl.multiple_of(core * half, half), half)]
 
 
-def middle_kernel(partial, other, normed, gain, place, hidden, outgoing, scratch):
-    _, width = partial.shape
-    half = width // 2
-    floats = normed[...].astype(F32) + (partial[...] + other[...])
-    hidden[...] = norm_rows(floats, gain[...]).astype(BF16)
+def middle_kernel(base, other, gain, place, hidden, outgoing, scratch):
+    half = base.shape[1] // 2
+    hidden[...] = norm_rows(base[...] + other[...], gain[...]).astype(BF16)
     mine = half_of(hidden, lax.axis_index("tp"), half)
     store_rows(scratch, dot(place[...], mine))
     outgoing[...] = scratch[...].astype(BF16)
 
 
-def middle(partial, other, normed, gain, place):
-    sequences, width = partial.shape
+def middle(base, other, gain, place):
+    sequences, width = base.shape
     packed = (place.shape[0] * (width // 2) // LANES, LANES)
     return pl.pallas_call(
         middle_kernel,
@@ -245,13 +265,13 @@
             jax.ShapeDtypeStruct((sequences, width), BF16),
             jax.ShapeDtypeStruct(packed, BF16),
         ),
-        in_specs=[in_vmem()] * 5,
+        in_specs=[in_vmem()] * 4,
         out_specs=(in_vmem(), in_vmem()),
         scratch_shapes=[VMEM(packed, F32)],
         compiler_params=params(12),
         cost_estimate=cost(1 << 28, 1 << 20),
         name="middle",
-    )(partial, other, normed, gain.reshape(1, -1), place)
+    )(base, other, gain.reshape(1, -1), place)
 
 
 def expert_kernel(own, other, gate, up, down, kept, sent, scratch, rows):
@@ -292,6 +312,29 @@
     )(own, other, gate, up, down)
 
 
+def fetch_kernel(*refs):
+    count = len(refs) // 2
+    sources, targets, sems = refs[:count], refs[count : 2 * count], refs[-1]
+    copies = [chunked(src, dst, sems, i) for i, (src, dst) in enumerate(zip(sources, targets))]
+    for group in copies:
+        start_all(group)
+    for group in copies:
+        wait_all(group)
+
+
+def fetch(*weights):
+    return pl.pallas_call(
+        fetch_kernel,
+        out_shape=tuple(jax.ShapeDtypeStruct(w.shape, w.dtype) for w in weights),
+        in_specs=[in_hbm()] * len(weights),
+        out_specs=tuple(in_vmem() for _ in weights),
+        scratch_shapes=[pltpu.SemaphoreType.DMA((len(weights), CHUNKS))],
+        compiler_params=params(49),
+        cost_estimate=cost(1 << 28, 6 << 20),
+        name="fetch",
+    )(*weights)
+
+
 def add_kernel(a, b, out):
     out[...] = (a[...].astype(F32) + b[...].astype(F32)).astype(BF16)
 
@@ -389,7 +432,13 @@
     return lax.ppermute(values, "ep", [(i, i ^ bit) for i in range(count)])
 
 
-def pack_kernel(gate, up, down, packed):
+def pack_kernel(gate_hbm, up_hbm, down_hbm, packed, gate, up, down, sems):
+    copies = [
+        pltpu.make_async_copy(src, dst, sems.at[i])
+        for i, (src, dst) in enumerate(((gate_hbm, gate), (up_hbm, up), (down_hbm, down)))
+    ]
+    start_all(copies)
+    wait_all(copies)
     core = lax.axis_index("tp")
     rows, units = gate.shape
     share = units // 2
@@ -405,10 +454,16 @@
     return pl.pallas_call(
         pack_kernel,
         out_shape=jax.ShapeDtypeStruct((rows + units // 4, units), BF16),
-        in_specs=[in_vmem()] * 3,
+        in_specs=[in_hbm()] * 3,
         out_specs=in_vmem(),
-        compiler_params=params(8),
-        cost_estimate=cost(1 << 18, 1 << 18),
+        scratch_shapes=[
+            VMEM(gate.shape, BF16),
+            VMEM(up.shape, BF16),
+            VMEM(down.shape, BF16),
+            pltpu.SemaphoreType.DMA((3,)),
+        ],
+        compiler_params=pltpu.CompilerParams(vmem_limit_bytes=(53 << 20) + (10240 << 10)),
+        cost_estimate=cost(1 << 32, 1 << 18),
         name="pack",
     )(gate, up, down)
 
@@ -539,15 +594,18 @@
             if bit > 4 or bit == 4:
                 block = join(block, far[-1])
             bit //= 2
-    partial, normed = attention(
+    partial = attention(
         tokens, norm_in, w_query, cache_keys, cache_values, cache_lengths, stick_bias, w_output
     )
-    place, portion = plan(routes, route_weights, slots, capacity)
+    place, portion, base, normed = plan(
+        routes, route_weights, partial, tokens, norm_in, slots, capacity
+    )
     partial_other = swap_core(partial)
-    hidden, outgoing = middle(partial, partial_other, normed, norm_mid, place)
+    hidden, outgoing = middle(base, partial_other, norm_mid, place)
     received = exchange(outgoing, ep_count)
     received_other = swap_core(received)
-    kept, sent = expert(received, received_other, expert_gate[0], expert_up[0], expert_down[0])
+    weights = fetch(expert_gate[0], expert_up[0], expert_down[0])
+    kept, sent = expert(received, received_other, *weights)
     sent_other = swap_core(sent)
     summed = add_rounded(kept, sent_other)
     returned = exchange(summed, ep_count)

time: 63.1 us -> 64.5 us (1.022)
  Pallas kernels: 11.4 us -> 13.8 us
  waiting for transfers between devices: 23.7 us -> 22 us
  local copies, waits for them, and re-layouts: 4.28 us -> 5.01 us
    pallas_call x1, Pallas kernels: 0.03 us -> 1.58 us  [pack(): pl.pallas_call(pack_kernel, out_shape=jax.ShapeDtypeStruct((rows + units...]
    ppermute x6, waiting for transfers between devices: 21.2 us -> 19.8 us  [swap_far(): return lax.ppermute(values, 'ep', [(i, i ^ bit) for i in range(count)])]
    unnamed x32 -> x26, local copies, waits for them, and re-layouts: 4.25 us -> 4.99 us
    pallas_call x1 -> x2, Pallas kernels: 5.7 us -> 6.43 us  [the longest x1 4.75 us: attention(): pl.pallas_call(attention_kernel, out_shape=jax.ShapeDtypeStruct((sequence...]
  transfers between devices with their start and end apart: 13 -> 13, of which waited for: 6 -> 6; matrix products, arithmetic and copies ran while one was open for 0% -> 0% of each run, Pallas kernels for 6% -> 11%
where the time goes in v3:
time: 64.5 us; the launch traced here: 64 us
  starting transfers between devices  22.3 us (35%)
  waiting for transfers between devices  22 us (34%)
  Pallas kernels  13.8 us (21%)
  local copies, waits for them, and re-layouts  5.01 us (8%)
  between operations  0.82 us (1%)
    ppermute x6, waiting for transfers between devices, swap_far(): return lax.ppermute(values, 'ep', [(i, i ^ bit) for i in range(count)])  19.8 us
    all_to_all x2, starting transfers between devices, exchange(): lax.all_to_all(blocks, 'ep', split_axis=0, concat_axis=0, tiled=True)  11.7 us
    ppermute x6, starting transfers between devices, swap_far(): return lax.ppermute(values, 'ep', [(i, i ^ bit) for i in range(count)])  9.36 us
    unnamed x26, local copies, waits for them, and re-layouts  4.99 us
    pallas_call x1, Pallas kernels, attention(): pl.pallas_call(attention_kernel, out_shape=jax.ShapeDtypeStruct((sequence...  4.75 us
    ppermute x5, waiting for transfers between devices, swap_core(): return lax.ppermute(values, 'tp', [(0, 1), (1, 0)])  2.23 us
    pallas_call x1, Pallas kernels, fetch(): pl.pallas_call(fetch_kernel, out_shape=tuple((jax.ShapeDtypeStruct(w.shap...  1.68 us
    pallas_call x1, Pallas kernels, pack(): pl.pallas_call(pack_kernel, out_shape=jax.ShapeDtypeStruct((rows + units...  1.58 us
  transfers between devices with their start and end apart: 13, of which 6 were waited for; matrix products, arithmetic and copies ran while one was open for 0% of the time, Pallas kernels for 11%

profile of v3, /device:TPU:0, one launch (start us, length us, event | category | flops | bytes accessed | tf_op | source)
XLA Modules:
  0.0 64.0 jit_solution(8285928040443845392)
XLA Ops:
  0.6 0.8 %copy-done.4 = bf16[16,2048]{1,0:T(8,128)(2,1)S(1)} copy-done((bf16[16,2048]{1,0:T(8,128)(2,1)S(1)}, bf16[16,2048]{1,0:T(8,128)(2,1)}, u32[]{:S(2)}) %copy-start.4) | copy-done | bytes 65560
  3.5 4.8 %attention.1.partial = f32[16,2048]{1,0:T(8,128)S(1)} custom-call(s32[16]{0:T(128)S(1)} %copy-done.11, f32[4]{0:T(128)S(1)} %copy-done.12, bf16[16,2048]{1,0:T(8,128)(2,1)S(1)} %copy-done.4, f32[1,2048]{1,0:T(1,128)S(1)} %bitcast.25, bf16[2048,256]{1,0:T(8,128)(2,1)} %wq_hbm.1, bf16[1024,1024]{1,0:T(8,128)(2,1)} %bitcast.32, bf16[1024,1024]{1,0:T(8,128)(2,1)} %bitcast.33, ...), custom_call_target="tpu_custom_call" | custom-call | flops 4294967296 | bytes 7340032 | tf_op jit(solution)/shard_map/attention/pallas_call | solution.py:176
  9.0 0.8 %collective-permute-done.other = f32[16,2048]{1,0:T(8,128)S(1)} collective-permute-done((f32[16,2048]{1,0:T(8,128)S(1)}, f32[16,2048]{1,0:T(8,128)S(1)}, u32[]{:S(2)}, u32[]{:S(2)}) %collective-permute-start) | collective-permute-done | bytes 131104 | tf_op jit(solution)/shard_map/ppermute | solution.py:421
  9.8 1.1 %middle.1 = (bf16[16,2048]{1,0:T(8,128)(2,1)S(1)}, bf16[768,128]{1,0:T(8,128)(2,1)}) custom-call(f32[16,2048]{1,0:T(8,128)S(1)} %get-tuple-element.16.base, f32[16,2048]{1,0:T(8,128)S(1)} %collective-permute-done.other, f32[1,2048]{1,0:T(1,128)S(1)} %bitcast.29, bf16[96,16]{1,0:T(8,128)(2,1)S(1)} %get-tuple-element.17.place), custom_call_target="tpu_custom_call" | custom-call | flops 268435456 | bytes 1048576 | tf_op jit(solution)/shard_map/middle/pallas_call | solution.py:262
  10.9 8.2 %all-to-all-start = ((bf16[16,48,128]{2,1,0:T(8,128)(2,1)}), bf16[16,48,128]{2,1,0:T(8,128)(2,1)S(1)}, u32[]{:S(2)}, u32[]{:S(2)}) async-start(bf16[16,48,128]{2,1,0:T(8,128)(2,1)} %bitcast.6), calls=%async_computation | async-start | bytes 393216 | tf_op jit(solution)/shard_map/all_to_all | solution.py:426
  19.1 1.6 %pack.1.refs_0_ = bf16[192,256]{1,0:T(8,128)(2,1)} custom-call(bf16[128,256]{1,0:T(8,128)(2,1)} %gate_hbm.1, bf16[128,256]{1,0:T(8,128)(2,1)} %up_hbm.1, bf16[256,128]{1,0:T(8,128)(2,1)} %down_hbm.1), custom_call_target="tpu_custom_call" | custom-call | flops 4294967296 | bytes 262144 | tf_op jit(solution)/shard_map/pack/pallas_call | solution.py:454
  20.7 2.9 %collective-permute-start.4 = (bf16[192,256]{1,0:T(8,128)(2,1)}, bf16[192,256]{1,0:T(8,128)(2,1)S(1)}, u32[]{:S(2)}, u32[]{:S(2)}) collective-permute-start(bf16[192,256]{1,0:T(8,128)(2,1)} %pack.1.refs_0_), channel_id=1, source_target_pairs={{0,16},{2,18},{4,20},{6,22},{8,24},{10,26},{12,28},{14,30},{16,0},... | collective-permute-start | bytes 294920 | tf_op jit(solution)/shard_map/ppermute | solution.py:432
  23.6 7.4 %collective-permute-done.4.refs_1_ = bf16[192,256]{1,0:T(8,128)(2,1)S(1)} collective-permute-done((bf16[192,256]{1,0:T(8,128)(2,1)}, bf16[192,256]{1,0:T(8,128)(2,1)S(1)}, u32[]{:S(2)}, u32[]{:S(2)}) %collective-permute-start.4) | collective-permute-done | bytes 98336 | tf_op jit(solution)/shard_map/ppermute | solution.py:432
  31.0 0.9 %copy-done.3 = bf16[192,256]{1,0:T(8,128)(2,1)S(1)} copy-done((bf16[192,256]{1,0:T(8,128)(2,1)S(1)}, bf16[192,256]{1,0:T(8,128)(2,1)}, u32[]{:S(2)}) %copy-start.3) | copy-done | bytes 98328
  32.1 5.9 %collective-permute-done.5.refs_1_ = bf16[384,256]{1,0:T(8,128)(2,1)S(1)} collective-permute-done((bf16[384,256]{1,0:T(8,128)(2,1)S(1)}, bf16[384,256]{1,0:T(8,128)(2,1)S(1)}, u32[]{:S(2)}, u32[]{:S(2)}) %collective-permute-start.5) | collective-permute-done | bytes 196640 | tf_op jit(solution)/shard_map/ppermute | solution.py:432
  38.0 1.5 %collective-permute-start.7 = (bf16[768,256]{1,0:T(8,128)(2,1)S(1)}, bf16[768,256]{1,0:T(8,128)(2,1)S(1)}, u32[]{:S(2)}, u32[]{:S(2)}) collective-permute-start(bf16[768,256]{1,0:T(8,128)(2,1)S(1)} %join.3.refs_0_), channel_id=1, source_target_pairs={{0,4},{2,6},{4,0},{6,2},{8,12},{10,14},{12,8},{14,10},{16,20},{18,... | collective-permute-start | bytes 1179656 | tf_op jit(solution)/shard_map/ppermute | solution.py:432
  39.5 1.5 %collective-permute-start.6 = (bf16[768,256]{1,0:T(8,128)(2,1)S(1)}, bf16[768,256]{1,0:T(8,128)(2,1)S(1)}, u32[]{:S(2)}, u32[]{:S(2)}) collective-permute-start(bf16[768,256]{1,0:T(8,128)(2,1)S(1)} %join.3.refs_0_), channel_id=1, source_target_pairs={{0,2},{2,0},{4,6},{6,4},{8,10},{10,8},{12,14},{14,12},{16,18},{18,... | collective-permute-start | bytes 1179656 | tf_op jit(solution)/shard_map/ppermute | solution.py:432
  41.0 1.2 %copy-done = bf16[1,2048,256]{2,1,0:T(8,128)(2,1)S(1)} copy-done((bf16[1,2048,256]{2,1,0:T(8,128)(2,1)S(1)}, bf16[1,2048,256]{2,1,0:T(8,128)(2,1)}, u32[]{:S(2)}) %copy-start) | copy-done | bytes 1048600
  42.2 1.7 %fetch.1 = (bf16[2048,256]{1,0:T(8,128)(2,1)S(1)}, bf16[2048,256]{1,0:T(8,128)(2,1)S(1)}, bf16[256,2048]{1,0:T(8,128)(2,1)S(1)}) custom-call(bf16[2048,256]{1,0:T(8,128)(2,1)S(1)} %bitcast.17, bf16[2048,256]{1,0:T(8,128)(2,1)} %bitcast.30, bf16[256,2048]{1,0:T(8,128)(2,1)} %bitcast.31), custom_call_target="tpu_custom_call" | custom-call | flops 268435456 | bytes 6291456 | tf_op jit(solution)/shard_map/fetch/pallas_call | solution.py:326
  43.9 0.9 %expert.1 = (bf16[768,128]{1,0:T(8,128)(2,1)S(1)}, bf16[768,128]{1,0:T(8,128)(2,1)S(1)}) custom-call(bf16[768,128]{1,0:T(8,128)(2,1)S(1)} %bitcast.22, bf16[768,128]{1,0:T(8,128)(2,1)S(1)} %collective-permute-done.1.other, bf16[2048,256]{1,0:T(8,128)(2,1)S(1)} %get-tuple-element.19.gate, bf16[2048,256]{1,0:T(8,128)(2,1)S(1)} %get-tuple-element.20.up, ...), custom_call_target="tpu_custom_call" | custom-call | flops 1073741824 | bytes 4194304 | tf_op jit(solution)/shard_map/expert/pallas_call | solution.py:303
  44.9 1.4 %collective-permute-done.2.b = bf16[768,128]{1,0:T(8,128)(2,1)S(1)} collective-permute-done((bf16[768,128]{1,0:T(8,128)(2,1)S(1)}, bf16[768,128]{1,0:T(8,128)(2,1)S(1)}, u32[]{:S(2)}, u32[]{:S(2)}) %collective-permute-start.2) | collective-permute-done | bytes 196640 | tf_op jit(solution)/shard_map/ppermute | solution.py:421
  47.1 3.5 %all-to-all-start.1 = ((bf16[16,48,128]{2,1,0:T(8,128)(2,1)}), bf16[16,48,128]{2,1,0:T(8,128)(2,1)S(1)}, u32[]{:S(2)}, u32[]{:S(2)}) async-start(bf16[16,48,128]{2,1,0:T(8,128)(2,1)} %bitcast.11), calls=%async_computation.1 | async-start | bytes 393216 | tf_op jit(solution)/shard_map/all_to_all | solution.py:426
  50.6 1.9 %collective-permute-start.8 = (bf16[384,256]{1,0:T(8,128)(2,1)S(1)}, bf16[384,256]{1,0:T(8,128)(2,1)S(1)}, u32[]{:S(2)}, u32[]{:S(2)}) collective-permute-start(bf16[384,256]{1,0:T(8,128)(2,1)S(1)} %slice.8), channel_id=1, source_target_pairs={{0,2},{2,0},{4,6},{6,4},{8,10},{10,8},{12,14},{14,12},{16,18},{18,... | collective-permute-start | bytes 589832 | tf_op jit(solution)/shard_map/ppermute | solution.py:432
  52.5 1.5 %collective-permute-start.9 = (bf16[384,256]{1,0:T(8,128)(2,1)S(1)}, bf16[384,256]{1,0:T(8,128)(2,1)S(1)}, u32[]{:S(2)}, u32[]{:S(2)}) collective-permute-start(bf16[384,256]{1,0:T(8,128)(2,1)S(1)} %slice.9), channel_id=1, source_target_pairs={{0,4},{2,6},{4,0},{6,2},{8,12},{10,14},{12,8},{14,10},{16,20},{18,... | collective-permute-start | bytes 589832 | tf_op jit(solution)/shard_map/ppermute | solution.py:432
  54.1 5.6 %collective-permute-done.8.refs_3_ = bf16[384,256]{1,0:T(8,128)(2,1)S(1)} collective-permute-done((bf16[384,256]{1,0:T(8,128)(2,1)S(1)}, bf16[384,256]{1,0:T(8,128)(2,1)S(1)}, u32[]{:S(2)}, u32[]{:S(2)}) %collective-permute-start.8) | collective-permute-done | bytes 196640 | tf_op jit(solution)/shard_map/ppermute | solution.py:432
  59.6 0.9 %collective-permute-done.9.refs_4_ = bf16[384,256]{1,0:T(8,128)(2,1)S(1)} collective-permute-done((bf16[384,256]{1,0:T(8,128)(2,1)S(1)}, bf16[384,256]{1,0:T(8,128)(2,1)S(1)}, u32[]{:S(2)}, u32[]{:S(2)}) %collective-permute-start.9) | collective-permute-done | bytes 196640 | tf_op jit(solution)/shard_map/ppermute | solution.py:432
  60.6 0.7 %dense.1 = f32[16,2048]{1,0:T(8,128)S(1)} custom-call(bf16[16,2048]{1,0:T(8,128)(2,1)S(1)} %get-tuple-element.25.hidden, bf16[768,256]{1,0:T(8,128)(2,1)S(1)} %join.3.refs_0_, bf16[768,256]{1,0:T(8,128)(2,1)S(1)} %collective-permute-done.6.refs_1_, bf16[768,256]{1,0:T(8,128)(2,1)S(1)} %collective-permute-done.7.refs_2_, ...), custom_call_target="tpu_custom_call" | custom-call | flops 268435456 | bytes 2097152 | tf_op jit(solution)/shard_map/dense/pallas_call | solution.py:515
  62.1 0.8 %fresh.1 = (bf16[16,64]{1,0:T(8,128)(2,1)}, bf16[16,64]{1,0:T(8,128)(2,1)}) custom-call(bf16[16,2048]{1,0:T(8,128)(2,1)S(1)} %get-tuple-element.26.normed, bf16[64,2048]{1,0:T(8,128)(2,1)S(1)} %bitcast.19, bf16[64,2048]{1,0:T(8,128)(2,1)S(1)} %bitcast.20), custom_call_target="tpu_custom_call" | custom-call | flops 16777216 | bytes 524288 | tf_op jit(solution)/shard_map/fresh/pallas_call | solution.py:409
  63.0 1.0 %last.1 = bf16[16,2048]{1,0:T(8,128)(2,1)} custom-call(f32[16,1024]{1,0:T(8,128)S(1)} %combine.1.own, f32[16,1024]{1,0:T(8,128)S(1)} %collective-permute-done.3.other, f32[16,2048]{1,0:T(8,128)S(1)} %dense.1, f32[16,2048]{1,0:T(8,128)S(1)} %collective-permute-done.10.dense_other, bf16[16,2048]{1,0:T(8,128)(2,1)S(1)} %get-tuple-element.25.hidden, ...), custom_call_target="tpu_custom_call" | custom-call | flops 1048576 | bytes 1048576 | tf_op jit(solution)/shard_map/last/pallas_call | solution.py:389
  (43 shorter events, 4.6 us)
Async XLA Ops:
  0.6 0.8 %copy-start.4 = (bf16[16,2048]{1,0:T(8,128)(2,1)S(1)}, bf16[16,2048]{1,0:T(8,128)(2,1)}, u32[]{:S(2)}) copy-start(bf16[16,2048]{1,0:T(8,128)(2,1)} %tokens.3) | copy-start | bytes 196612
  1.5 0.7 %copy-start.7 = (f32[2048]{0:T(1024)S(1)}, f32[2048]{0:T(1024)}, u32[]{:S(2)}) copy-start(f32[2048]{0:T(1024)} %param.25) | copy-start | bytes 24580
  3.5 5.3 %copy-start.8 = (s32[16,6]{0,1:T(8,128)S(1)}, s32[16,6]{0,1:T(8,128)}, u32[]{:S(2)}) copy-start(s32[16,6]{0,1:T(8,128)} %param.32) | copy-start | bytes 1156
  3.5 5.3 %copy-start.9 = (f32[16,6]{0,1:T(8,128)S(1)}, f32[16,6]{0,1:T(8,128)}, u32[]{:S(2)}) copy-start(f32[16,6]{0,1:T(8,128)} %param.33) | copy-start | bytes 1156
  3.5 6.3 %copy-start.10 = (f32[2048]{0:T(1024)S(1)}, f32[2048]{0:T(1024)}, u32[]{:S(2)}) copy-start(f32[2048]{0:T(1024)} %param.31) | copy-start | bytes 24580
  8.3 1.5 %collective-permute-start = (f32[16,2048]{1,0:T(8,128)S(1)}, f32[16,2048]{1,0:T(8,128)S(1)}, u32[]{:S(2)}, u32[]{:S(2)}) collective-permute-start(f32[16,2048]{1,0:T(8,128)S(1)} %attention.1.partial), channel_id=1, source_target_pairs={{0,1},{1,0},{2,3},{3,2},{4,5},{5,4},{6,7},{7,6},{8,9},{9,8},{10,11... | collective-permute-start | bytes 393224 | tf_op jit(solution)/shard_map/ppermute | solution.py:421
  10.9 21.1 %all-to-all-start = ((bf16[16,48,128]{2,1,0:T(8,128)(2,1)}), bf16[16,48,128]{2,1,0:T(8,128)(2,1)S(1)}, u32[]{:S(2)}, u32[]{:S(2)}) async-start(bf16[16,48,128]{2,1,0:T(8,128)(2,1)} %bitcast.6), calls=%async_computation | async-start | bytes 393216 | tf_op jit(solution)/shard_map/all_to_all | solution.py:426
  20.7 10.3 %collective-permute-start.4 = (bf16[192,256]{1,0:T(8,128)(2,1)}, bf16[192,256]{1,0:T(8,128)(2,1)S(1)}, u32[]{:S(2)}, u32[]{:S(2)}) collective-permute-start(bf16[192,256]{1,0:T(8,128)(2,1)} %pack.1.refs_0_), channel_id=1, source_target_pairs={{0,16},{2,18},{4,20},{6,22},{8,24},{10,26},{12,28},{14,30},{16,0},... | collective-permute-start | bytes 294920 | tf_op jit(solution)/shard_map/ppermute | solution.py:432
  31.0 0.9 %copy-start.3 = (bf16[192,256]{1,0:T(8,128)(2,1)S(1)}, bf16[192,256]{1,0:T(8,128)(2,1)}, u32[]{:S(2)}) copy-start(bf16[192,256]{1,0:T(8,128)(2,1)} %pack.1.refs_0_) | copy-start | bytes 294916
  31.9 6.0 %collective-permute-start.5 = (bf16[384,256]{1,0:T(8,128)(2,1)S(1)}, bf16[384,256]{1,0:T(8,128)(2,1)S(1)}, u32[]{:S(2)}, u32[]{:S(2)}) collective-permute-start(bf16[384,256]{1,0:T(8,128)(2,1)S(1)} %join.2.refs_0_), channel_id=1, source_target_pairs={{0,8},{2,10},{4,12},{6,14},{8,0},{10,2},{12,4},{14,6},{16,24},{18,... | collective-permute-start | bytes 589832 | tf_op jit(solution)/shard_map/ppermute | solution.py:432
  32.0 11.9 %collective-permute-start.1 = (bf16[768,128]{1,0:T(8,128)(2,1)S(1)}, bf16[768,128]{1,0:T(8,128)(2,1)S(1)}, u32[]{:S(2)}, u32[]{:S(2)}) collective-permute-start(bf16[768,128]{1,0:T(8,128)(2,1)S(1)} %bitcast.21), channel_id=1, source_target_pairs={{0,1},{1,0},{2,3},{3,2},{4,5},{5,4},{6,7},{7,6},{8,9},{9,8},{10,11... | collective-permute-start | bytes 589832 | tf_op jit(solution)/shard_map/ppermute | solution.py:421
  38.0 12.6 %collective-permute-start.7 = (bf16[768,256]{1,0:T(8,128)(2,1)S(1)}, bf16[768,256]{1,0:T(8,128)(2,1)S(1)}, u32[]{:S(2)}, u32[]{:S(2)}) collective-permute-start(bf16[768,256]{1,0:T(8,128)(2,1)S(1)} %join.3.refs_0_), channel_id=1, source_target_pairs={{0,4},{2,6},{4,0},{6,2},{8,12},{10,14},{12,8},{14,10},{16,20},{18,... | collective-permute-start | bytes 1179656 | tf_op jit(solution)/shard_map/ppermute | solution.py:432
  39.5 13.0 %collective-permute-start.6 = (bf16[768,256]{1,0:T(8,128)(2,1)S(1)}, bf16[768,256]{1,0:T(8,128)(2,1)S(1)}, u32[]{:S(2)}, u32[]{:S(2)}) collective-permute-start(bf16[768,256]{1,0:T(8,128)(2,1)S(1)} %join.3.refs_0_), channel_id=1, source_target_pairs={{0,2},{2,0},{4,6},{6,4},{8,10},{10,8},{12,14},{14,12},{16,18},{18,... | collective-permute-start | bytes 1179656 | tf_op jit(solution)/shard_map/ppermute | solution.py:432
  41.0 1.2 %copy-start = (bf16[1,2048,256]{2,1,0:T(8,128)(2,1)S(1)}, bf16[1,2048,256]{2,1,0:T(8,128)(2,1)}, u32[]{:S(2)}) copy-start(bf16[1,2048,256]{2,1,0:T(8,128)(2,1)} %param.34) | copy-start | bytes 3145732
  44.8 17.3 %copy-start.1 = (bf16[2048,64]{0,1:T(8,128)(2,1)S(1)}, bf16[2048,64]{0,1:T(8,128)(2,1)}, u32[]{:S(2)}) copy-start(bf16[2048,64]{0,1:T(8,128)(2,1)} %param.27) | copy-start | bytes 786436
  44.8 17.3 %copy-start.2 = (bf16[2048,64]{0,1:T(8,128)(2,1)S(1)}, bf16[2048,64]{0,1:T(8,128)(2,1)}, u32[]{:S(2)}) copy-start(bf16[2048,64]{0,1:T(8,128)(2,1)} %param.28) | copy-start | bytes 786436
  44.8 1.5 %collective-permute-start.2 = (bf16[768,128]{1,0:T(8,128)(2,1)S(1)}, bf16[768,128]{1,0:T(8,128)(2,1)S(1)}, u32[]{:S(2)}, u32[]{:S(2)}) collective-permute-start(bf16[768,128]{1,0:T(8,128)(2,1)S(1)} %get-tuple-element.23), channel_id=1, source_target_pairs={{0,1},{1,0},{2,3},{3,2},{4,5},{5,4},{6,7},{7,6},{8,9},{9,8},{10,11... | collective-permute-start | bytes 589832 | tf_op jit(solution)/shard_map/ppermute | solution.py:421
  46.4 16.6 %copy-start.5 = (f32[2048]{0:T(1024)S(1)}, f32[2048]{0:T(1024)}, u32[]{:S(2)}) copy-start(f32[2048]{0:T(1024)} %param.40) | copy-start | bytes 24580
  46.4 16.6 %copy-start.6 = (f32[2048]{0:T(1024)S(1)}, f32[2048]{0:T(1024)}, u32[]{:S(2)}) copy-start(f32[2048]{0:T(1024)} %param.41) | copy-start | bytes 24580
  47.1 14.3 %all-to-all-start.1 = ((bf16[16,48,128]{2,1,0:T(8,128)(2,1)}), bf16[16,48,128]{2,1,0:T(8,128)(2,1)S(1)}, u32[]{:S(2)}, u32[]{:S(2)}) async-start(bf16[16,48,128]{2,1,0:T(8,128)(2,1)} %bitcast.11), calls=%async_computation.1 | async-start | bytes 393216 | tf_op jit(solution)/shard_map/all_to_all | solution.py:426
  50.6 9.0 %collective-permute-start.8 = (bf16[384,256]{1,0:T(8,128)(2,1)S(1)}, bf16[384,256]{1,0:T(8,128)(2,1)S(1)}, u32[]{:S(2)}, u32[]{:S(2)}) collective-permute-start(bf16[384,256]{1,0:T(8,128)(2,1)S(1)} %slice.8), channel_id=1, source_target_pairs={{0,2},{2,0},{4,6},{6,4},{8,10},{10,8},{12,14},{14,12},{16,18},{18,... | collective-permute-start | bytes 589832 | tf_op jit(solution)/shard_map/ppermute | solution.py:432
  52.5 8.0 %collective-permute-start.9 = (bf16[384,256]{1,0:T(8,128)(2,1)S(1)}, bf16[384,256]{1,0:T(8,128)(2,1)S(1)}, u32[]{:S(2)}, u32[]{:S(2)}) collective-permute-start(bf16[384,256]{1,0:T(8,128)(2,1)S(1)} %slice.9), channel_id=1, source_target_pairs={{0,4},{2,6},{4,0},{6,2},{8,12},{10,14},{12,8},{14,10},{16,20},{18,... | collective-permute-start | bytes 589832 | tf_op jit(solution)/shard_map/ppermute | solution.py:432
  61.3 1.6 %collective-permute-start.10 = (f32[16,2048]{1,0:T(8,128)S(1)}, f32[16,2048]{1,0:T(8,128)S(1)}, u32[]{:S(2)}, u32[]{:S(2)}) collective-permute-start(f32[16,2048]{1,0:T(8,128)S(1)} %dense.1), channel_id=1, source_target_pairs={{0,1},{1,0},{2,3},{3,2},{4,5},{5,4},{6,7},{7,6},{8,9},{9,8},{10,11... | collective-permute-start | bytes 393224 | tf_op jit(solution)/shard_map/ppermute | solution.py:421
  61.6 1.4 %collective-permute-start.3 = (f32[16,1024]{1,0:T(8,128)S(1)}, f32[16,1024]{1,0:T(8,128)S(1)}, u32[]{:S(2)}, u32[]{:S(2)}) collective-permute-start(f32[16,1024]{1,0:T(8,128)S(1)} %combine.1.own), channel_id=1, source_target_pairs={{0,1},{1,0},{2,3},{3,2},{4,5},{5,4},{6,7},{7,6},{8,9},{9,8},{10,11... | collective-permute-start | bytes 196616 | tf_op jit(solution)/shard_map/ppermute | solution.py:421
  (2 other events, 1.3 us)

commit v4 on v3

--- a/solution.py
+++ b/solution.py
@@ -9,7 +9,7 @@
 
 
 LANES = 128
-CHUNKS = 4
+CHUNKS = 2
 F32 = jnp.float32
 BF16 = jnp.bfloat16
 VMEM = pltpu.VMEM
@@ -85,8 +85,45 @@
         copy.wait()
 
 
+def plan_slots(capacity, routes, weights, place, share):
+    topk, sequences = routes.shape
+    slots = place.shape[0]
+    expert = iota((slots, sequences), 0) // capacity
+    hit = jnp.zeros((slots, sequences), F32)
+    weight = jnp.zeros((slots, sequences), F32)
+    for j in range(topk):
+        match = routes[j : j + 1, :] == expert
+        hit = jnp.where(match, 1.0, hit)
+        weight = jnp.where(match, weights[j : j + 1, :], weight)
+    earlier = (iota((sequences, sequences), 0) < iota((sequences, sequences), 1)).astype(BF16)
+    rank = dot(hit.astype(BF16), earlier)
+    turn = (iota((slots, sequences), 0) % capacity).astype(F32)
+    chosen = (hit > 0.0) & (rank == turn)
+    place[...] = jnp.where(chosen, 1.0, 0.0).astype(BF16)
+    share[...] = jnp.where(chosen, weight, 0.0)
+
+
 def attention_kernel(
-    lengths, bias, tokens, gain, wq_hbm, k_hbm, v_hbm, wo_hbm, partial, wq, k, v, wo, sems
+    capacity,
+    lengths,
+    bias,
+    tokens,
+    gain,
+    routes,
+    weights,
+    wq_hbm,
+    k_hbm,
+    v_hbm,
+    wo_hbm,
+    partial,
+    normed,
+    place,
+    share,
+    wq,
+    k,
+    v,
+    wo,
+    sems,
 ):
     copies = [
         chunked(src, dst, sems, i) for i, (src, dst) in enumerate(((wq_hbm, wq), (k_hbm, k), (v_hbm, v), (wo_hbm, wo)))
@@ -99,6 +136,8 @@
     rows = heads * sequences
     wide = sequences * head_dim
     rounded = norm_rows(tokens[...].astype(F32), gain[...]).astype(BF16)
+    normed[...] = rounded
+    plan_slots(capacity, routes, weights, place, share)
     wait_all(copies[0])
     start_all(copies[2] + copies[3])
     queries = dot(rounded, wq[...]).astype(BF16).astype(F32) * head_dim ** (-0.5)
@@ -167,17 +206,24 @@
     partial[...] = dot(attended, wo[...])
 
 
-def attention(tokens, gain, w_query, keys, values, lengths, bias, w_output):
+def attention(
+    tokens, gain, w_query, keys, values, lengths, bias, w_output, routes, weights, slots, capacity
+):
     sequences, kv_local, head_dim, length = keys.shape
     assert kv_local == 1 and head_dim * 2 == LANES
     width = tokens.shape[1]
     wide = sequences * head_dim
     flat = (wide, length)
     return pl.pallas_call(
-        attention_kernel,
-        out_shape=jax.ShapeDtypeStruct((sequences, width), F32),
-        in_specs=[in_smem(), in_smem(), in_vmem(), in_vmem()] + [in_hbm()] * 4,
-        out_specs=in_vmem(),
+        functools.partial(attention_kernel, capacity),
+        out_shape=(
+            jax.ShapeDtypeStruct((sequences, width), F32),
+            jax.ShapeDtypeStruct((sequences, width), BF16),
+            jax.ShapeDtypeStruct((slots, sequences), BF16),
+            jax.ShapeDtypeStruct((slots, sequences), F32),
+        ),
+        in_specs=[in_smem()] * 2 + [in_vmem()] * 4 + [in_hbm()] * 4,
+        out_specs=(in_vmem(),) * 4,
         scratch_shapes=[
             VMEM(w_query.shape, BF16),
             VMEM(flat, BF16),
@@ -188,46 +234,18 @@
         compiler_params=params(53),
         cost_estimate=cost(1 << 32, 7 << 20),
         name="attention",
-    )(lengths, bias, tokens, gain.reshape(1, -1), w_query, keys.reshape(flat), values.reshape(flat), w_output)
-
-
-def plan_kernel(capacity, routes, weights, partial, tokens, gain, place, share, base, normed):
-    topk, sequences = routes.shape
-    slots = place.shape[0]
-    expert = iota((slots, sequences), 0) // capacity
-    hit = jnp.zeros((slots, sequences), F32)
-    weight = jnp.zeros((slots, sequences), F32)
-    for j in range(topk):
-        match = routes[j : j + 1, :] == expert
-        hit = jnp.where(match, 1.0, hit)
-        weight = jnp.where(match, weights[j : j + 1, :], weight)
-    earlier = (iota((sequences, sequences), 0) < iota((sequences, sequences), 1)).astype(BF16)
-    rank = dot(hit.astype(BF16), earlier)
-    turn = (iota((slots, sequences), 0) % capacity).astype(F32)
-    chosen = (hit > 0.0) & (rank == turn)
-    place[...] = jnp.where(chosen, 1.0, 0.0).astype(BF16)
-    share[...] = jnp.where(chosen, weight, 0.0)
-    rounded = norm_rows(tokens[...].astype(F32), gain[...]).astype(BF16)
-    normed[...] = rounded
-    base[...] = rounded.astype(F32) + partial[...]
-
-
-def plan(routes, route_weights, partial, tokens, gain, slots, capacity):
-    sequences = routes.shape[0]
-    return pl.pallas_call(
-        functools.partial(plan_kernel, capacity),
-        out_shape=(
-            jax.ShapeDtypeStruct((slots, sequences), BF16),
-            jax.ShapeDtypeStruct((slots, sequences), F32),
-            jax.ShapeDtypeStruct(tokens.shape, F32),
-            jax.ShapeDtypeStruct(tokens.shape, BF16),
-        ),
-        in_specs=[in_vmem()] * 5,
-        out_specs=(in_vmem(),) * 4,
-        compiler_params=params(8),
-        cost_estimate=cost(1 << 20, 1 << 16),
-        name="plan",
-    )(jnp.transpose(routes), jnp.transpose(route_weights), partial, tokens, gain.reshape(1, -1))
+    )(
+        lengths,
+        bias,
+        tokens,
+        gain.reshape(1, -1),
+        jnp.transpose(routes),
+        jnp.transpose(weights),
+        w_query,
+        keys.reshape(flat),
+        values.reshape(flat),
+        w_output,
+    )
 
 
 def store_rows(scratch, values):
@@ -248,16 +266,17 @@
     return ref[:, pl.ds(pl.multiple_of(core * half, half), half)]
 
 
-def middle_kernel(base, other, gain, place, hidden, outgoing, scratch):
-    half = base.shape[1] // 2
-    hidden[...] = norm_rows(base[...] + other[...], gain[...]).astype(BF16)
+def middle_kernel(partial, other, normed, gain, place, hidden, outgoing, scratch):
+    half = partial.shape[1] // 2
+    floats = normed[...].astype(F32) + (partial[...] + other[...])
+    hidden[...] = norm_rows(floats, gain[...]).astype(BF16)
     mine = half_of(hidden, lax.axis_index("tp"), half)
     store_rows(scratch, dot(place[...], mine))
     outgoing[...] = scratch[...].astype(BF16)
 
 
-def middle(base, other, gain, place):
-    sequences, width = base.shape
+def middle(partial, other, normed, gain, place):
+    sequences, width = partial.shape
     packed = (place.shape[0] * (width // 2) // LANES, LANES)
     return pl.pallas_call(
         middle_kernel,
@@ -265,74 +284,110 @@
             jax.ShapeDtypeStruct((sequences, width), BF16),
             jax.ShapeDtypeStruct(packed, BF16),
         ),
-        in_specs=[in_vmem()] * 4,
+        in_specs=[in_vmem()] * 5,
         out_specs=(in_vmem(), in_vmem()),
         scratch_shapes=[VMEM(packed, F32)],
         compiler_params=params(12),
         cost_estimate=cost(1 << 28, 1 << 20),
         name="middle",
-    )(base, other, gain.reshape(1, -1), place)
-
-
-def expert_kernel(own, other, gate, up, down, kept, sent, scratch, rows):
+    )(partial, other, normed, gain.reshape(1, -1), place)
+
+
+def first_kernel(own, gate_hbm, up_hbm, down_hbm, pre, gate, up, down, scratch, gate_own, up_own, sems):
     core = lax.axis_index("tp")
-    packed = own.shape[0]
-    width = gate.shape[0]
+    half = gate.shape[0]
+    mine = pl.ds(pl.multiple_of(core * half, half), half)
+    theirs = pl.ds(pl.multiple_of((1 - core) * half, half), half)
+    early = chunked(gate_hbm.at[mine], gate_own, sems, 0) + chunked(up_hbm.at[mine], up_own, sems, 1)
+    late = chunked(gate_hbm.at[theirs], gate, sems, 2) + chunked(up_hbm.at[theirs], up, sems, 3)
+    late = late + chunked(down_hbm, down, sems, 4)
+    start_all(early + late)
+    scratch[...] = own[...].astype(F32)
+    rows = load_rows(scratch, pre.shape[0]).astype(BF16)
+    wait_all(early)
+    units = gate.shape[1]
+    pre[:, 0:units] = dot(rows, gate_own[...])
+    pre[:, units:] = dot(rows, up_own[...])
+    wait_all(late)
+
+
+def expert_first(own, gate, up, down):
+    packed = own.shape
+    width, units = gate.shape
     half = width // 2
-    count = packed * LANES // half
-    scratch[...] = own[...].astype(F32)
-    own_rows = load_rows(scratch, count).astype(BF16)
+    count = packed[0] * LANES // half
+    part = jax.ShapeDtypeStruct((half, units), BF16)
+    return pl.pallas_call(
+        first_kernel,
+        out_shape=(
+            jax.ShapeDtypeStruct((count, 2 * units), F32),
+            part,
+            part,
+            jax.ShapeDtypeStruct(down.shape, BF16),
+        ),
+        in_specs=[in_vmem()] + [in_hbm()] * 3,
+        out_specs=(in_vmem(),) * 4,
+        scratch_shapes=[
+            VMEM(packed, F32),
+            VMEM(part.shape, BF16),
+            VMEM(part.shape, BF16),
+            pltpu.SemaphoreType.DMA((5, CHUNKS)),
+        ],
+        compiler_params=params(50),
+        cost_estimate=cost(1 << 28, 4 << 20),
+        name="expert_first",
+    )(own, gate, up, down)
+
+
+def second_kernel(other, pre, gate, up, down, sent, act_out, scratch):
+    core = lax.axis_index("tp")
+    units = gate.shape[1]
+    half = down.shape[1] // 2
     scratch[...] = other[...].astype(F32)
-    other_rows = load_rows(scratch, count).astype(BF16)
-    rows[:, pl.ds(pl.multiple_of(core * half, half), half)] = own_rows
-    rows[:, pl.ds(pl.multiple_of((1 - core) * half, half), half)] = other_rows
-    inputs = rows[...]
-    gate_pre = dot(inputs, gate[...])
-    up_pre = dot(inputs, up[...])
+    rows = load_rows(scratch, pre.shape[0]).astype(BF16)
+    gate_pre = pre[:, 0:units] + dot(rows, gate[...])
+    up_pre = pre[:, units:] + dot(rows, up[...])
     act = (jax.nn.silu(gate_pre) * up_pre).astype(BF16)
-    store_rows(scratch, dot(act, half_of(down, core, half)))
-    kept[...] = scratch[...].astype(BF16)
+    act_out[...] = act
     store_rows(scratch, dot(act, half_of(down, 1 - core, half)))
     sent[...] = scratch[...].astype(BF16)
 
 
-def expert(own, other, gate, up, down):
-    packed = own.shape
-    width = gate.shape[0]
-    count = packed[0] * LANES * 2 // width
-    return pl.pallas_call(
-        expert_kernel,
-        out_shape=(jax.ShapeDtypeStruct(packed, BF16), jax.ShapeDtypeStruct(packed, BF16)),
+def expert_second(other, pre, gate, up, down):
+    packed = other.shape
+    return pl.pallas_call(
+        second_kernel,
+        out_shape=(
+            jax.ShapeDtypeStruct(packed, BF16),
+            jax.ShapeDtypeStruct((pre.shape[0], gate.shape[1]), BF16),
+        ),
         in_specs=[in_vmem()] * 5,
         out_specs=(in_vmem(), in_vmem()),
-        scratch_shapes=[VMEM(packed, F32), VMEM((count, width), BF16)],
-        compiler_params=params(24),
-        cost_estimate=cost(1 << 30, 4 << 20),
-        name="expert",
-    )(own, other, gate, up, down)
-
-
-def fetch_kernel(*refs):
-    count = len(refs) // 2
-    sources, targets, sems = refs[:count], refs[count : 2 * count], refs[-1]
-    copies = [chunked(src, dst, sems, i) for i, (src, dst) in enumerate(zip(sources, targets))]
-    for group in copies:
-        start_all(group)
-    for group in copies:
-        wait_all(group)
-
-
-def fetch(*weights):
-    return pl.pallas_call(
-        fetch_kernel,
-        out_shape=tuple(jax.ShapeDtypeStruct(w.shape, w.dtype) for w in weights),
-        in_specs=[in_hbm()] * len(weights),
-        out_specs=tuple(in_vmem() for _ in weights),
-        scratch_shapes=[pltpu.SemaphoreType.DMA((len(weights), CHUNKS))],
-        compiler_params=params(49),
-        cost_estimate=cost(1 << 28, 6 << 20),
-        name="fetch",
-    )(*weights)
+        scratch_shapes=[VMEM(packed, F32)],
+        compiler_params=params(16),
+        cost_estimate=cost(1 << 28, 2 << 20),
+        name="expert_second",
+    )(other, pre, gate, up, down)
+
+
+def third_kernel(act, down, kept, scratch):
+    half = down.shape[1] // 2
+    store_rows(scratch, dot(act[...], half_of(down, lax.axis_index("tp"), half)))
+    kept[...] = scratch[...].astype(BF16)
+
+
+def expert_third(act, down):
+    packed = (act.shape[0] * down.shape[1] // 2 // LANES, LANES)
+    return pl.pallas_call(
+        third_kernel,
+        out_shape=jax.ShapeDtypeStruct(packed, BF16),
+        in_specs=[in_vmem()] * 2,
+        out_specs=in_vmem(),
+        scratch_shapes=[VMEM(packed, F32)],
+        compiler_params=params(16),
+        cost_estimate=cost(1 << 26, 2 << 20),
+        name="expert_third",
+    )(act, down)
 
 
 def add_kernel(a, b, out):
@@ -462,7 +517,7 @@
             VMEM(down.shape, BF16),
             pltpu.SemaphoreType.DMA((3,)),
         ],
-        compiler_params=pltpu.CompilerParams(vmem_limit_bytes=(53 << 20) + (10240 << 10)),
+        compiler_params=params(63),
         cost_estimate=cost(1 << 32, 1 << 18),
         name="pack",
     )(gate, up, down)
@@ -488,39 +543,68 @@
     )(*blocks)
 
 
-def dense_kernel(offsets, hidden, *refs):
+def slabs_of(sources, offsets):
+    height = LANES + sources[0].shape[1] // 4
+    me = lax.axis_index("ep")
+    return [
+        (ref, n * height, pl.ds(pl.multiple_of((me ^ offset) * LANES, LANES), LANES))
+        for ref, group in zip(sources, offsets)
+        for n, offset in enumerate(group)
+    ]
+
+
+def add_slabs(pre, hidden, slabs):
+    for j in range(0, len(slabs), 2):
+        left = [hidden[:, at] for _, _, at in slabs[j : j + 2]]
+        right = [ref[start : start + LANES, :] for ref, start, _ in slabs[j : j + 2]]
+        pre = pre + dot(jnp.concatenate(left, axis=1), jnp.concatenate(right, axis=0))
+    return pre
+
+
+def early_kernel(offsets, hidden, *refs):
     sources, out = refs[:-1], refs[-1]
-    units = sources[0].shape[1]
-    share = units // 2
-    rows = LANES
-    height = rows + share // 2
-    me = lax.axis_index("ep")
-    blocks = []
-    for ref, group in zip(sources, offsets):
-        for n, offset in enumerate(group):
-            blocks.append((ref, n * height, (me ^ offset) * rows))
-    pre = jnp.zeros((hidden.shape[0], units), F32)
-    for j in range(0, len(blocks), 2):
-        left = [hidden[:, pl.ds(pl.multiple_of(at, rows), rows)] for _, _, at in blocks[j : j + 2]]
-        right = [ref[start : start + rows, :] for ref, start, _ in blocks[j : j + 2]]
-        pre = pre + dot(jnp.concatenate(left, axis=1), jnp.concatenate(right, axis=0))
-    act = (jax.nn.silu(pre[:, 0:share]) * pre[:, share:units]).astype(BF16)
-    for ref, start, at in blocks:
-        tail = ref[start + rows : start + height, :]
-        down = jnp.concatenate([tail[:, 0:share], tail[:, share:units]], axis=0)
-        out[:, pl.ds(pl.multiple_of(at, rows), rows)] = dot(act, down)
-
-
-def dense(hidden, sources, offsets):
-    return pl.pallas_call(
-        functools.partial(dense_kernel, offsets),
+    out[...] = add_slabs(jnp.zeros(out.shape, F32), hidden, slabs_of(sources, offsets))
+
+
+def dense_early(hidden, sources, offsets):
+    return pl.pallas_call(
+        functools.partial(early_kernel, offsets),
+        out_shape=jax.ShapeDtypeStruct((hidden.shape[0], sources[0].shape[1]), F32),
+        in_specs=[in_vmem()] * (1 + len(sources)),
+        out_specs=in_vmem(),
+        compiler_params=params(8),
+        cost_estimate=cost(1 << 26, 1 << 20),
+        name="dense_early",
+    )(hidden, *sources)
+
+
+def dense_kernel(late, offsets, hidden, early, *refs):
+    sources, out = refs[:-1], refs[-1]
+    share = early.shape[1] // 2
+    slabs = slabs_of(sources, offsets)
+    count = sum(len(group) for group in offsets[:late])
+    pre = add_slabs(early[...], hidden, slabs[:count])
+    act = (jax.nn.silu(pre[:, 0:share]) * pre[:, share:]).astype(BF16)
+    for j in range(0, len(slabs), 2):
+        downs = []
+        for ref, start, _ in slabs[j : j + 2]:
+            tail = ref[start + LANES : start + LANES + share // 2, :]
+            downs.append(jnp.concatenate([tail[:, 0:share], tail[:, share:]], axis=0))
+        both = dot(act, jnp.concatenate(downs, axis=1))
+        for n, (_, _, at) in enumerate(slabs[j : j + 2]):
+            out[:, at] = both[:, n * LANES : (n + 1) * LANES]
+
+
+def dense(hidden, early, late, sources, offsets):
+    return pl.pallas_call(
+        functools.partial(dense_kernel, len(late), offsets),
         out_shape=jax.ShapeDtypeStruct(hidden.shape, F32),
-        in_specs=[in_vmem()] * (1 + len(sources)),
+        in_specs=[in_vmem()] * (2 + len(late) + len(sources)),
         out_specs=in_vmem(),
         compiler_params=params(8),
         cost_estimate=cost(1 << 28, 2 << 20),
         name="dense",
-    )(hidden, *sources)
+    )(hidden, early, *late, *sources)
 
 
 def dense_weights(dense_gate, dense_up, dense_down):
@@ -594,19 +678,28 @@
             if bit > 4 or bit == 4:
                 block = join(block, far[-1])
             bit //= 2
-    partial = attention(
-        tokens, norm_in, w_query, cache_keys, cache_values, cache_lengths, stick_bias, w_output
-    )
-    place, portion, base, normed = plan(
-        routes, route_weights, partial, tokens, norm_in, slots, capacity
+    partial, normed, place, portion = attention(
+        tokens,
+        norm_in,
+        w_query,
+        cache_keys,
+        cache_values,
+        cache_lengths,
+        stick_bias,
+        w_output,
+        routes,
+        route_weights,
+        slots,
+        capacity,
     )
     partial_other = swap_core(partial)
-    hidden, outgoing = middle(base, partial_other, norm_mid, place)
+    hidden, outgoing = middle(partial, partial_other, normed, norm_mid, place)
     received = exchange(outgoing, ep_count)
     received_other = swap_core(received)
-    weights = fetch(expert_gate[0], expert_up[0], expert_down[0])
-    kept, sent = expert(received, received_other, *weights)
+    pre, gate, up, down = expert_first(received, expert_gate[0], expert_up[0], expert_down[0])
+    sent, act = expert_second(received_other, pre, gate, up, down)
     sent_other = swap_core(sent)
+    kept = expert_third(act, down)
     summed = add_rounded(kept, sent_other)
     returned = exchange(summed, ep_count)
     fresh_keys, fresh_values = fresh(normed, w_key, w_value)
@@ -624,7 +717,14 @@
             tuple(c ^ 3 for c in columns[:count]),
             tuple(c ^ 3 for c in columns[count:]),
         )
-        dense_out = dense(hidden, (block, from_x, from_y, diagonal_low, diagonal_high), offsets)
+        pre = dense_early(hidden, (block, from_x, from_y), offsets[:3])
+        dense_out = dense(
+            hidden,
+            pre,
+            (diagonal_low, diagonal_high),
+            (block, from_x, from_y),
+            offsets[3:] + offsets[:3],
+        )
     else:
         packed = dense_weights(dense_gate, dense_up, dense_down)
         dense_out = dense_narrow(hidden, packed, rows, share)

time: 64.5 us -> 65.1 us (level)
  local copies, waits for them, and re-layouts: 5.01 us -> 6.39 us
    unnamed x26, local copies, waits for them, and re-layouts: 4.99 us -> 6.36 us
    pallas_call x5 -> x6, Pallas kernels: 8.3 us -> 7.69 us  [the longest x1 4.68 us: attention(): pl.pallas_call(functools.partial(attention_kernel, capacity), out_shape=(...]
  transfers between devices with their start and end apart: 13 -> 13, of which waited for: 6 -> 6; matrix products, arithmetic and copies ran while one was open for 0% -> 0% of each run, Pallas kernels for 11% -> 10%
where the time goes in v4:
time: 65.1 us; the launch traced here: 64.5 us
  starting transfers between devices  22.3 us (34%)
  waiting for transfers between devices  21.8 us (33%)
  Pallas kernels  13.2 us (20%)
  local copies, waits for them, and re-layouts  6.39 us (10%)
  between operations  0.83 us (1%)
    ppermute x6, waiting for transfers between devices, swap_far(): return lax.ppermute(values, 'ep', [(i, i ^ bit) for i in range(count)])  19.6 us
    all_to_all x2, starting transfers between devices, exchange(): lax.all_to_all(blocks, 'ep', split_axis=0, concat_axis=0, tiled=True)  11.7 us
    ppermute x6, starting transfers between devices, swap_far(): return lax.ppermute(values, 'ep', [(i, i ^ bit) for i in range(count)])  9.36 us
    unnamed x26, local copies, waits for them, and re-layouts  6.36 us
    pallas_call x1, Pallas kernels, attention(): pl.pallas_call(functools.partial(attention_kernel, capacity), out_shape=(...  4.68 us
    ppermute x5, waiting for transfers between devices, swap_core(): return lax.ppermute(values, 'tp', [(0, 1), (1, 0)])  2.2 us
    pallas_call x1, Pallas kernels, expert_first(): pl.pallas_call(first_kernel, out_shape=(jax.ShapeDtypeStruct((count, 2 *...  1.65 us
    pallas_call x1, Pallas kernels, pack(): pl.pallas_call(pack_kernel, out_shape=jax.ShapeDtypeStruct((rows + units...  1.58 us
  transfers between devices with their start and end apart: 13, of which 6 were waited for; matrix products, arithmetic and copies ran while one was open for 0% of the time, Pallas kernels for 10%

profile of v4, /device:TPU:0, one launch (start us, length us, event | category | flops | bytes accessed | tf_op | source)
XLA Modules:
  0.0 64.5 jit_solution(8672597040340630202)
XLA Ops:
  0.6 0.8 %copy-done.6 = bf16[16,2048]{1,0:T(8,128)(2,1)S(1)} copy-done((bf16[16,2048]{1,0:T(8,128)(2,1)S(1)}, bf16[16,2048]{1,0:T(8,128)(2,1)}, u32[]{:S(2)}) %copy-start.6) | copy-done | bytes 65560
  1.5 0.7 %copy-done.7 = f32[2048]{0:T(1024)S(1)} copy-done((f32[2048]{0:T(1024)S(1)}, f32[2048]{0:T(1024)}, u32[]{:S(2)}) %copy-start.7) | copy-done | bytes 8216
  4.9 4.7 %attention.1 = (f32[16,2048]{1,0:T(8,128)S(1)}, bf16[16,2048]{1,0:T(8,128)(2,1)S(1)}, bf16[96,16]{1,0:T(8,128)(2,1)S(1)}, f32[96,16]{1,0:T(8,128)S(1)}) custom-call(s32[16]{0:T(128)S(1)} %copy-done.11, f32[4]{0:T(128)S(1)} %copy-done.12, bf16[16,2048]{1,0:T(8,128)(2,1)S(1)} %copy-done.6, f32[1,2048]{1,0:T(1,128)S(1)} %bitcast.25, s32[6,16]{1,0:T(8,128)S(1)} %bitcast.27, ...), custom_call_target="tpu_custom_call" | custom-call | flops 4294967296 | bytes 7340032 | tf_op jit(solution)/shard_map/attention/pallas_call | solution.py:217
  10.1 1.0 %collective-permute-done.other = f32[16,2048]{1,0:T(8,128)S(1)} collective-permute-done((f32[16,2048]{1,0:T(8,128)S(1)}, f32[16,2048]{1,0:T(8,128)S(1)}, u32[]{:S(2)}, u32[]{:S(2)}) %collective-permute-start) | collective-permute-done | bytes 131104 | tf_op jit(solution)/shard_map/ppermute | solution.py:476
  11.1 1.1 %middle.1 = (bf16[16,2048]{1,0:T(8,128)(2,1)S(1)}, bf16[768,128]{1,0:T(8,128)(2,1)}) custom-call(f32[16,2048]{1,0:T(8,128)S(1)} %get-tuple-element.17.partial, f32[16,2048]{1,0:T(8,128)S(1)} %collective-permute-done.other, bf16[16,2048]{1,0:T(8,128)(2,1)S(1)} %get-tuple-element.18.normed, f32[1,2048]{1,0:T(1,128)S(1)} %bitcast.26, ...), custom_call_target="tpu_custom_call" | custom-call | flops 268435456 | bytes 1048576 | tf_op jit(solution)/shard_map/middle/pallas_call | solution.py:281
  12.2 8.2 %all-to-all-start = ((bf16[16,48,128]{2,1,0:T(8,128)(2,1)}), bf16[16,48,128]{2,1,0:T(8,128)(2,1)S(1)}, u32[]{:S(2)}, u32[]{:S(2)}) async-start(bf16[16,48,128]{2,1,0:T(8,128)(2,1)} %bitcast.6), calls=%async_computation | async-start | bytes 393216 | tf_op jit(solution)/shard_map/all_to_all | solution.py:481
  20.4 1.6 %pack.1.refs_0_ = bf16[192,256]{1,0:T(8,128)(2,1)} custom-call(bf16[128,256]{1,0:T(8,128)(2,1)} %gate_hbm.1, bf16[128,256]{1,0:T(8,128)(2,1)} %up_hbm.1, bf16[256,128]{1,0:T(8,128)(2,1)} %down_hbm.1), custom_call_target="tpu_custom_call" | custom-call | flops 4294967296 | bytes 262144 | tf_op jit(solution)/shard_map/pack/pallas_call | solution.py:509
  22.0 2.9 %collective-permute-start.4 = (bf16[192,256]{1,0:T(8,128)(2,1)}, bf16[192,256]{1,0:T(8,128)(2,1)S(1)}, u32[]{:S(2)}, u32[]{:S(2)}) collective-permute-start(bf16[192,256]{1,0:T(8,128)(2,1)} %pack.1.refs_0_), channel_id=1, source_target_pairs={{0,16},{2,18},{4,20},{6,22},{8,24},{10,26},{12,28},{14,30},{16,0},... | collective-permute-start | bytes 294920 | tf_op jit(solution)/shard_map/ppermute | solution.py:487
  24.9 7.4 %collective-permute-done.4.refs_1_ = bf16[192,256]{1,0:T(8,128)(2,1)S(1)} collective-permute-done((bf16[192,256]{1,0:T(8,128)(2,1)}, bf16[192,256]{1,0:T(8,128)(2,1)S(1)}, u32[]{:S(2)}, u32[]{:S(2)}) %collective-permute-start.4) | collective-permute-done | bytes 98336 | tf_op jit(solution)/shard_map/ppermute | solution.py:487
  32.3 0.9 %copy-done.3 = bf16[192,256]{1,0:T(8,128)(2,1)S(1)} copy-done((bf16[192,256]{1,0:T(8,128)(2,1)S(1)}, bf16[192,256]{1,0:T(8,128)(2,1)}, u32[]{:S(2)}) %copy-start.3) | copy-done | bytes 98328
  33.4 5.9 %collective-permute-done.5.refs_1_ = bf16[384,256]{1,0:T(8,128)(2,1)S(1)} collective-permute-done((bf16[384,256]{1,0:T(8,128)(2,1)S(1)}, bf16[384,256]{1,0:T(8,128)(2,1)S(1)}, u32[]{:S(2)}, u32[]{:S(2)}) %collective-permute-start.5) | collective-permute-done | bytes 196640 | tf_op jit(solution)/shard_map/ppermute | solution.py:487
  39.3 1.5 %collective-permute-start.7 = (bf16[768,256]{1,0:T(8,128)(2,1)S(1)}, bf16[768,256]{1,0:T(8,128)(2,1)S(1)}, u32[]{:S(2)}, u32[]{:S(2)}) collective-permute-start(bf16[768,256]{1,0:T(8,128)(2,1)S(1)} %join.3.refs_0_.refs_2_), channel_id=1, source_target_pairs={{0,4},{2,6},{4,0},{6,2},{8,12},{10,14},{12,8},{14,10},{16,20},{18,... | collective-permute-start | bytes 1179656 | tf_op jit(solution)/shard_map/ppermute | solution.py:487
  40.8 1.5 %collective-permute-start.6 = (bf16[768,256]{1,0:T(8,128)(2,1)S(1)}, bf16[768,256]{1,0:T(8,128)(2,1)S(1)}, u32[]{:S(2)}, u32[]{:S(2)}) collective-permute-start(bf16[768,256]{1,0:T(8,128)(2,1)S(1)} %join.3.refs_0_.refs_2_), channel_id=1, source_target_pairs={{0,2},{2,0},{4,6},{6,4},{8,10},{10,8},{12,14},{14,12},{16,18},{18,... | collective-permute-start | bytes 1179656 | tf_op jit(solution)/shard_map/ppermute | solution.py:487
  42.3 1.2 %copy-done = bf16[1,2048,256]{2,1,0:T(8,128)(2,1)S(1)} copy-done((bf16[1,2048,256]{2,1,0:T(8,128)(2,1)S(1)}, bf16[1,2048,256]{2,1,0:T(8,128)(2,1)}, u32[]{:S(2)}) %copy-start) | copy-done | bytes 1048600
  43.5 1.6 %expert_first.1 = (f32[96,512]{1,0:T(8,128)S(1)}, bf16[1024,256]{1,0:T(8,128)(2,1)S(1)}, bf16[1024,256]{1,0:T(8,128)(2,1)S(1)}, bf16[256,2048]{1,0:T(8,128)(2,1)S(1)}) custom-call(bf16[768,128]{1,0:T(8,128)(2,1)S(1)} %bitcast.19, bf16[2048,256]{1,0:T(8,128)(2,1)S(1)} %bitcast.17, bf16[2048,256]{1,0:T(8,128)(2,1)} %bitcast.29, bf16[256,2048]{1,0:T(8,128)(2,1)} %bitcast.30), custom_call_target="tpu_custom_call" | custom-call | flops 268435456 | bytes 4194304 | tf_op jit(solution)/shard_map/expert_first/pallas_call | solution.py:320
  46.0 1.2 %collective-permute-done.2.b = bf16[768,128]{1,0:T(8,128)(2,1)S(1)} collective-permute-done((bf16[768,128]{1,0:T(8,128)(2,1)S(1)}, bf16[768,128]{1,0:T(8,128)(2,1)S(1)}, u32[]{:S(2)}, u32[]{:S(2)}) %collective-permute-start.2) | collective-permute-done | bytes 196640 | tf_op jit(solution)/shard_map/ppermute | solution.py:476
  47.2 0.7 %add_parts.1 = bf16[768,128]{1,0:T(8,128)(2,1)} custom-call(bf16[768,128]{1,0:T(8,128)(2,1)S(1)} %expert_third.1.a, bf16[768,128]{1,0:T(8,128)(2,1)S(1)} %collective-permute-done.2.b), custom_call_target="tpu_custom_call" | custom-call | flops 262144 | bytes 524288 | tf_op jit(solution)/shard_map/add_parts/pallas_call | solution.py:398
  47.9 3.5 %all-to-all-start.1 = ((bf16[16,48,128]{2,1,0:T(8,128)(2,1)}), bf16[16,48,128]{2,1,0:T(8,128)(2,1)S(1)}, u32[]{:S(2)}, u32[]{:S(2)}) async-start(bf16[16,48,128]{2,1,0:T(8,128)(2,1)} %bitcast.11), calls=%async_computation.1 | async-start | bytes 393216 | tf_op jit(solution)/shard_map/all_to_all | solution.py:481
  51.5 1.9 %collective-permute-start.8 = (bf16[384,256]{1,0:T(8,128)(2,1)S(1)}, bf16[384,256]{1,0:T(8,128)(2,1)S(1)}, u32[]{:S(2)}, u32[]{:S(2)}) collective-permute-start(bf16[384,256]{1,0:T(8,128)(2,1)S(1)} %slice.8), channel_id=1, source_target_pairs={{0,2},{2,0},{4,6},{6,4},{8,10},{10,8},{12,14},{14,12},{16,18},{18,... | collective-permute-start | bytes 589832 | tf_op jit(solution)/shard_map/ppermute | solution.py:487
  53.4 1.5 %collective-permute-start.9 = (bf16[384,256]{1,0:T(8,128)(2,1)S(1)}, bf16[384,256]{1,0:T(8,128)(2,1)S(1)}, u32[]{:S(2)}, u32[]{:S(2)}) collective-permute-start(bf16[384,256]{1,0:T(8,128)(2,1)S(1)} %slice.9), channel_id=1, source_target_pairs={{0,4},{2,6},{4,0},{6,2},{8,12},{10,14},{12,8},{14,10},{16,20},{18,... | collective-permute-start | bytes 589832 | tf_op jit(solution)/shard_map/ppermute | solution.py:487
  55.2 5.3 %collective-permute-done.8.refs_0_ = bf16[384,256]{1,0:T(8,128)(2,1)S(1)} collective-permute-done((bf16[384,256]{1,0:T(8,128)(2,1)S(1)}, bf16[384,256]{1,0:T(8,128)(2,1)S(1)}, u32[]{:S(2)}, u32[]{:S(2)}) %collective-permute-start.8) | collective-permute-done | bytes 196640 | tf_op jit(solution)/shard_map/ppermute | solution.py:487
  60.5 1.0 %collective-permute-done.9.refs_1_ = bf16[384,256]{1,0:T(8,128)(2,1)S(1)} collective-permute-done((bf16[384,256]{1,0:T(8,128)(2,1)S(1)}, bf16[384,256]{1,0:T(8,128)(2,1)S(1)}, u32[]{:S(2)}, u32[]{:S(2)}) %collective-permute-start.9) | collective-permute-done | bytes 196640 | tf_op jit(solution)/shard_map/ppermute | solution.py:487
  62.6 0.8 %fresh.1 = (bf16[16,64]{1,0:T(8,128)(2,1)}, bf16[16,64]{1,0:T(8,128)(2,1)}) custom-call(bf16[16,2048]{1,0:T(8,128)(2,1)S(1)} %get-tuple-element.18.normed, bf16[64,2048]{1,0:T(8,128)(2,1)S(1)} %bitcast.21, bf16[64,2048]{1,0:T(8,128)(2,1)S(1)} %bitcast.22), custom_call_target="tpu_custom_call" | custom-call | flops 16777216 | bytes 524288 | tf_op jit(solution)/shard_map/fresh/pallas_call | solution.py:464
  63.5 1.0 %last.1 = bf16[16,2048]{1,0:T(8,128)(2,1)} custom-call(f32[16,1024]{1,0:T(8,128)S(1)} %combine.1.own, f32[16,1024]{1,0:T(8,128)S(1)} %collective-permute-done.3.other, f32[16,2048]{1,0:T(8,128)S(1)} %dense.1, f32[16,2048]{1,0:T(8,128)S(1)} %collective-permute-done.10.dense_other, bf16[16,2048]{1,0:T(8,128)(2,1)S(1)} %get-tuple-element.28.hidden, ...), custom_call_target="tpu_custom_call" | custom-call | flops 1048576 | bytes 1048576 | tf_op jit(solution)/shard_map/last/pallas_call | solution.py:444
  (44 shorter events, 5.8 us)
Async XLA Ops:
  0.6 0.8 %copy-start.6 = (bf16[16,2048]{1,0:T(8,128)(2,1)S(1)}, bf16[16,2048]{1,0:T(8,128)(2,1)}, u32[]{:S(2)}) copy-start(bf16[16,2048]{1,0:T(8,128)(2,1)} %tokens.1) | copy-start | bytes 196612
  1.5 0.7 %copy-start.7 = (f32[2048]{0:T(1024)S(1)}, f32[2048]{0:T(1024)}, u32[]{:S(2)}) copy-start(f32[2048]{0:T(1024)} %param.25) | copy-start | bytes 24580
  2.2 0.7 %copy-start.9 = (s32[16,6]{0,1:T(8,128)S(1)}, s32[16,6]{0,1:T(8,128)}, u32[]{:S(2)}) copy-start(s32[16,6]{0,1:T(8,128)} %param.32) | copy-start | bytes 1156
  2.9 0.7 %copy-start.10 = (f32[16,6]{0,1:T(8,128)S(1)}, f32[16,6]{0,1:T(8,128)}, u32[]{:S(2)}) copy-start(f32[16,6]{0,1:T(8,128)} %param.33) | copy-start | bytes 1156
  4.9 6.2 %copy-start.8 = (f32[2048]{0:T(1024)S(1)}, f32[2048]{0:T(1024)}, u32[]{:S(2)}) copy-start(f32[2048]{0:T(1024)} %param.31) | copy-start | bytes 24580
  9.6 1.5 %collective-permute-start = (f32[16,2048]{1,0:T(8,128)S(1)}, f32[16,2048]{1,0:T(8,128)S(1)}, u32[]{:S(2)}, u32[]{:S(2)}) collective-permute-start(f32[16,2048]{1,0:T(8,128)S(1)} %get-tuple-element.17.partial), channel_id=1, source_target_pairs={{0,1},{1,0},{2,3},{3,2},{4,5},{5,4},{6,7},{7,6},{8,9},{9,8},{10,11... | collective-permute-start | bytes 393224 | tf_op jit(solution)/shard_map/ppermute | solution.py:476
  12.2 21.1 %all-to-all-start = ((bf16[16,48,128]{2,1,0:T(8,128)(2,1)}), bf16[16,48,128]{2,1,0:T(8,128)(2,1)S(1)}, u32[]{:S(2)}, u32[]{:S(2)}) async-start(bf16[16,48,128]{2,1,0:T(8,128)(2,1)} %bitcast.6), calls=%async_computation | async-start | bytes 393216 | tf_op jit(solution)/shard_map/all_to_all | solution.py:481
  22.0 10.3 %collective-permute-start.4 = (bf16[192,256]{1,0:T(8,128)(2,1)}, bf16[192,256]{1,0:T(8,128)(2,1)S(1)}, u32[]{:S(2)}, u32[]{:S(2)}) collective-permute-start(bf16[192,256]{1,0:T(8,128)(2,1)} %pack.1.refs_0_), channel_id=1, source_target_pairs={{0,16},{2,18},{4,20},{6,22},{8,24},{10,26},{12,28},{14,30},{16,0},... | collective-permute-start | bytes 294920 | tf_op jit(solution)/shard_map/ppermute | solution.py:487
  32.3 0.9 %copy-start.3 = (bf16[192,256]{1,0:T(8,128)(2,1)S(1)}, bf16[192,256]{1,0:T(8,128)(2,1)}, u32[]{:S(2)}) copy-start(bf16[192,256]{1,0:T(8,128)(2,1)} %pack.1.refs_0_) | copy-start | bytes 294916
  33.2 6.0 %collective-permute-start.5 = (bf16[384,256]{1,0:T(8,128)(2,1)S(1)}, bf16[384,256]{1,0:T(8,128)(2,1)S(1)}, u32[]{:S(2)}, u32[]{:S(2)}) collective-permute-start(bf16[384,256]{1,0:T(8,128)(2,1)S(1)} %join.2.refs_0_), channel_id=1, source_target_pairs={{0,8},{2,10},{4,12},{6,14},{8,0},{10,2},{12,4},{14,6},{16,24},{18,... | collective-permute-start | bytes 589832 | tf_op jit(solution)/shard_map/ppermute | solution.py:487
  33.3 11.9 %collective-permute-start.1 = (bf16[768,128]{1,0:T(8,128)(2,1)S(1)}, bf16[768,128]{1,0:T(8,128)(2,1)S(1)}, u32[]{:S(2)}, u32[]{:S(2)}) collective-permute-start(bf16[768,128]{1,0:T(8,128)(2,1)S(1)} %bitcast.18), channel_id=1, source_target_pairs={{0,1},{1,0},{2,3},{3,2},{4,5},{5,4},{6,7},{7,6},{8,9},{9,8},{10,11... | collective-permute-start | bytes 589832 | tf_op jit(solution)/shard_map/ppermute | solution.py:476
  39.3 12.2 %collective-permute-start.7 = (bf16[768,256]{1,0:T(8,128)(2,1)S(1)}, bf16[768,256]{1,0:T(8,128)(2,1)S(1)}, u32[]{:S(2)}, u32[]{:S(2)}) collective-permute-start(bf16[768,256]{1,0:T(8,128)(2,1)S(1)} %join.3.refs_0_.refs_2_), channel_id=1, source_target_pairs={{0,4},{2,6},{4,0},{6,2},{8,12},{10,14},{12,8},{14,10},{16,20},{18,... | collective-permute-start | bytes 1179656 | tf_op jit(solution)/shard_map/ppermute | solution.py:487
  40.8 12.6 %collective-permute-start.6 = (bf16[768,256]{1,0:T(8,128)(2,1)S(1)}, bf16[768,256]{1,0:T(8,128)(2,1)S(1)}, u32[]{:S(2)}, u32[]{:S(2)}) collective-permute-start(bf16[768,256]{1,0:T(8,128)(2,1)S(1)} %join.3.refs_0_.refs_2_), channel_id=1, source_target_pairs={{0,2},{2,0},{4,6},{6,4},{8,10},{10,8},{12,14},{14,12},{16,18},{18,... | collective-permute-start | bytes 1179656 | tf_op jit(solution)/shard_map/ppermute | solution.py:487
  42.3 1.2 %copy-start = (bf16[1,2048,256]{2,1,0:T(8,128)(2,1)S(1)}, bf16[1,2048,256]{2,1,0:T(8,128)(2,1)}, u32[]{:S(2)}) copy-start(bf16[1,2048,256]{2,1,0:T(8,128)(2,1)} %param.34) | copy-start | bytes 3145732
  45.7 1.5 %collective-permute-start.2 = (bf16[768,128]{1,0:T(8,128)(2,1)S(1)}, bf16[768,128]{1,0:T(8,128)(2,1)S(1)}, u32[]{:S(2)}, u32[]{:S(2)}) collective-permute-start(bf16[768,128]{1,0:T(8,128)(2,1)S(1)} %get-tuple-element.26), channel_id=1, source_target_pairs={{0,1},{1,0},{2,3},{3,2},{4,5},{5,4},{6,7},{7,6},{8,9},{9,8},{10,11... | collective-permute-start | bytes 589832 | tf_op jit(solution)/shard_map/ppermute | solution.py:476
  47.9 14.0 %all-to-all-start.1 = ((bf16[16,48,128]{2,1,0:T(8,128)(2,1)}), bf16[16,48,128]{2,1,0:T(8,128)(2,1)S(1)}, u32[]{:S(2)}, u32[]{:S(2)}) async-start(bf16[16,48,128]{2,1,0:T(8,128)(2,1)} %bitcast.11), calls=%async_computation.1 | async-start | bytes 393216 | tf_op jit(solution)/shard_map/all_to_all | solution.py:481
  51.5 11.2 %copy-start.1 = (bf16[2048,64]{0,1:T(8,128)(2,1)S(1)}, bf16[2048,64]{0,1:T(8,128)(2,1)}, u32[]{:S(2)}) copy-start(bf16[2048,64]{0,1:T(8,128)(2,1)} %param.27) | copy-start | bytes 786436
  51.5 11.2 %copy-start.2 = (bf16[2048,64]{0,1:T(8,128)(2,1)S(1)}, bf16[2048,64]{0,1:T(8,128)(2,1)}, u32[]{:S(2)}) copy-start(bf16[2048,64]{0,1:T(8,128)(2,1)} %param.28) | copy-start | bytes 786436
  51.5 12.0 %copy-start.4 = (f32[2048]{0:T(1024)S(1)}, f32[2048]{0:T(1024)}, u32[]{:S(2)}) copy-start(f32[2048]{0:T(1024)} %param.40) | copy-start | bytes 24580
  51.5 12.0 %copy-start.5 = (f32[2048]{0:T(1024)S(1)}, f32[2048]{0:T(1024)}, u32[]{:S(2)}) copy-start(f32[2048]{0:T(1024)} %param.41) | copy-start | bytes 24580
  51.5 9.0 %collective-permute-start.8 = (bf16[384,256]{1,0:T(8,128)(2,1)S(1)}, bf16[384,256]{1,0:T(8,128)(2,1)S(1)}, u32[]{:S(2)}, u32[]{:S(2)}) collective-permute-start(bf16[384,256]{1,0:T(8,128)(2,1)S(1)} %slice.8), channel_id=1, source_target_pairs={{0,2},{2,0},{4,6},{6,4},{8,10},{10,8},{12,14},{14,12},{16,18},{18,... | collective-permute-start | bytes 589832 | tf_op jit(solution)/shard_map/ppermute | solution.py:487
  53.4 8.0 %collective-permute-start.9 = (bf16[384,256]{1,0:T(8,128)(2,1)S(1)}, bf16[384,256]{1,0:T(8,128)(2,1)S(1)}, u32[]{:S(2)}, u32[]{:S(2)}) collective-permute-start(bf16[384,256]{1,0:T(8,128)(2,1)S(1)} %slice.9), channel_id=1, source_target_pairs={{0,4},{2,6},{4,0},{6,2},{8,12},{10,14},{12,8},{14,10},{16,20},{18,... | collective-permute-start | bytes 589832 | tf_op jit(solution)/shard_map/ppermute | solution.py:487
  61.8 1.7 %collective-permute-start.10 = (f32[16,2048]{1,0:T(8,128)S(1)}, f32[16,2048]{1,0:T(8,128)S(1)}, u32[]{:S(2)}, u32[]{:S(2)}) collective-permute-start(f32[16,2048]{1,0:T(8,128)S(1)} %dense.1), channel_id=1, source_target_pairs={{0,1},{1,0},{2,3},{3,2},{4,5},{5,4},{6,7},{7,6},{8,9},{9,8},{10,11... | collective-permute-start | bytes 393224 | tf_op jit(solution)/shard_map/ppermute | solution.py:476
  62.1 1.4 %collective-permute-start.3 = (f32[16,1024]{1,0:T(8,128)S(1)}, f32[16,1024]{1,0:T(8,128)S(1)}, u32[]{:S(2)}, u32[]{:S(2)}) collective-permute-start(f32[16,1024]{1,0:T(8,128)S(1)} %combine.1.own), channel_id=1, source_target_pairs={{0,1},{1,0},{2,3},{3,2},{4,5},{5,4},{6,7},{7,6},{8,9},{9,8},{10,11... | collective-permute-start | bytes 196616 | tf_op jit(solution)/shard_map/ppermute | solution.py:476
  (2 other events, 1.3 us)

commit v5 on v4

--- a/solution.py
+++ b/solution.py
@@ -706,22 +706,18 @@
     if wide:
         from_x = swap_far(block, 1)
         from_y = swap_far(block, 2)
-        part = block.shape[0] // 2
-        diagonal_low = swap_far(from_y[:part], 1)
-        diagonal_high = swap_far(from_x[part:], 2)
-        count = len(columns) // 2
+        from_d = swap_far(block, 3)
         offsets = (
             tuple(columns),
             tuple(c ^ 1 for c in columns),
             tuple(c ^ 2 for c in columns),
-            tuple(c ^ 3 for c in columns[:count]),
-            tuple(c ^ 3 for c in columns[count:]),
+            tuple(c ^ 3 for c in columns),
         )
         pre = dense_early(hidden, (block, from_x, from_y), offsets[:3])
         dense_out = dense(
             hidden,
             pre,
-            (diagonal_low, diagonal_high),
+            (from_d,),
             (block, from_x, from_y),
             offsets[3:] + offsets[:3],
         )

time: 65.1 us -> 71.5 us (1.098)
  blocking collectives: 0 us -> 17 us
  starting transfers between devices: 22.3 us -> 9.47 us
  waiting for transfers between devices: 21.8 us -> 24.9 us
    all_to_all x0 -> x1, blocking collectives: none -> 17 us  [exchange(): lax.all_to_all(blocks, 'ep', split_axis=0, concat_axis=0, tiled=True)]
    all_to_all x2 -> x1, starting transfers between devices: 11.7 us -> 3.85 us  [exchange(): lax.all_to_all(blocks, 'ep', split_axis=0, concat_axis=0, tiled=True)]
    ppermute x6 -> x5, starting transfers between devices: 9.36 us -> 4.43 us  [swap_far(): return lax.ppermute(values, 'ep', [(i, i ^ bit) for i in range(count)])]
    ppermute x6 -> x5, waiting for transfers between devices: 19.6 us -> 23.8 us  [swap_far(): return lax.ppermute(values, 'ep', [(i, i ^ bit) for i in range(count)])]
    ppermute x5, waiting for transfers between devices: 2.2 us -> 1.04 us  [swap_core(): return lax.ppermute(values, 'tp', [(0, 1), (1, 0)])]
  transfers between devices with their start and end apart: 13 -> 11, of which waited for: 6 -> 5; matrix products, arithmetic and copies ran while one was open for 0% -> 0% of each run, Pallas kernels for 10% -> 9%
where the time goes in v5:
time: 71.5 us; the launch traced here: 70.9 us
  waiting for transfers between devices  24.9 us (35%)
  blocking collectives  17 us (24%)
  Pallas kernels  12.5 us (17%)
  starting transfers between devices  9.47 us (13%)
  local copies, waits for them, and re-layouts  6.35 us (9%)
  between operations  0.79 us (1%)
    ppermute x5, waiting for transfers between devices, swap_far(): return lax.ppermute(values, 'ep', [(i, i ^ bit) for i in range(count)])  23.8 us
    all_to_all x1, blocking collectives, exchange(): lax.all_to_all(blocks, 'ep', split_axis=0, concat_axis=0, tiled=True)  17 us
    unnamed x26, local copies, waits for them, and re-layouts  6.35 us
    pallas_call x1, Pallas kernels, attention(): pl.pallas_call(functools.partial(attention_kernel, capacity), out_shape=(...  4.68 us
    ppermute x5, starting transfers between devices, swap_far(): return lax.ppermute(values, 'ep', [(i, i ^ bit) for i in range(count)])  4.43 us
    all_to_all x1, starting transfers between devices, exchange(): lax.all_to_all(blocks, 'ep', split_axis=0, concat_axis=0, tiled=True)  3.85 us
    pallas_call x1, Pallas kernels, expert_first(): pl.pallas_call(first_kernel, out_shape=(jax.ShapeDtypeStruct((count, 2 *...  1.65 us
    pallas_call x1, Pallas kernels, pack(): pl.pallas_call(pack_kernel, out_shape=jax.ShapeDtypeStruct((rows + units...  1.58 us
  transfers between devices with their start and end apart: 11, of which 5 were waited for; matrix products, arithmetic and copies ran while one was open for 0% of the time, Pallas kernels for 9%

profile of v5, /device:TPU:0, one launch (start us, length us, event | category | flops | bytes accessed | tf_op | source)
XLA Modules:
  0.0 70.9 jit_solution(9555781592093755855)
XLA Ops:
  0.6 0.8 %copy-done.6 = bf16[16,2048]{1,0:T(8,128)(2,1)S(1)} copy-done((bf16[16,2048]{1,0:T(8,128)(2,1)S(1)}, bf16[16,2048]{1,0:T(8,128)(2,1)}, u32[]{:S(2)}) %copy-start.6) | copy-done | bytes 65560
  1.5 0.7 copy-done.7
  2.2 0.7 copy-done.9
  2.9 0.7 copy-done.10
  3.5 0.7 copy-done.11
  4.2 0.7 copy-done.12
  4.9 4.7 %attention.1 = (f32[16,2048]{1,0:T(8,128)S(1)}, bf16[16,2048]{1,0:T(8,128)(2,1)S(1)}, bf16[96,16]{1,0:T(8,128)(2,1)S(1)}, f32[96,16]{1,0:T(8,128)S(1)}) custom-call(s32[16]{0:T(128)S(1)} %copy-done.11, f32[4]{0:T(128)S(1)} %copy-done.12, bf16[16,2048]{1,0:T(8,128)(2,1)S(1)} %copy-done.6, f32[1,2048]{1,0:T(1,128)S(1)} %bitcast.26, s32[6,16]{1,0:T(8,128)S(1)} %bitcast.28, ...), custom_call_target="tpu_custom_call" | custom-call | flops 4294967296 | bytes 7340032 | tf_op jit(solution)/shard_map/attention/pallas_call | solution.py:217
  10.1 1.0 %collective-permute-done.other = f32[16,2048]{1,0:T(8,128)S(1)} collective-permute-done((f32[16,2048]{1,0:T(8,128)S(1)}, f32[16,2048]{1,0:T(8,128)S(1)}, u32[]{:S(2)}, u32[]{:S(2)}) %collective-permute-start) | collective-permute-done | bytes 131104 | tf_op jit(solution)/shard_map/ppermute | solution.py:476
  11.5 17.0 %all_to_all.10 = bf16[16,48,128]{2,1,0:T(8,128)(2,1)S(1)} all-to-all(bf16[16,48,128]{2,1,0:T(8,128)(2,1)S(1)} %bitcast.23), channel_id=1, replica_groups=mesh['ep'=16,'tp'=2] {'ep'}, dimensions={0} | all-to-all | bytes 393216 | tf_op jit(solution)/shard_map/all_to_all | solution.py:481
  28.5 1.6 %pack.1.refs_0_ = bf16[192,256]{1,0:T(8,128)(2,1)} custom-call(bf16[128,256]{1,0:T(8,128)(2,1)} %gate_hbm.1, bf16[128,256]{1,0:T(8,128)(2,1)} %up_hbm.1, bf16[256,128]{1,0:T(8,128)(2,1)} %down_hbm.1), custom_call_target="tpu_custom_call" | custom-call | flops 4294967296 | bytes 262144 | tf_op jit(solution)/shard_map/pack/pallas_call | solution.py:509
  30.1 0.8 %collective-permute-start.4 = (bf16[192,256]{1,0:T(8,128)(2,1)}, bf16[192,256]{1,0:T(8,128)(2,1)S(1)}, u32[]{:S(2)}, u32[]{:S(2)}) collective-permute-start(bf16[192,256]{1,0:T(8,128)(2,1)} %pack.1.refs_0_), channel_id=1, source_target_pairs={{0,16},{2,18},{4,20},{6,22},{8,24},{10,26},{12,28},{14,30},{16,0},... | collective-permute-start | bytes 294920 | tf_op jit(solution)/shard_map/ppermute | solution.py:487
  30.9 7.7 %collective-permute-done.4.refs_1_ = bf16[192,256]{1,0:T(8,128)(2,1)S(1)} collective-permute-done((bf16[192,256]{1,0:T(8,128)(2,1)}, bf16[192,256]{1,0:T(8,128)(2,1)S(1)}, u32[]{:S(2)}, u32[]{:S(2)}) %collective-permute-start.4) | collective-permute-done | bytes 98336 | tf_op jit(solution)/shard_map/ppermute | solution.py:487
  38.6 0.9 %copy-done.3 = bf16[192,256]{1,0:T(8,128)(2,1)S(1)} copy-done((bf16[192,256]{1,0:T(8,128)(2,1)S(1)}, bf16[192,256]{1,0:T(8,128)(2,1)}, u32[]{:S(2)}) %copy-start.3) | copy-done | bytes 98328
  39.6 1.2 %copy-done = bf16[1,2048,256]{2,1,0:T(8,128)(2,1)S(1)} copy-done((bf16[1,2048,256]{2,1,0:T(8,128)(2,1)S(1)}, bf16[1,2048,256]{2,1,0:T(8,128)(2,1)}, u32[]{:S(2)}) %copy-start) | copy-done | bytes 1048600
  40.8 1.6 %expert_first.1 = (f32[96,512]{1,0:T(8,128)S(1)}, bf16[1024,256]{1,0:T(8,128)(2,1)S(1)}, bf16[1024,256]{1,0:T(8,128)(2,1)S(1)}, bf16[256,2048]{1,0:T(8,128)(2,1)S(1)}) custom-call(bf16[768,128]{1,0:T(8,128)(2,1)S(1)} %bitcast.19, bf16[2048,256]{1,0:T(8,128)(2,1)S(1)} %bitcast.17, bf16[2048,256]{1,0:T(8,128)(2,1)} %bitcast.30, bf16[256,2048]{1,0:T(8,128)(2,1)} %bitcast.31), custom_call_target="tpu_custom_call" | custom-call | flops 268435456 | bytes 4194304 | tf_op jit(solution)/shard_map/expert_first/pallas_call | solution.py:320
  43.0 3.0 %collective-permute-done.5.refs_1_ = bf16[384,256]{1,0:T(8,128)(2,1)S(1)} collective-permute-done((bf16[384,256]{1,0:T(8,128)(2,1)S(1)}, bf16[384,256]{1,0:T(8,128)(2,1)S(1)}, u32[]{:S(2)}, u32[]{:S(2)}) %collective-permute-start.5) | collective-permute-done | bytes 196640 | tf_op jit(solution)/shard_map/ppermute | solution.py:487
  46.0 1.3 %collective-permute-start.6 = (bf16[768,256]{1,0:T(8,128)(2,1)S(1)}, bf16[768,256]{1,0:T(8,128)(2,1)S(1)}, u32[]{:S(2)}, u32[]{:S(2)}) collective-permute-start(bf16[768,256]{1,0:T(8,128)(2,1)S(1)} %join.3.refs_0_.refs_1_), channel_id=1, source_target_pairs={{0,2},{2,0},{4,6},{6,4},{8,10},{10,8},{12,14},{14,12},{16,18},{18,... | collective-permute-start | bytes 1179656 | tf_op jit(solution)/shard_map/ppermute | solution.py:487
  47.6 2.0 %collective-permute-start.8 = (bf16[768,256]{1,0:T(8,128)(2,1)S(1)}, bf16[768,256]{1,0:T(8,128)(2,1)S(1)}, u32[]{:S(2)}, u32[]{:S(2)}) collective-permute-start(bf16[768,256]{1,0:T(8,128)(2,1)S(1)} %join.3.refs_0_.refs_1_), channel_id=1, source_target_pairs={{0,6},{2,4},{4,2},{6,0},{8,14},{10,12},{12,10},{14,8},{16,22},{18,... | collective-permute-start | bytes 1179656 | tf_op jit(solution)/shard_map/ppermute | solution.py:487
  49.9 0.7 %add_parts.1 = bf16[768,128]{1,0:T(8,128)(2,1)} custom-call(bf16[768,128]{1,0:T(8,128)(2,1)S(1)} %expert_third.1.a, bf16[768,128]{1,0:T(8,128)(2,1)S(1)} %collective-permute-done.2.b), custom_call_target="tpu_custom_call" | custom-call | flops 262144 | bytes 524288 | tf_op jit(solution)/shard_map/add_parts/pallas_call | solution.py:398
  50.6 3.8 %all-to-all-start.1 = ((bf16[16,48,128]{2,1,0:T(8,128)(2,1)}), bf16[16,48,128]{2,1,0:T(8,128)(2,1)S(1)}, u32[]{:S(2)}, u32[]{:S(2)}) async-start(bf16[16,48,128]{2,1,0:T(8,128)(2,1)} %bitcast.11), calls=%async_computation.1 | async-start | bytes 393216 | tf_op jit(solution)/shard_map/all_to_all | solution.py:481
  54.5 4.1 %collective-permute-done.6.refs_1_.refs_2_ = bf16[768,256]{1,0:T(8,128)(2,1)S(1)} collective-permute-done((bf16[768,256]{1,0:T(8,128)(2,1)S(1)}, bf16[768,256]{1,0:T(8,128)(2,1)S(1)}, u32[]{:S(2)}, u32[]{:S(2)}) %collective-permute-start.6) | collective-permute-done | bytes 393248 | tf_op jit(solution)/shard_map/ppermute | solution.py:487
  58.6 9.1 %collective-permute-done.7.refs_2_.refs_3_ = bf16[768,256]{1,0:T(8,128)(2,1)S(1)} collective-permute-done((bf16[768,256]{1,0:T(8,128)(2,1)S(1)}, bf16[768,256]{1,0:T(8,128)(2,1)S(1)}, u32[]{:S(2)}, u32[]{:S(2)}) %collective-permute-start.7) | collective-permute-done | bytes 393248 | tf_op jit(solution)/shard_map/ppermute | solution.py:487
  69.1 0.8 %fresh.1 = (bf16[16,64]{1,0:T(8,128)(2,1)}, bf16[16,64]{1,0:T(8,128)(2,1)}) custom-call(bf16[16,2048]{1,0:T(8,128)(2,1)S(1)} %get-tuple-element.18.normed, bf16[64,2048]{1,0:T(8,128)(2,1)S(1)} %bitcast.21, bf16[64,2048]{1,0:T(8,128)(2,1)S(1)} %bitcast.22), custom_call_target="tpu_custom_call" | custom-call | flops 16777216 | bytes 524288 | tf_op jit(solution)/shard_map/fresh/pallas_call | solution.py:464
  70.0 1.0 %last.1 = bf16[16,2048]{1,0:T(8,128)(2,1)} custom-call(f32[16,1024]{1,0:T(8,128)S(1)} %combine.1.own, f32[16,1024]{1,0:T(8,128)S(1)} %collective-permute-done.3.other, f32[16,2048]{1,0:T(8,128)S(1)} %dense.1, f32[16,2048]{1,0:T(8,128)S(1)} %collective-permute-done.9.dense_other, bf16[16,2048]{1,0:T(8,128)(2,1)S(1)} %get-tuple-element.28.hidden, ...), custom_call_target="tpu_custom_call" | custom-call | flops 1048576 | bytes 1048576 | tf_op jit(solution)/shard_map/last/pallas_call | solution.py:444
  (39 shorter events, 3.6 us)
Async XLA Ops:
  0.6 0.8 %copy-start.6 = (bf16[16,2048]{1,0:T(8,128)(2,1)S(1)}, bf16[16,2048]{1,0:T(8,128)(2,1)}, u32[]{:S(2)}) copy-start(bf16[16,2048]{1,0:T(8,128)(2,1)} %tokens.1) | copy-start | bytes 196612
  1.5 0.7 copy-start.7
  2.2 0.7 copy-start.9
  2.9 0.7 copy-start.10
  3.5 0.7 copy-start.11
  4.2 0.7 copy-start.12
  4.9 6.2 %copy-start.8 = (f32[2048]{0:T(1024)S(1)}, f32[2048]{0:T(1024)}, u32[]{:S(2)}) copy-start(f32[2048]{0:T(1024)} %param.31) | copy-start | bytes 24580
  9.6 1.5 %collective-permute-start = (f32[16,2048]{1,0:T(8,128)S(1)}, f32[16,2048]{1,0:T(8,128)S(1)}, u32[]{:S(2)}, u32[]{:S(2)}) collective-permute-start(f32[16,2048]{1,0:T(8,128)S(1)} %get-tuple-element.17.partial), channel_id=1, source_target_pairs={{0,1},{1,0},{2,3},{3,2},{4,5},{5,4},{6,7},{7,6},{8,9},{9,8},{10,11... | collective-permute-start | bytes 393224 | tf_op jit(solution)/shard_map/ppermute | solution.py:476
  28.5 14.0 %collective-permute-start.1 = (bf16[768,128]{1,0:T(8,128)(2,1)S(1)}, bf16[768,128]{1,0:T(8,128)(2,1)S(1)}, u32[]{:S(2)}, u32[]{:S(2)}) collective-permute-start(bf16[768,128]{1,0:T(8,128)(2,1)S(1)} %bitcast.18), channel_id=1, source_target_pairs={{0,1},{1,0},{2,3},{3,2},{4,5},{5,4},{6,7},{7,6},{8,9},{9,8},{10,11... | collective-permute-start | bytes 589832 | tf_op jit(solution)/shard_map/ppermute | solution.py:476
  30.1 8.5 %collective-permute-start.4 = (bf16[192,256]{1,0:T(8,128)(2,1)}, bf16[192,256]{1,0:T(8,128)(2,1)S(1)}, u32[]{:S(2)}, u32[]{:S(2)}) collective-permute-start(bf16[192,256]{1,0:T(8,128)(2,1)} %pack.1.refs_0_), channel_id=1, source_target_pairs={{0,16},{2,18},{4,20},{6,22},{8,24},{10,26},{12,28},{14,30},{16,0},... | collective-permute-start | bytes 294920 | tf_op jit(solution)/shard_map/ppermute | solution.py:487
  38.6 0.9 %copy-start.3 = (bf16[192,256]{1,0:T(8,128)(2,1)S(1)}, bf16[192,256]{1,0:T(8,128)(2,1)}, u32[]{:S(2)}) copy-start(bf16[192,256]{1,0:T(8,128)(2,1)} %pack.1.refs_0_) | copy-start | bytes 294916
  39.5 6.5 %collective-permute-start.5 = (bf16[384,256]{1,0:T(8,128)(2,1)S(1)}, bf16[384,256]{1,0:T(8,128)(2,1)S(1)}, u32[]{:S(2)}, u32[]{:S(2)}) collective-permute-start(bf16[384,256]{1,0:T(8,128)(2,1)S(1)} %join.2.refs_0_), channel_id=1, source_target_pairs={{0,8},{2,10},{4,12},{6,14},{8,0},{10,2},{12,4},{14,6},{16,24},{18,... | collective-permute-start | bytes 589832 | tf_op jit(solution)/shard_map/ppermute | solution.py:487
  39.5 1.2 %copy-start = (bf16[1,2048,256]{2,1,0:T(8,128)(2,1)S(1)}, bf16[1,2048,256]{2,1,0:T(8,128)(2,1)}, u32[]{:S(2)}) copy-start(bf16[1,2048,256]{2,1,0:T(8,128)(2,1)} %param.34) | copy-start | bytes 3145732
  43.0 6.9 %collective-permute-start.2 = (bf16[768,128]{1,0:T(8,128)(2,1)S(1)}, bf16[768,128]{1,0:T(8,128)(2,1)S(1)}, u32[]{:S(2)}, u32[]{:S(2)}) collective-permute-start(bf16[768,128]{1,0:T(8,128)(2,1)S(1)} %get-tuple-element.26), channel_id=1, source_target_pairs={{0,1},{1,0},{2,3},{3,2},{4,5},{5,4},{6,7},{7,6},{8,9},{9,8},{10,11... | collective-permute-start | bytes 589832 | tf_op jit(solution)/shard_map/ppermute | solution.py:476
  46.0 12.6 %collective-permute-start.6 = (bf16[768,256]{1,0:T(8,128)(2,1)S(1)}, bf16[768,256]{1,0:T(8,128)(2,1)S(1)}, u32[]{:S(2)}, u32[]{:S(2)}) collective-permute-start(bf16[768,256]{1,0:T(8,128)(2,1)S(1)} %join.3.refs_0_.refs_1_), channel_id=1, source_target_pairs={{0,2},{2,0},{4,6},{6,4},{8,10},{10,8},{12,14},{14,12},{16,18},{18,... | collective-permute-start | bytes 1179656 | tf_op jit(solution)/shard_map/ppermute | solution.py:487
  47.4 20.3 %collective-permute-start.7 = (bf16[768,256]{1,0:T(8,128)(2,1)S(1)}, bf16[768,256]{1,0:T(8,128)(2,1)S(1)}, u32[]{:S(2)}, u32[]{:S(2)}) collective-permute-start(bf16[768,256]{1,0:T(8,128)(2,1)S(1)} %join.3.refs_0_.refs_1_), channel_id=1, source_target_pairs={{0,4},{2,6},{4,0},{6,2},{8,12},{10,14},{12,8},{14,10},{16,20},{18,... | collective-permute-start | bytes 1179656 | tf_op jit(solution)/shard_map/ppermute | solution.py:487
  47.6 20.3 %collective-permute-start.8 = (bf16[768,256]{1,0:T(8,128)(2,1)S(1)}, bf16[768,256]{1,0:T(8,128)(2,1)S(1)}, u32[]{:S(2)}, u32[]{:S(2)}) collective-permute-start(bf16[768,256]{1,0:T(8,128)(2,1)S(1)} %join.3.refs_0_.refs_1_), channel_id=1, source_target_pairs={{0,6},{2,4},{4,2},{6,0},{8,14},{10,12},{12,10},{14,8},{16,22},{18,... | collective-permute-start | bytes 1179656 | tf_op jit(solution)/shard_map/ppermute | solution.py:487
  49.8 19.2 %copy-start.1 = (bf16[2048,64]{0,1:T(8,128)(2,1)S(1)}, bf16[2048,64]{0,1:T(8,128)(2,1)}, u32[]{:S(2)}) copy-start(bf16[2048,64]{0,1:T(8,128)(2,1)} %param.27) | copy-start | bytes 786436
  49.9 19.2 %copy-start.2 = (bf16[2048,64]{0,1:T(8,128)(2,1)S(1)}, bf16[2048,64]{0,1:T(8,128)(2,1)}, u32[]{:S(2)}) copy-start(bf16[2048,64]{0,1:T(8,128)(2,1)} %param.28) | copy-start | bytes 786436
  50.6 19.4 %copy-start.4 = (f32[2048]{0:T(1024)S(1)}, f32[2048]{0:T(1024)}, u32[]{:S(2)}) copy-start(f32[2048]{0:T(1024)} %param.40) | copy-start | bytes 24580
  50.6 19.4 %copy-start.5 = (f32[2048]{0:T(1024)S(1)}, f32[2048]{0:T(1024)}, u32[]{:S(2)}) copy-start(f32[2048]{0:T(1024)} %param.41) | copy-start | bytes 24580
  50.6 17.7 %all-to-all-start.1 = ((bf16[16,48,128]{2,1,0:T(8,128)(2,1)}), bf16[16,48,128]{2,1,0:T(8,128)(2,1)S(1)}, u32[]{:S(2)}, u32[]{:S(2)}) async-start(bf16[16,48,128]{2,1,0:T(8,128)(2,1)} %bitcast.11), calls=%async_computation.1 | async-start | bytes 393216 | tf_op jit(solution)/shard_map/all_to_all | solution.py:481
  68.3 1.7 %collective-permute-start.9 = (f32[16,2048]{1,0:T(8,128)S(1)}, f32[16,2048]{1,0:T(8,128)S(1)}, u32[]{:S(2)}, u32[]{:S(2)}) collective-permute-start(f32[16,2048]{1,0:T(8,128)S(1)} %dense.1), channel_id=1, source_target_pairs={{0,1},{1,0},{2,3},{3,2},{4,5},{5,4},{6,7},{7,6},{8,9},{9,8},{10,11... | collective-permute-start | bytes 393224 | tf_op jit(solution)/shard_map/ppermute | solution.py:476
  68.6 1.4 %collective-permute-start.3 = (f32[16,1024]{1,0:T(8,128)S(1)}, f32[16,1024]{1,0:T(8,128)S(1)}, u32[]{:S(2)}, u32[]{:S(2)}) collective-permute-start(f32[16,1024]{1,0:T(8,128)S(1)} %combine.1.own), channel_id=1, source_target_pairs={{0,1},{1,0},{2,3},{3,2},{4,5},{5,4},{6,7},{7,6},{8,9},{9,8},{10,11... | collective-permute-start | bytes 196616 | tf_op jit(solution)/shard_map/ppermute | solution.py:476

commit v6 on v5

--- a/solution.py
+++ b/solution.py
@@ -666,18 +666,15 @@
     slots = experts * capacity
     rows = dense_gate.shape[0]
     share = dense_gate.shape[1] // lax.axis_size("tp")
-    wide = rows == LANES and share == LANES
+    wide = rows == LANES and share == LANES and ep_count == 16
     if wide:
         block = pack(dense_gate, dense_up, dense_down)
-        columns = [0]
-        bit = ep_count // 2
-        far = []
-        while bit > 2:
-            far.append(swap_far(block, bit))
-            columns = columns + [c ^ bit for c in columns]
-            if bit > 4 or bit == 4:
-                block = join(block, far[-1])
-            bit //= 2
+        far, near = ep_count // 2, ep_count // 4
+        block_far = swap_far(block, far)
+        block_near = swap_far(block, near)
+        block_both = swap_far(block_far, near)
+        block = join(block, block_far, block_near, block_both)
+        columns = [0, far, near, far + near]
     partial, normed, place, portion = attention(
         tokens,
         norm_in,

time: 71.5 us -> 68.6 us (0.959)
  waiting for transfers between devices: 24.9 us -> 21.6 us
  starting transfers between devices: 9.47 us -> 10.8 us
  local copies, waits for them, and re-layouts: 6.35 us -> 5.46 us
    ppermute x5 -> x6, waiting for transfers between devices: 23.8 us -> 20.6 us  [swap_far(): return lax.ppermute(values, 'ep', [(i, i ^ bit) for i in range(count)])]
    ppermute x5 -> x6, starting transfers between devices: 4.43 us -> 5.91 us  [swap_far(): return lax.ppermute(values, 'ep', [(i, i ^ bit) for i in range(count)])]
    unnamed x26, local copies, waits for them, and re-layouts: 6.35 us -> 5.46 us
  transfers between devices with their start and end apart: 11 -> 12, of which waited for: 5 -> 5; matrix products, arithmetic and copies ran while one was open for 0% -> 0% of each run, Pallas kernels for 9% -> 9%
where the time goes in v6:
time: 68.6 us; the launch traced here: 68.1 us
  waiting for transfers between devices  21.6 us (31%)
  blocking collectives  17 us (25%)
  Pallas kernels  12.5 us (18%)
  starting transfers between devices  10.8 us (16%)
  local copies, waits for them, and re-layouts  5.46 us (8%)
  between operations  0.78 us (1%)
    ppermute x6, waiting for transfers between devices, swap_far(): return lax.ppermute(values, 'ep', [(i, i ^ bit) for i in range(count)])  20.6 us
    all_to_all x1, blocking collectives, exchange(): lax.all_to_all(blocks, 'ep', split_axis=0, concat_axis=0, tiled=True)  17 us
    ppermute x6, starting transfers between devices, swap_far(): return lax.ppermute(values, 'ep', [(i, i ^ bit) for i in range(count)])  5.91 us
    unnamed x26, local copies, waits for them, and re-layouts  5.46 us
    pallas_call x1, Pallas kernels, attention(): pl.pallas_call(functools.partial(attention_kernel, capacity), out_shape=(...  4.68 us
    all_to_all x1, starting transfers between devices, exchange(): lax.all_to_all(blocks, 'ep', split_axis=0, concat_axis=0, tiled=True)  3.65 us
    pallas_call x1, Pallas kernels, expert_first(): pl.pallas_call(first_kernel, out_shape=(jax.ShapeDtypeStruct((count, 2 *...  1.67 us
    pallas_call x1, Pallas kernels, pack(): pl.pallas_call(pack_kernel, out_shape=jax.ShapeDtypeStruct((rows + units...  1.59 us
  transfers between devices with their start and end apart: 12, of which 5 were waited for; matrix products, arithmetic and copies ran while one was open for 0% of the time, Pallas kernels for 9%

profile of v6, /device:TPU:0, one launch (start us, length us, event | category | flops | bytes accessed | tf_op | source)
XLA Modules:
  0.0 68.1 jit_solution(4865603656955684357)
XLA Ops:
  0.6 0.8 %copy-done.6 = bf16[16,2048]{1,0:T(8,128)(2,1)S(1)} copy-done((bf16[16,2048]{1,0:T(8,128)(2,1)S(1)}, bf16[16,2048]{1,0:T(8,128)(2,1)}, u32[]{:S(2)}) %copy-start.6) | copy-done | bytes 65560
  1.5 0.7 %copy-done.7 = f32[2048]{0:T(1024)S(1)} copy-done((f32[2048]{0:T(1024)S(1)}, f32[2048]{0:T(1024)}, u32[]{:S(2)}) %copy-start.7) | copy-done | bytes 8216
  2.2 0.7 %copy-done.9 = s32[16,6]{0,1:T(8,128)S(1)} copy-done((s32[16,6]{0,1:T(8,128)S(1)}, s32[16,6]{0,1:T(8,128)}, u32[]{:S(2)}) %copy-start.9) | copy-done | bytes 408
  2.9 0.7 %copy-done.10 = f32[16,6]{0,1:T(8,128)S(1)} copy-done((f32[16,6]{0,1:T(8,128)S(1)}, f32[16,6]{0,1:T(8,128)}, u32[]{:S(2)}) %copy-start.10) | copy-done | bytes 408
  3.5 0.7 copy-done.11
  4.2 0.7 copy-done.12
  4.9 4.7 %attention.1 = (f32[16,2048]{1,0:T(8,128)S(1)}, bf16[16,2048]{1,0:T(8,128)(2,1)S(1)}, bf16[96,16]{1,0:T(8,128)(2,1)S(1)}, f32[96,16]{1,0:T(8,128)S(1)}) custom-call(s32[16]{0:T(128)S(1)} %copy-done.11, f32[4]{0:T(128)S(1)} %copy-done.12, bf16[16,2048]{1,0:T(8,128)(2,1)S(1)} %copy-done.6, f32[1,2048]{1,0:T(1,128)S(1)} %bitcast.26, s32[6,16]{1,0:T(8,128)S(1)} %bitcast.28, ...), custom_call_target="tpu_custom_call" | custom-call | flops 4294967296 | bytes 7340032 | tf_op jit(solution)/shard_map/attention/pallas_call | solution.py:217
  10.1 1.0 %collective-permute-done.other = f32[16,2048]{1,0:T(8,128)S(1)} collective-permute-done((f32[16,2048]{1,0:T(8,128)S(1)}, f32[16,2048]{1,0:T(8,128)S(1)}, u32[]{:S(2)}, u32[]{:S(2)}) %collective-permute-start) | collective-permute-done | bytes 131104 | tf_op jit(solution)/shard_map/ppermute | solution.py:476
  11.5 17.0 %all_to_all.10 = bf16[16,48,128]{2,1,0:T(8,128)(2,1)S(1)} all-to-all(bf16[16,48,128]{2,1,0:T(8,128)(2,1)S(1)} %bitcast.23), channel_id=1, replica_groups=mesh['ep'=16,'tp'=2] {'ep'}, dimensions={0} | all-to-all | bytes 393216 | tf_op jit(solution)/shard_map/all_to_all | solution.py:481
  28.5 1.6 %pack.1.refs_0_ = bf16[192,256]{1,0:T(8,128)(2,1)} custom-call(bf16[128,256]{1,0:T(8,128)(2,1)} %gate_hbm.1, bf16[128,256]{1,0:T(8,128)(2,1)} %up_hbm.1, bf16[256,128]{1,0:T(8,128)(2,1)} %down_hbm.1), custom_call_target="tpu_custom_call" | custom-call | flops 4294967296 | bytes 262144 | tf_op jit(solution)/shard_map/pack/pallas_call | solution.py:509
  30.1 0.8 %collective-permute-start.4 = (bf16[192,256]{1,0:T(8,128)(2,1)}, bf16[192,256]{1,0:T(8,128)(2,1)S(1)}, u32[]{:S(2)}, u32[]{:S(2)}) collective-permute-start(bf16[192,256]{1,0:T(8,128)(2,1)} %pack.1.refs_0_), channel_id=1, source_target_pairs={{0,16},{2,18},{4,20},{6,22},{8,24},{10,26},{12,28},{14,30},{16,0},... | collective-permute-start | bytes 294920 | tf_op jit(solution)/shard_map/ppermute | solution.py:487
  30.9 1.5 %collective-permute-start.5 = (bf16[192,256]{1,0:T(8,128)(2,1)}, bf16[192,256]{1,0:T(8,128)(2,1)S(1)}, u32[]{:S(2)}, u32[]{:S(2)}) collective-permute-start(bf16[192,256]{1,0:T(8,128)(2,1)} %pack.1.refs_0_), channel_id=1, source_target_pairs={{0,8},{2,10},{4,12},{6,14},{8,0},{10,2},{12,4},{14,6},{16,24},{18,... | collective-permute-start | bytes 294920 | tf_op jit(solution)/shard_map/ppermute | solution.py:487
  32.4 6.1 %collective-permute-done.4.refs_1_ = bf16[192,256]{1,0:T(8,128)(2,1)S(1)} collective-permute-done((bf16[192,256]{1,0:T(8,128)(2,1)}, bf16[192,256]{1,0:T(8,128)(2,1)S(1)}, u32[]{:S(2)}, u32[]{:S(2)}) %collective-permute-start.4) | collective-permute-done | bytes 98336 | tf_op jit(solution)/shard_map/ppermute | solution.py:487
  38.6 1.2 %copy-done = bf16[1,2048,256]{2,1,0:T(8,128)(2,1)S(1)} copy-done((bf16[1,2048,256]{2,1,0:T(8,128)(2,1)S(1)}, bf16[1,2048,256]{2,1,0:T(8,128)(2,1)}, u32[]{:S(2)}) %copy-start) | copy-done | bytes 1048600
  39.8 1.7 %expert_first.1 = (f32[96,512]{1,0:T(8,128)S(1)}, bf16[1024,256]{1,0:T(8,128)(2,1)S(1)}, bf16[1024,256]{1,0:T(8,128)(2,1)S(1)}, bf16[256,2048]{1,0:T(8,128)(2,1)S(1)}) custom-call(bf16[768,128]{1,0:T(8,128)(2,1)S(1)} %bitcast.19, bf16[2048,256]{1,0:T(8,128)(2,1)S(1)} %bitcast.17, bf16[2048,256]{1,0:T(8,128)(2,1)} %bitcast.30, bf16[256,2048]{1,0:T(8,128)(2,1)} %bitcast.31), custom_call_target="tpu_custom_call" | custom-call | flops 268435456 | bytes 4194304 | tf_op jit(solution)/shard_map/expert_first/pallas_call | solution.py:320
  42.1 1.1 %collective-permute-done.6.refs_3_ = bf16[192,256]{1,0:T(8,128)(2,1)S(1)} collective-permute-done((bf16[192,256]{1,0:T(8,128)(2,1)S(1)}, bf16[192,256]{1,0:T(8,128)(2,1)S(1)}, u32[]{:S(2)}, u32[]{:S(2)}) %collective-permute-start.6) | collective-permute-done | bytes 98336 | tf_op jit(solution)/shard_map/ppermute | solution.py:487
  43.2 1.1 %collective-permute-start.7 = (bf16[768,256]{1,0:T(8,128)(2,1)S(1)}, bf16[768,256]{1,0:T(8,128)(2,1)S(1)}, u32[]{:S(2)}, u32[]{:S(2)}) collective-permute-start(bf16[768,256]{1,0:T(8,128)(2,1)S(1)} %join.1.refs_0_.refs_1_), channel_id=1, source_target_pairs={{0,2},{2,0},{4,6},{6,4},{8,10},{10,8},{12,14},{14,12},{16,18},{18,... | collective-permute-start | bytes 1179656 | tf_op jit(solution)/shard_map/ppermute | solution.py:487
  44.7 2.1 %collective-permute-start.9 = (bf16[768,256]{1,0:T(8,128)(2,1)S(1)}, bf16[768,256]{1,0:T(8,128)(2,1)S(1)}, u32[]{:S(2)}, u32[]{:S(2)}) collective-permute-start(bf16[768,256]{1,0:T(8,128)(2,1)S(1)} %join.1.refs_0_.refs_1_), channel_id=1, source_target_pairs={{0,6},{2,4},{4,2},{6,0},{8,14},{10,12},{12,10},{14,8},{16,22},{18,... | collective-permute-start | bytes 1179656 | tf_op jit(solution)/shard_map/ppermute | solution.py:487
  47.1 0.7 %add_parts.1 = bf16[768,128]{1,0:T(8,128)(2,1)} custom-call(bf16[768,128]{1,0:T(8,128)(2,1)S(1)} %expert_third.1.a, bf16[768,128]{1,0:T(8,128)(2,1)S(1)} %collective-permute-done.2.b), custom_call_target="tpu_custom_call" | custom-call | flops 262144 | bytes 524288 | tf_op jit(solution)/shard_map/add_parts/pallas_call | solution.py:398
  47.8 3.7 %all-to-all-start.1 = ((bf16[16,48,128]{2,1,0:T(8,128)(2,1)}), bf16[16,48,128]{2,1,0:T(8,128)(2,1)S(1)}, u32[]{:S(2)}, u32[]{:S(2)}) async-start(bf16[16,48,128]{2,1,0:T(8,128)(2,1)} %bitcast.11), calls=%async_computation.1 | async-start | bytes 393216 | tf_op jit(solution)/shard_map/all_to_all | solution.py:481
  51.5 4.3 %collective-permute-done.7.refs_1_.refs_2_ = bf16[768,256]{1,0:T(8,128)(2,1)S(1)} collective-permute-done((bf16[768,256]{1,0:T(8,128)(2,1)S(1)}, bf16[768,256]{1,0:T(8,128)(2,1)S(1)}, u32[]{:S(2)}, u32[]{:S(2)}) %collective-permute-start.7) | collective-permute-done | bytes 393248 | tf_op jit(solution)/shard_map/ppermute | solution.py:487
  55.8 9.0 %collective-permute-done.8.refs_2_.refs_3_ = bf16[768,256]{1,0:T(8,128)(2,1)S(1)} collective-permute-done((bf16[768,256]{1,0:T(8,128)(2,1)S(1)}, bf16[768,256]{1,0:T(8,128)(2,1)S(1)}, u32[]{:S(2)}, u32[]{:S(2)}) %collective-permute-start.8) | collective-permute-done | bytes 393248 | tf_op jit(solution)/shard_map/ppermute | solution.py:487
  66.2 0.8 %fresh.1 = (bf16[16,64]{1,0:T(8,128)(2,1)}, bf16[16,64]{1,0:T(8,128)(2,1)}) custom-call(bf16[16,2048]{1,0:T(8,128)(2,1)S(1)} %get-tuple-element.18.normed, bf16[64,2048]{1,0:T(8,128)(2,1)S(1)} %bitcast.21, bf16[64,2048]{1,0:T(8,128)(2,1)S(1)} %bitcast.22), custom_call_target="tpu_custom_call" | custom-call | flops 16777216 | bytes 524288 | tf_op jit(solution)/shard_map/fresh/pallas_call | solution.py:464
  67.1 1.0 %last.1 = bf16[16,2048]{1,0:T(8,128)(2,1)} custom-call(f32[16,1024]{1,0:T(8,128)S(1)} %combine.1.own, f32[16,1024]{1,0:T(8,128)S(1)} %collective-permute-done.3.other, f32[16,2048]{1,0:T(8,128)S(1)} %dense.1, f32[16,2048]{1,0:T(8,128)S(1)} %collective-permute-done.10.dense_other, bf16[16,2048]{1,0:T(8,128)(2,1)S(1)} %get-tuple-element.28.hidden, ...), custom_call_target="tpu_custom_call" | custom-call | flops 1048576 | bytes 1048576 | tf_op jit(solution)/shard_map/last/pallas_call | solution.py:444
  (40 shorter events, 3.7 us)
Async XLA Ops:
  0.6 0.8 %copy-start.6 = (bf16[16,2048]{1,0:T(8,128)(2,1)S(1)}, bf16[16,2048]{1,0:T(8,128)(2,1)}, u32[]{:S(2)}) copy-start(bf16[16,2048]{1,0:T(8,128)(2,1)} %tokens.1) | copy-start | bytes 196612
  1.5 0.7 %copy-start.7 = (f32[2048]{0:T(1024)S(1)}, f32[2048]{0:T(1024)}, u32[]{:S(2)}) copy-start(f32[2048]{0:T(1024)} %param.25) | copy-start | bytes 24580
  2.2 0.7 %copy-start.9 = (s32[16,6]{0,1:T(8,128)S(1)}, s32[16,6]{0,1:T(8,128)}, u32[]{:S(2)}) copy-start(s32[16,6]{0,1:T(8,128)} %param.32) | copy-start | bytes 1156
  2.9 0.7 %copy-start.10 = (f32[16,6]{0,1:T(8,128)S(1)}, f32[16,6]{0,1:T(8,128)}, u32[]{:S(2)}) copy-start(f32[16,6]{0,1:T(8,128)} %param.33) | copy-start | bytes 1156
  3.5 0.7 copy-start.11
  4.9 6.2 %copy-start.8 = (f32[2048]{0:T(1024)S(1)}, f32[2048]{0:T(1024)}, u32[]{:S(2)}) copy-start(f32[2048]{0:T(1024)} %param.31) | copy-start | bytes 24580
  9.6 1.5 %collective-permute-start = (f32[16,2048]{1,0:T(8,128)S(1)}, f32[16,2048]{1,0:T(8,128)S(1)}, u32[]{:S(2)}, u32[]{:S(2)}) collective-permute-start(f32[16,2048]{1,0:T(8,128)S(1)} %get-tuple-element.17.partial), channel_id=1, source_target_pairs={{0,1},{1,0},{2,3},{3,2},{4,5},{5,4},{6,7},{7,6},{8,9},{9,8},{10,11... | collective-permute-start | bytes 393224 | tf_op jit(solution)/shard_map/ppermute | solution.py:476
  28.5 13.0 %collective-permute-start.1 = (bf16[768,128]{1,0:T(8,128)(2,1)S(1)}, bf16[768,128]{1,0:T(8,128)(2,1)S(1)}, u32[]{:S(2)}, u32[]{:S(2)}) collective-permute-start(bf16[768,128]{1,0:T(8,128)(2,1)S(1)} %bitcast.18), channel_id=1, source_target_pairs={{0,1},{1,0},{2,3},{3,2},{4,5},{5,4},{6,7},{7,6},{8,9},{9,8},{10,11... | collective-permute-start | bytes 589832 | tf_op jit(solution)/shard_map/ppermute | solution.py:476
  30.1 8.5 %collective-permute-start.4 = (bf16[192,256]{1,0:T(8,128)(2,1)}, bf16[192,256]{1,0:T(8,128)(2,1)S(1)}, u32[]{:S(2)}, u32[]{:S(2)}) collective-permute-start(bf16[192,256]{1,0:T(8,128)(2,1)} %pack.1.refs_0_), channel_id=1, source_target_pairs={{0,16},{2,18},{4,20},{6,22},{8,24},{10,26},{12,28},{14,30},{16,0},... | collective-permute-start | bytes 294920 | tf_op jit(solution)/shard_map/ppermute | solution.py:487
  30.9 11.2 %collective-permute-start.5 = (bf16[192,256]{1,0:T(8,128)(2,1)}, bf16[192,256]{1,0:T(8,128)(2,1)S(1)}, u32[]{:S(2)}, u32[]{:S(2)}) collective-permute-start(bf16[192,256]{1,0:T(8,128)(2,1)} %pack.1.refs_0_), channel_id=1, source_target_pairs={{0,8},{2,10},{4,12},{6,14},{8,0},{10,2},{12,4},{14,6},{16,24},{18,... | collective-permute-start | bytes 294920 | tf_op jit(solution)/shard_map/ppermute | solution.py:487
  38.6 4.6 %collective-permute-start.6 = (bf16[192,256]{1,0:T(8,128)(2,1)S(1)}, bf16[192,256]{1,0:T(8,128)(2,1)S(1)}, u32[]{:S(2)}, u32[]{:S(2)}) collective-permute-start(bf16[192,256]{1,0:T(8,128)(2,1)S(1)} %collective-permute-done.4.refs_1_), channel_id=1, source_target_pairs={{0,8},{2,10},{4,12},{6,14},{8,0},{10,2},{12,4},{14,6},{16,24},{18,... | collective-permute-start | bytes 294920 | tf_op jit(solution)/shard_map/ppermute | solution.py:487
  38.6 1.2 %copy-start = (bf16[1,2048,256]{2,1,0:T(8,128)(2,1)S(1)}, bf16[1,2048,256]{2,1,0:T(8,128)(2,1)}, u32[]{:S(2)}) copy-start(bf16[1,2048,256]{2,1,0:T(8,128)(2,1)} %param.34) | copy-start | bytes 3145732
  39.8 3.4 %copy-start.3 = (bf16[192,256]{1,0:T(8,128)(2,1)S(1)}, bf16[192,256]{1,0:T(8,128)(2,1)}, u32[]{:S(2)}) copy-start(bf16[192,256]{1,0:T(8,128)(2,1)} %pack.1.refs_0_) | copy-start | bytes 294916
  42.0 5.0 %collective-permute-start.2 = (bf16[768,128]{1,0:T(8,128)(2,1)S(1)}, bf16[768,128]{1,0:T(8,128)(2,1)S(1)}, u32[]{:S(2)}, u32[]{:S(2)}) collective-permute-start(bf16[768,128]{1,0:T(8,128)(2,1)S(1)} %get-tuple-element.26), channel_id=1, source_target_pairs={{0,1},{1,0},{2,3},{3,2},{4,5},{5,4},{6,7},{7,6},{8,9},{9,8},{10,11... | collective-permute-start | bytes 589832 | tf_op jit(solution)/shard_map/ppermute | solution.py:476
  43.2 12.6 %collective-permute-start.7 = (bf16[768,256]{1,0:T(8,128)(2,1)S(1)}, bf16[768,256]{1,0:T(8,128)(2,1)S(1)}, u32[]{:S(2)}, u32[]{:S(2)}) collective-permute-start(bf16[768,256]{1,0:T(8,128)(2,1)S(1)} %join.1.refs_0_.refs_1_), channel_id=1, source_target_pairs={{0,2},{2,0},{4,6},{6,4},{8,10},{10,8},{12,14},{14,12},{16,18},{18,... | collective-permute-start | bytes 1179656 | tf_op jit(solution)/shard_map/ppermute | solution.py:487
  44.3 20.5 %collective-permute-start.8 = (bf16[768,256]{1,0:T(8,128)(2,1)S(1)}, bf16[768,256]{1,0:T(8,128)(2,1)S(1)}, u32[]{:S(2)}, u32[]{:S(2)}) collective-permute-start(bf16[768,256]{1,0:T(8,128)(2,1)S(1)} %join.1.refs_0_.refs_1_), channel_id=1, source_target_pairs={{0,4},{2,6},{4,0},{6,2},{8,12},{10,14},{12,8},{14,10},{16,20},{18,... | collective-permute-start | bytes 1179656 | tf_op jit(solution)/shard_map/ppermute | solution.py:487
  44.7 20.3 %collective-permute-start.9 = (bf16[768,256]{1,0:T(8,128)(2,1)S(1)}, bf16[768,256]{1,0:T(8,128)(2,1)S(1)}, u32[]{:S(2)}, u32[]{:S(2)}) collective-permute-start(bf16[768,256]{1,0:T(8,128)(2,1)S(1)} %join.1.refs_0_.refs_1_), channel_id=1, source_target_pairs={{0,6},{2,4},{4,2},{6,0},{8,14},{10,12},{12,10},{14,8},{16,22},{18,... | collective-permute-start | bytes 1179656 | tf_op jit(solution)/shard_map/ppermute | solution.py:487
  47.0 19.2 %copy-start.1 = (bf16[2048,64]{0,1:T(8,128)(2,1)S(1)}, bf16[2048,64]{0,1:T(8,128)(2,1)}, u32[]{:S(2)}) copy-start(bf16[2048,64]{0,1:T(8,128)(2,1)} %param.27) | copy-start | bytes 786436
  47.0 19.2 %copy-start.2 = (bf16[2048,64]{0,1:T(8,128)(2,1)S(1)}, bf16[2048,64]{0,1:T(8,128)(2,1)}, u32[]{:S(2)}) copy-start(bf16[2048,64]{0,1:T(8,128)(2,1)} %param.28) | copy-start | bytes 786436
  47.8 19.3 %copy-start.4 = (f32[2048]{0:T(1024)S(1)}, f32[2048]{0:T(1024)}, u32[]{:S(2)}) copy-start(f32[2048]{0:T(1024)} %param.40) | copy-start | bytes 24580
  47.8 19.3 %copy-start.5 = (f32[2048]{0:T(1024)S(1)}, f32[2048]{0:T(1024)}, u32[]{:S(2)}) copy-start(f32[2048]{0:T(1024)} %param.41) | copy-start | bytes 24580
  47.8 17.7 %all-to-all-start.1 = ((bf16[16,48,128]{2,1,0:T(8,128)(2,1)}), bf16[16,48,128]{2,1,0:T(8,128)(2,1)S(1)}, u32[]{:S(2)}, u32[]{:S(2)}) async-start(bf16[16,48,128]{2,1,0:T(8,128)(2,1)} %bitcast.11), calls=%async_computation.1 | async-start | bytes 393216 | tf_op jit(solution)/shard_map/all_to_all | solution.py:481
  65.4 1.7 %collective-permute-start.10 = (f32[16,2048]{1,0:T(8,128)S(1)}, f32[16,2048]{1,0:T(8,128)S(1)}, u32[]{:S(2)}, u32[]{:S(2)}) collective-permute-start(f32[16,2048]{1,0:T(8,128)S(1)} %dense.1), channel_id=1, source_target_pairs={{0,1},{1,0},{2,3},{3,2},{4,5},{5,4},{6,7},{7,6},{8,9},{9,8},{10,11... | collective-permute-start | bytes 393224 | tf_op jit(solution)/shard_map/ppermute | solution.py:476
  65.7 1.4 %collective-permute-start.3 = (f32[16,1024]{1,0:T(8,128)S(1)}, f32[16,1024]{1,0:T(8,128)S(1)}, u32[]{:S(2)}, u32[]{:S(2)}) collective-permute-start(f32[16,1024]{1,0:T(8,128)S(1)} %combine.1.own), channel_id=1, source_target_pairs={{0,1},{1,0},{2,3},{3,2},{4,5},{5,4},{6,7},{7,6},{8,9},{9,8},{10,11... | collective-permute-start | bytes 196616 | tf_op jit(solution)/shard_map/ppermute | solution.py:476
  (1 other events, 0.7 us)
